TPU v7x, 256 devices: a whole 4x4x8 slice. The times are simulated.
256 devices in a mesh: sp: 64 (over z, x, core), tp: 4 (over y).
Axes of the slice: x: 4, y: 4, z: 8, core: 2. Of those that a mesh axis runs over, the one named last changes fastest.
Arguments:
- moe_input: bfloat16 [16384, 2048], P('sp'), may hold values from -6 to 6
- out_cotangent: bfloat16 [16384, 2048], P('sp'), may hold values from -16 to 16
- routes: int32 [16384, 2], P('sp'), may hold values from 0 to 63, all different within a row; in each aligned block of 256 rows (0 to 255, 256 to 511, ...) at most 12 rows name the same one
- group_weight: float32 [16384], P('sp'), may hold values from 0.5 to 1
- inner_weight: float32 [16384, 2], P('sp'), may hold values from 0.3 to 1
- gate_weight: bfloat16 [64, 2048, 1024], P('sp', None, 'tp'), may hold values from -0.125 to 0.125
- up_weight: bfloat16 [64, 2048, 1024], P('sp', None, 'tp'), may hold values from -0.125 to 0.125
- down_weight: bfloat16 [64, 1024, 2048], P('sp', 'tp'), may hold values from -0.1875 to 0.1875
- value_in: bfloat16 [16384, 1024], P('sp', 'tp'), may hold values from -6 to 6
- gate_in: bfloat16 [16384, 1024], P('sp', 'tp'), may hold values from -6 to 6
- conv_taps: bfloat16 [31, 1024], P(None, 'tp'), may hold values from -1 to 1
- norm_hat: bfloat16 [16384, 1024], P('sp', 'tp'), may hold values from -6 to 6
- norm_rstd: float32 [16384], P('sp'), may hold values from 0.3 to 3
- norm_gain: float32 [1024], P('tp'), may hold values from 0.1 to 1.9
- out_proj: bfloat16 [2048, 1024], P(None, 'tp'), may hold values from -0.1875 to 0.1875
Outputs:
- gate_grad: bfloat16 [64, 2048, 1024], P('sp', None, 'tp')
- up_grad: bfloat16 [64, 2048, 1024], P('sp', None, 'tp')
- down_grad: bfloat16 [64, 1024, 2048], P('sp', 'tp')
- proj_grad: float32 [2048, 1024], P('sp', 'tp')
- value_grad: bfloat16 [16384, 1024], P('sp', 'tp')
- gate_in_grad: bfloat16 [16384, 1024], P('sp', 'tp')
Inputs may be any that keep to these rules, and one draw needn't show every extreme that they name: In the rows of one device (aligned blocks of 256 tokens) no expert is named by more than 12 routes, and in every draw some expert is named by exactly 12 in some block; a token's two experts differ.
All inputs are finite; a program needn't handle non-finite values.
Results may differ from a plain program's by a relative error of at most 0.009.
Values may be sent and summed in bfloat16 or wider, within the bound.
No kernel may reach another device: no remote copies, remote signals or barrier semaphores. Data moves between devices by JAX's collectives and lax.ppermute only.
A program may use at most 128 MiB of HBM per device.

v0:
```python
import jax
import jax.numpy as jnp
import numpy as np
from jax import lax
from jax.experimental import pallas as pl
from jax.experimental.pallas import tpu as pltpu
from jax.sharding import PartitionSpec as P


BF = jnp.bfloat16
F32 = jnp.float32
TOK = 256
WIDTH = 2048
HALF = 1024
QUART = 512
CH = 256
HID = 256
EXPERTS = 64
CAP = 12
SUB = 6
ROWS = 64 * SUB
SLOTS = 64 * 24
AUX = 512 + 256 + 16
VMEM_SMALL = 16 * 1024 * 1024
VMEM_LARGE = 24 * 1024 * 1024
VMEM_WHOLE = 60 * 1024 * 1024
PAIR_W = [(0, 1), (1, 0), (2, 3), (3, 2)]
PAIR_R = [(0, 3), (3, 0), (1, 2), (2, 1)]

NT = (((1,), (1,)), ((), ()))
TN = (((0,), (0,)), ((), ()))


def dot(a, b):
    return jnp.dot(a, b, preferred_element_type=F32)


def dotg(a, b, dims):
    return lax.dot_general(a, b, dims, preferred_element_type=F32)


def spot():
    j = lax.axis_index("tp")
    half = lax.shift_right_logical(j, 1)
    row_class = lax.rem(lax.shift_right_logical(j + 1, 1), 2)
    return j, half, row_class


def at(start, size):
    return pl.ds(pl.multiple_of(start, 128), size)


def call(body, outs, args, flops, in_place=(), scratch=(), vmem=VMEM_SMALL):
    bytes_moved = sum(a.size * a.dtype.itemsize for a in args) + sum(
        np.prod(s) * np.dtype(d).itemsize for s, d in outs
    )
    return pl.pallas_call(
        body,
        out_shape=[jax.ShapeDtypeStruct(s, d) for s, d in outs],
        in_specs=[
            pl.BlockSpec(memory_space=pltpu.HBM if i in in_place else pltpu.VMEM)
            for i in range(len(args))
        ],
        out_specs=[pl.BlockSpec(memory_space=pltpu.VMEM)] * len(outs),
        scratch_shapes=list(scratch),
        cost_estimate=pl.CostEstimate(
            flops=int(flops), bytes_accessed=int(bytes_moved), transcendentals=0
        ),
        compiler_params=pltpu.CompilerParams(vmem_limit_bytes=vmem),
    )(*args)


def slot_parts(i):
    who = lax.shift_right_logical(i * 2731, 16)
    rest = i - who * 24
    part = lax.shift_right_logical(rest * 43, 8)
    return who, part, rest - part * 6


def half_copy(from_ref, to_ref, sem, half):
    return pltpu.make_async_copy(from_ref.at[:, at(half * HALF, HALF)], to_ref, sem)


def pick_rows(code_first, code_second, row_class, data, send_ref, weights=None):
    step = 384
    who, part, rank = slot_parts(lax.broadcasted_iota(jnp.int32, (step, TOK), 0))
    base = who * CAP + rank
    for k in range(SLOTS // step):
        target = base + (k * (step // 24) * CAP + row_class * SUB)
        hit_first = target == code_first
        hit_second = target == code_second
        pick = jnp.where(hit_first, 1.0, jnp.where(hit_second, 1.0, 0.0))
        picks = jnp.concatenate(
            [jnp.where(part == q, pick, 0.0).astype(BF) for q in range(4)], axis=1
        )
        rows = dot(picks, data)
        if weights is not None:
            rows = rows * jnp.sum(
                jnp.where(hit_first, weights[0:1, :], 0.0)
                + jnp.where(hit_second, weights[1:2, :], 0.0),
                axis=1,
                keepdims=True,
            )
        send_ref[k * step : (k + 1) * step, :] = rows.astype(BF)


def stacked_quarters(buffer):
    return jnp.concatenate([buffer[:, q * 256 : (q + 1) * 256] for q in range(4)], axis=0)


def pack_input_body(routes_ref, input_ref, send_ref, row_ref, buffer, sem):
    _, half, row_class = spot()
    copy = half_copy(input_ref, buffer, sem, half)
    copy.start()
    experts = lax.broadcasted_iota(jnp.int32, (EXPERTS, TOK), 0)
    first, second = routes_ref[0:1, :], routes_ref[1:2, :]
    before = lax.broadcasted_iota(jnp.int32, (TOK, TOK), 0) < lax.broadcasted_iota(
        jnp.int32, (TOK, TOK), 1
    )
    before = jnp.where(before, 1.0, 0.0).astype(BF)
    one_first = jnp.where(experts == first, 1.0, 0.0)
    one_second = jnp.where(experts == second, 1.0, 0.0)
    count_first = dot(one_first.astype(BF), before)
    count_second = dot(one_second.astype(BF), before) + jnp.sum(one_first, axis=1, keepdims=True)
    rank_first = jnp.sum(one_first * count_first, axis=0, keepdims=True).astype(jnp.int32)
    rank_second = jnp.sum(one_second * count_second, axis=0, keepdims=True).astype(jnp.int32)
    code_first = first * CAP + rank_first
    code_second = second * CAP + rank_second
    row_ref[0:1, :] = code_first
    row_ref[1:2, :] = code_second
    copy.wait()
    pick_rows(code_first, code_second, row_class, stacked_quarters(buffer[...]), send_ref)


def pack_grad_body(row_ref, weight_ref, grad_ref, send_ref, code_ref, cols_ref, buffer, sem):
    j, half, row_class = spot()
    copy = half_copy(grad_ref, buffer, sem, half)
    copy.start()
    code_first, code_second = row_ref[0:1, :], row_ref[1:2, :]
    codes = jnp.concatenate(
        [
            jnp.broadcast_to(code_first.astype(F32), (64, TOK)),
            jnp.broadcast_to(code_second.astype(F32), (64, TOK)),
        ],
        axis=0,
    )
    code_ref[...] = jnp.transpose(codes)
    copy.wait()
    cols_ref[...] = buffer[:, at(lax.rem(j, 2) * QUART, QUART)]
    pick_rows(
        code_first,
        code_second,
        row_class,
        stacked_quarters(buffer[...]),
        send_ref,
        weight_ref[...],
    )


def unpack_body(recv_ref, perm_ref, out_ref):
    for group in range(8):
        rows = dot(perm_ref[...], recv_ref[group * 192 : (group + 1) * 192, :]).astype(BF)
        for q in range(4):
            out_ref[group * 48 : (group + 1) * 48, q * 256 : (q + 1) * 256] = rows[
                q * 48 : (q + 1) * 48
            ]


def whole_rows(own_ref, other_ref, half, out_ref):
    out_ref[:, at(half * HALF, HALF)] = own_ref[...]
    out_ref[:, at((1 - half) * HALF, HALF)] = other_ref[...]


def forward_body(own_ref, other_ref, wg_ref, wg2_ref, wu_ref, wu2_ref, x_ref, gate_ref, up_ref):
    _, half, _ = spot()
    whole_rows(own_ref, other_ref, half, x_ref)
    x = x_ref[...]
    gate_ref[:, :HID] = dot(x, wg_ref[...])
    gate_ref[:, HID:] = dot(x, wg2_ref[...])
    up_ref[:, :HID] = dot(x, wu_ref[...])
    up_ref[:, HID:] = dot(x, wu2_ref[...])


def partial_rows(gd, ud, gd2, ud2, wg_ref, wg2_ref, wu_ref, wu2_ref, start):
    rows = at(start, HALF)
    return (
        dotg(gd, wg_ref[rows, :], NT)
        + dotg(ud, wu_ref[rows, :], NT)
        + dotg(gd2, wg2_ref[rows, :], NT)
        + dotg(ud2, wu2_ref[rows, :], NT)
    )


def delta_body(
    own_ref, other_ref, gate_ref, up_ref, wd_ref, wd2_ref, wg_ref, wg2_ref, wu_ref, wu2_ref,
    g_ref, h_ref, h2_ref, gd_ref, gd2_ref, ud_ref, ud2_ref, send_ref,
):
    _, half, _ = spot()
    whole_rows(own_ref, other_ref, half, g_ref)
    g = g_ref[...]
    for k, (w_ref, ho, go, uo) in enumerate(
        ((wd_ref, h_ref, gd_ref, ud_ref), (wd2_ref, h2_ref, gd2_ref, ud2_ref))
    ):
        act_grad = dotg(g, w_ref[...], NT)
        gate = gate_ref[:, k * HID : (k + 1) * HID]
        up = up_ref[:, k * HID : (k + 1) * HID]
        sigma = jax.nn.sigmoid(gate)
        act = gate * sigma
        ho[...] = (act * up).astype(BF)
        go[...] = (act_grad * up * (sigma * (1.0 + gate * (1.0 - sigma)))).astype(BF)
        uo[...] = (act_grad * act).astype(BF)
    send_ref[...] = partial_rows(
        gd_ref[...], ud_ref[...], gd2_ref[...], ud2_ref[...],
        wg_ref, wg2_ref, wu_ref, wu2_ref, (1 - half) * HALF,
    ).astype(BF)


def keep_body(gd_ref, gd2_ref, ud_ref, ud2_ref, wg_ref, wg2_ref, wu_ref, wu2_ref, keep_ref):
    _, half, _ = spot()
    keep_ref[...] = partial_rows(
        gd_ref[...], ud_ref[...], gd2_ref[...], ud2_ref[...],
        wg_ref, wg2_ref, wu_ref, wu2_ref, half * HALF,
    )


def back_body(keep_ref, recv_ref, perm_ref, send_ref):
    for group in range(8):
        rows = slice(group * 48, (group + 1) * 48)
        total = (keep_ref[rows, :] + recv_ref[rows, :].astype(F32)).astype(BF)
        stacked = jnp.concatenate([total[:, q * 256 : (q + 1) * 256] for q in range(4)], axis=0)
        send_ref[group * 192 : (group + 1) * 192, :] = dot(perm_ref[...], stacked).astype(BF)


def combine_body(back_ref, code_ref, grad_ref, keep_ref, send_ref):
    j, _, row_class = spot()
    who, part, rank = slot_parts(lax.broadcasted_iota(jnp.int32, (1, SLOTS), 1))
    target = (who * CAP + rank + row_class * SUB).astype(F32)
    hit = jnp.where(
        target == code_ref[:, 0:1], 1.0, jnp.where(target == code_ref[:, 64:65], 1.0, 0.0)
    )
    kept = lax.rem(j, 2) * 2
    back = back_ref[...]
    for a in range(2):
        theirs = dot(jnp.where(part == 2 - kept + a, hit, 0.0).astype(BF), back)
        send_ref[:, a * 256 : (a + 1) * 256] = theirs.astype(BF)
    for a in range(2):
        cols = slice(a * 256, (a + 1) * 256)
        mine = dot(jnp.where(part == kept + a, hit, 0.0).astype(BF), back)
        keep_ref[:, cols] = grad_ref[:, cols].astype(F32) + mine


def aux_body(proj_ref, hat_ref, gain_ref, *out_refs):
    j, _, _ = spot()
    gain = gain_ref[...]
    top = gain.astype(BF)
    rest = gain - top.astype(F32)
    mid = rest.astype(BF)
    low = (rest - mid.astype(F32)).astype(BF)
    row = lax.broadcasted_iota(jnp.int32, (16, CH), 0)
    gains = jnp.where(
        row == 0,
        top.astype(F32),
        jnp.where(row == 1, mid.astype(F32), jnp.where(row == 2, low.astype(F32), 0.0)),
    ).astype(BF)
    for d, out_ref in enumerate(out_refs):
        to = lax.rem(j + d, 4)
        out_ref[0:512, :] = proj_ref[pl.ds(pl.multiple_of(to * 512, 512), 512), :]
        out_ref[512:768, :] = hat_ref[...]
        out_ref[768:784, :] = gains


def channel_body(
    b0_ref, b1_ref, b3_ref, b2_ref, row_ref, proj_ref, act_ref, slope_ref, hat_ref, rstd_ref
):
    rstd_ref[...] = jnp.transpose(jnp.broadcast_to(row_ref[...], (128, TOK)))
    j, _, _ = spot()
    for d, ref in zip((0, 1, 3, 2), (b0_ref, b1_ref, b3_ref, b2_ref)):
        cols = at(lax.rem(j + 4 - d, 4) * CH, CH)
        proj_ref[:, cols] = ref[0:512, :]
        hat = ref[512:768, :]
        gains = ref[768:784, :].astype(F32)
        gain = gains[0:1, :] + gains[1:2, :] + gains[2:3, :]
        normed = hat.astype(F32) * gain
        sigma = jax.nn.sigmoid(normed)
        hat_ref[:, cols] = hat
        act_ref[:, cols] = (normed * sigma).astype(BF)
        slope_ref[:, cols] = sigma * (1.0 + normed * (1.0 - sigma)) * gain


def mixed(keep_ref, recv_ref):
    return (keep_ref[...] + recv_ref[...].astype(F32)).astype(BF)


def outer_body(keep_ref, recv_ref, act_ref, own_ref, other_ref, turned_ref):
    mix = mixed(keep_ref, recv_ref)
    turned_ref[...] = jnp.transpose(mix.astype(F32))
    core = lax.rem(lax.axis_index("sp"), 2)

    def rows_of(parity):
        return jnp.concatenate(
            [
                turned_ref[pl.ds(pl.multiple_of((2 * b + parity) * 32, 32), 32), :]
                for b in range(8)
            ],
            axis=0,
        ).astype(BF)

    theirs, mine = rows_of(1 - core), rows_of(core)
    for k in range(4):
        act = act_ref[:, k * CH : (k + 1) * CH]
        other_ref[k * 256 : (k + 1) * 256, :] = dot(theirs, act).astype(BF)
        own_ref[k * 256 : (k + 1) * 256, :] = dot(mine, act)


def sum_body(own_ref, recv_ref, out_ref):
    out_ref[...] = (own_ref[...] + recv_ref[...].astype(F32)).astype(BF)


def silu_body(keep_ref, recv_ref, proj_ref, slope_ref, hat_ref, *refs):
    j, _, _ = spot()
    out_refs, part_ref = refs[:4], refs[4]
    mix = mixed(keep_ref, recv_ref)
    part = dot(mix, proj_ref[...])
    sloped = part * slope_ref[...]
    dotted = sloped * hat_ref[...].astype(F32)
    ones = jnp.ones((16, 4 * CH), BF)
    total = dotg(ones, sloped.astype(BF), NT)
    total_dot = dotg(ones, dotted.astype(BF), NT)
    row = lax.broadcasted_iota(jnp.int32, (16, TOK), 0)
    top, top_dot = total.astype(BF).astype(F32), total_dot.astype(BF).astype(F32)
    sums = jnp.where(
        row == 0,
        top,
        jnp.where(
            row == 1,
            total - top,
            jnp.where(row == 2, top_dot, jnp.where(row == 3, total_dot - top_dot, 0.0)),
        ),
    ).astype(BF)
    part_ref[...] = part
    for d, out_ref in enumerate(out_refs):
        out_ref[0:256, :] = part_ref[:, at(lax.rem(j + d, 4) * CH, CH)].astype(BF)
        out_ref[256:272, :] = sums


def conv_body(r0_ref, r1_ref, r2_ref, r3_ref, slope_ref, hat_ref, rstd_ref, out_ref, head_ref):
    j, _, _ = spot()
    recv_refs = (r0_ref, r1_ref, r2_ref, r3_ref)
    total = sum(ref[0:256, :].astype(F32) for ref in recv_refs)
    rows = jnp.concatenate([ref[256:272, :] for ref in recv_refs], axis=0)
    kind = lax.rem(lax.broadcasted_iota(jnp.int32, (64, CH), 0), 16)
    pick = jnp.where(kind < 2, 1.0, 0.0).astype(BF)
    pick_dot = jnp.where(kind < 2, 0.0, jnp.where(kind < 4, 1.0, 0.0)).astype(BF)
    mean = dotg(rows, pick, TN) * (1.0 / (4 * CH))
    mean_dot = dotg(rows, pick_dot, TN) * (1.0 / (4 * CH))
    hat_grad = total * slope_ref[:, at(j * CH, CH)]
    out_ref[...] = rstd_ref[:, 0:1] * (hat_grad - mean - hat_ref[...].astype(F32) * mean_dot)
    head_ref[...] = out_ref[0:32, :]


def taps_body(grad_ref, next_ref, taps_ref, gate_ref, value_ref, out_ref, gate_out_ref, long_ref):
    long_ref[0:256, :] = grad_ref[...]
    long_ref[256:288, :] = next_ref[...]
    for block in range(4):
        row = block * 64
        total = jnp.zeros((64, CH), F32)
        for k in range(31):
            tap = taps_ref[k : k + 1, :].astype(F32)
            total = total + tap * long_ref[row + 30 - k : row + 94 - k, :]
        rows = slice(row, row + 64)
        sigma = jax.nn.sigmoid(gate_ref[rows, :].astype(F32))
        out_ref[rows, :] = (total * sigma).astype(BF)
        gate_out_ref[rows, :] = (
            total * value_ref[rows, :].astype(F32) * sigma * (1.0 - sigma)
        ).astype(BF)


def around(blocks):
    return [lax.ppermute(blocks[d], "tp", [(i, (i + d) % 4) for i in range(4)]) for d in (1, 3, 2)]


def exchanged(array, **groups):
    return lax.all_to_all(array, "sp", split_axis=0, concat_axis=0, tiled=True, **groups)


def unmix_matrix():
    m = np.zeros((192, 192), np.float32)
    for q in range(4):
        for s in range(8):
            for r in range(6):
                m[q * 48 + s * 6 + r, s * 24 + q * 6 + r] = 1.0
    return m


def on_device(
    moe_input,
    out_cotangent,
    routes,
    group_weight,
    inner_weight,
    gate_weight,
    up_weight,
    down_weight,
    value_in,
    gate_in,
    conv_taps,
    norm_hat,
    norm_rstd,
    norm_gain,
    out_proj,
):
    sp_count = lax.axis_size("sp")
    unmix = unmix_matrix()
    unmix_to = jnp.asarray(unmix, BF)
    unmix_from = jnp.asarray(unmix.T, BF)
    wg, wu, wd = gate_weight[0], up_weight[0], down_weight[0]
    wg2 = lax.ppermute(wg, "tp", PAIR_W)
    wu2 = lax.ppermute(wu, "tp", PAIR_W)
    wd2 = lax.ppermute(wd, "tp", PAIR_W)

    route_weight = group_weight[None, :] * inner_weight.T
    buffer = [pltpu.VMEM((TOK, HALF), BF), pltpu.SemaphoreType.DMA]
    x_send, code_rows = call(
        pack_input_body,
        [((SLOTS, 256), BF), ((2, TOK), jnp.int32)],
        (routes.T, moe_input),
        2 * SLOTS * 1024 * 256,
        vmem=VMEM_WHOLE,
        in_place=(1,),
        scratch=buffer,
    )
    g_send, codes, own_cols = call(
        pack_grad_body,
        [((SLOTS, 256), BF), ((TOK, 128), F32), ((TOK, QUART), BF)],
        (code_rows, route_weight, out_cotangent),
        2 * SLOTS * 1024 * 256,
        in_place=(2,),
        scratch=buffer,
    )

    blocks = call(
        aux_body,
        [((AUX, CH), BF)] * 4,
        (out_proj, norm_hat, norm_gain[None, :]),
        0,
    )
    blocks = [blocks[0]] + around(blocks)
    proj_rows, act, slope, hat, rstd = call(
        channel_body,
        [((512, 4 * CH), BF), ((TOK, 4 * CH), BF), ((TOK, 4 * CH), F32), ((TOK, 4 * CH), BF), ((TOK, 128), F32)],
        (*blocks, norm_rstd[None, :]),
        0,
    )

    def dispatched(send):
        recv = exchanged(send.reshape(sp_count, 24, 256))
        (own,) = call(
            unpack_body,
            [((ROWS, HALF), BF)],
            (recv.reshape(SLOTS, 256), unmix_to),
            2 * SLOTS * 192 * 256,
        )
        return own, lax.ppermute(own, "tp", PAIR_R)

    x_own, x_other = dispatched(x_send)
    g_own, g_other = dispatched(g_send)
    x, gate_pre, up_pre = call(
        forward_body,
        [((ROWS, WIDTH), BF), ((ROWS, 2 * HID), F32), ((ROWS, 2 * HID), F32)],
        (x_own, x_other, wg, wg2, wu, wu2),
        2 * ROWS * WIDTH * 4 * HID,
        vmem=VMEM_LARGE,
    )
    small = ((ROWS, HID), BF)
    g, h, h2, gd, gd2, ud, ud2, rows_send = call(
        delta_body,
        [((ROWS, WIDTH), BF), small, small, small, small, small, small, ((ROWS, HALF), BF)],
        (g_own, g_other, gate_pre, up_pre, wd, wd2, wg, wg2, wu, wu2),
        2 * ROWS * WIDTH * 4 * HID,
        vmem=VMEM_LARGE,
    )
    rows_recv = lax.ppermute(rows_send, "tp", PAIR_R)
    (rows_keep,) = call(
        keep_body,
        [((ROWS, HALF), F32)],
        (gd, gd2, ud, ud2, wg, wg2, wu, wu2),
        2 * ROWS * HALF * 4 * HID,
        vmem=VMEM_LARGE,
    )

    def outer(a, b):
        return lax.dot_general(a, b, TN, preferred_element_type=F32)

    def finished(a, b, b_other):
        other = outer(*b_other).astype(BF)
        arrived = lax.ppermute(other, "tp", PAIR_W)
        return (outer(a, b) + arrived.astype(F32)).astype(BF)[None]

    gate_grad = finished(x, gd, (x, gd2))
    up_grad = finished(x, ud, (x, ud2))
    down_grad = finished(h, g, (h2, g))

    (back_send,) = call(
        back_body,
        [((SLOTS, 256), BF)],
        (rows_keep, rows_recv, unmix_from),
        2 * SLOTS * 192 * 256,
    )
    back = exchanged(back_send.reshape(sp_count, 24, 256))

    mix_keep, mix_send = call(
        combine_body,
        [((TOK, QUART), F32), ((TOK, QUART), BF)],
        (back.reshape(SLOTS, 256), codes, own_cols),
        2 * SLOTS * 1024 * 256,
    )
    mix_recv = lax.ppermute(mix_send, "tp", PAIR_W)
    outer_own, outer_other = call(
        outer_body,
        [((1024, CH), F32), ((1024, CH), BF)],
        (mix_keep, mix_recv, act),
        2 * TOK * 512 * 1024,
        scratch=[pltpu.VMEM((512, TOK), F32)],
    )
    outer_recv = lax.ppermute(outer_other, "sp", [(i, i ^ 1) for i in range(sp_count)])
    (outer_sum,) = call(sum_body, [((1024, CH), BF)], (outer_own, outer_recv), 0)
    pieces = exchanged(
        outer_sum.reshape(sp_count // 2, 32, CH),
        axis_index_groups=[list(range(c, sp_count, 2)) for c in range(2)],
    )
    piece = jnp.sum(pieces.astype(F32), axis=0)
    per_tp = sp_count // 4
    proj_grad = lax.ppermute(
        piece,
        ("sp", "tp"),
        [
            (s * 4 + t, (per_tp * t + s % per_tp) * 4 + s // per_tp)
            for s in range(sp_count)
            for t in range(4)
        ],
    )

    silu_parts = call(
        silu_body,
        [((272, CH), BF)] * 4,
        (mix_keep, mix_recv, proj_rows, slope, hat),
        2 * TOK * 512 * 1024,
        scratch=[pltpu.VMEM((TOK, 4 * CH), F32)],
    )
    silu_parts = [silu_parts[0]] + around(silu_parts)
    conv_grad, head = call(
        conv_body,
        [((TOK, CH), F32), ((32, CH), F32)],
        (*silu_parts, slope, norm_hat, rstd),
        0,
    )
    incoming = lax.ppermute(head, "sp", [(i, i - 1) for i in range(1, sp_count)])
    value_grad, gate_in_grad = call(
        taps_body,
        [((TOK, CH), BF), ((TOK, CH), BF)],
        (conv_grad, incoming, conv_taps, gate_in, value_in),
        0,
        scratch=[pltpu.VMEM((TOK + 32, CH), F32)],
    )
    return (gate_grad, up_grad, down_grad, proj_grad, value_grad, gate_in_grad)


def solution(mesh):
    return jax.shard_map(
        on_device,
        mesh=mesh,
        in_specs=(
            P("sp", None),
            P("sp", None),
            P("sp", None),
            P("sp"),
            P("sp", None),
            P("sp", None, "tp"),
            P("sp", None, "tp"),
            P("sp", "tp", None),
            P("sp", "tp"),
            P("sp", "tp"),
            P(None, "tp"),
            P("sp", "tp"),
            P("sp"),
            P("tp"),
            P(None, "tp"),
        ),
        out_specs=(
            P("sp", None, "tp"),
            P("sp", None, "tp"),
            P("sp", "tp", None),
            P("sp", "tp"),
            P("sp", "tp"),
            P("sp", "tp"),
        ),
        check_vma=False,
    )
```

profile of v0, /device:TPU:16, one launch (start us, length us, event | category | flops | bytes accessed | tf_op | source)
XLA Modules:
  0.0 285.1 jit_solution(14502565214559331979)
XLA Ops:
  0.7 3.7 %shard_map.208 = (bf16[1536,256]{1,0:T(8,128)(2,1)}, s32[2,256]{1,0:T(2,128)}) custom-call(s32[2,256]{1,0:T(2,128)} %bitcast.50, bf16[256,2048]{1,0:T(8,128)(2,1)} %input_ref.1), custom_call_target="tpu_custom_call" | custom-call | flops 805306368 | bytes 1839104 | tf_op jit(solution)/shard_map/pallas_call | solution.py:57
  4.4 11.9 %all-to-all-start = ((bf16[64,24,256]{2,1,0:T(8,128)(2,1)}), bf16[64,24,256]{2,1,0:T(8,128)(2,1)S(1)}, u32[]{:S(2)}, u32[]{:S(2)}) async-start(bf16[64,24,256]{2,1,0:T(8,128)(2,1)} %bitcast.49), calls=%async_computation | async-start | bytes 1572864 | tf_op jit(solution)/shard_map/all_to_all | solution.py:383
  16.4 1.2 copy-done.40
  17.6 1.3 shard_map.211
  19.9 19.7 %all-to-all-done = bf16[64,24,256]{2,1,0:T(8,128)(2,1)S(1)} async-done(((bf16[64,24,256]{2,1,0:T(8,128)(2,1)}), bf16[64,24,256]{2,1,0:T(8,128)(2,1)S(1)}, u32[]{:S(2)}, u32[]{:S(2)}) %all-to-all-start) | async-done | bytes 786464 | tf_op jit(solution)/shard_map/all_to_all | solution.py:383
  39.6 5.9 %all-to-all-start.1 = ((bf16[64,24,256]{2,1,0:T(8,128)(2,1)}), bf16[64,24,256]{2,1,0:T(8,128)(2,1)}, u32[]{:S(2)}, u32[]{:S(2)}) async-start(bf16[64,24,256]{2,1,0:T(8,128)(2,1)} %bitcast.45), calls=%async_computation.1 | async-start | bytes 1572864 | tf_op jit(solution)/shard_map/all_to_all | solution.py:383
  45.5 1.4 collective-permute-start.1
  47.6 1.3 collective-permute-start.4
  48.9 1.2 shard_map.209.own_ref
  50.2 18.4 %all-to-all-done.1 = bf16[64,24,256]{2,1,0:T(8,128)(2,1)} async-done(((bf16[64,24,256]{2,1,0:T(8,128)(2,1)}), bf16[64,24,256]{2,1,0:T(8,128)(2,1)}, u32[]{:S(2)}, u32[]{:S(2)}) %all-to-all-start.1) | async-done | bytes 786464 | tf_op jit(solution)/shard_map/all_to_all | solution.py:383
  68.6 1.5 shard_map.212.own_ref
  70.7 1.1 collective-permute-done.1.wg2_ref
  71.7 22.5 %collective-permute-done.2.wu2_ref = bf16[2048,256]{1,0:T(8,128)(2,1)} collective-permute-done((bf16[2048,256]{1,0:T(8,128)(2,1)S(1)}, bf16[2048,256]{1,0:T(8,128)(2,1)}, u32[]{:S(2)}, u32[]{:S(2)}) %collective-permute-start.2) | collective-permute-done | bytes 1048608 | tf_op jit(solution)/shard_map/ppermute | solution.py:418
  94.2 3.6 %shard_map.210 = (bf16[384,2048]{1,0:T(8,128)(2,1)S(1)}, f32[384,512]{1,0:T(8,128)S(1)}, f32[384,512]{1,0:T(8,128)S(1)}) custom-call(bf16[384,1024]{1,0:T(8,128)(2,1)} %shard_map.209.own_ref, bf16[384,1024]{1,0:T(8,128)(2,1)S(1)} %collective-permute-done.other_ref, bf16[2048,256]{1,0:T(8,128)(2,1)S(1)} %bitcast.34, ...), custom_call_target="tpu_custom_call" | custom-call | flops 1610612736 | bytes 8912896 | tf_op jit(solution)/shard_map/pallas_call | solution.py:57
  97.8 1.1 copy-done.41
  98.9 16.7 %collective-permute-done.4.wd2_ref = bf16[256,2048]{1,0:T(8,128)(2,1)} collective-permute-done((bf16[256,2048]{1,0:T(8,128)(2,1)}, bf16[256,2048]{1,0:T(8,128)(2,1)}, u32[]{:S(2)}, u32[]{:S(2)}) %collective-permute-start.4) | collective-permute-done | bytes 1048608 | tf_op jit(solution)/shard_map/ppermute | solution.py:419
  115.7 4.0 %shard_map.213 = (bf16[384,2048]{1,0:T(8,128)(2,1)S(1)}, bf16[384,256]{1,0:T(8,128)(2,1)S(1)}, bf16[384,256]{1,0:T(8,128)(2,1)S(1)}, bf16[384,256]{1,0:T(8,128)(...) custom-call(bf16[384,1024]{1,0:T(8,128)(2,1)S(1)} %shard_map.212.own, ...), custom_call_target="tpu_custom_call" | custom-call | flops 1610612736 | bytes 12976128 | tf_op jit(solution)/shard_map/pallas_call | solution.py:57
  120.5 2.6 shard_map.214.keep_ref
  123.1 15.5 %collective-permute-done.8.recv_ref = bf16[384,1024]{1,0:T(8,128)(2,1)S(1)} collective-permute-done((bf16[384,1024]{1,0:T(8,128)(2,1)S(1)}, bf16[384,1024]{1,0:T(8,128)(2,1)S(1)}, u32[]{:S(2)}, u32[]{:S(2)}) %collective-permute-start.8) | collective-permute-done | bytes 786464 | tf_op jit(solution)/shard_map/ppermute | solution.py:482
  138.6 1.3 shard_map.215
  139.9 10.6 %all-to-all-start.2 = ((bf16[64,24,256]{2,1,0:T(8,128)(2,1)}), bf16[64,24,256]{2,1,0:T(8,128)(2,1)S(1)}, u32[]{:S(2)}, u32[]{:S(2)}) async-start(bf16[64,24,256]{2,1,0:T(8,128)(2,1)} %bitcast.12), calls=%async_computation.2 | async-start | bytes 1572864 | tf_op jit(solution)/shard_map/all_to_all | solution.py:383
  150.6 1.1 shard_map.217
  152.4 2.5 collective-permute-start.10
  154.9 2.4 collective-permute-start.12
  157.3 16.5 %all-to-all-done.2 = bf16[64,24,256]{2,1,0:T(8,128)(2,1)S(1)} async-done(((bf16[64,24,256]{2,1,0:T(8,128)(2,1)}), bf16[64,24,256]{2,1,0:T(8,128)(2,1)S(1)}, u32[]{:S(2)}, u32[]{:S(2)}) %all-to-all-start.2) | async-done | bytes 786464 | tf_op jit(solution)/shard_map/all_to_all | solution.py:383
  174.7 1.1 copy-done.10
  178.7 2.6 collective-permute-start.9
  184.8 1.6 shard_map.218
  188.9 1.7 convolution_convert_fusion.1
  190.6 1.1 collective-permute-start.6
  191.7 1.7 convolution_convert_fusion.2
  195.3 5.2 %all-to-all-start.3 = ((bf16[32,32,256]{2,1,0:T(8,128)(2,1)}), bf16[32,32,256]{2,1,0:T(8,128)(2,1)}, u32[]{:S(2)}, u32[]{:S(2)}) async-start(bf16[32,32,256]{2,1,0:T(8,128)(2,1)} %bitcast.42), calls=%async_computation.3 | async-start | bytes 1048576 | tf_op jit(solution)/shard_map/all_to_all | solution.py:383
  200.5 2.8 convolution_convert_fusion
  203.3 1.1 collective-permute-start.7
  204.3 12.6 %collective-permute-done.6 = bf16[2048,256]{1,0:T(8,128)(2,1)} collective-permute-done((bf16[2048,256]{1,0:T(8,128)(2,1)}, bf16[2048,256]{1,0:T(8,128)(2,1)}, u32[]{:S(2)}, u32[]{:S(2)}) %collective-permute-start.6) | collective-permute-done | bytes 1048608 | tf_op jit(solution)/shard_map/ppermute | solution.py:496
  217.0 3.0 %fusion.4 = bf16[1,2048,256]{2,1,0:T(8,128)(2,1)} fusion(bf16[384,2048]{1,0:T(8,128)(2,1)S(1)} %copy-done.43, bf16[384,256]{1,0:T(8,128)(2,1)S(1)} %copy-done.24, bf16[2048,256]{1,0:T(8,128)(2,1)} %collective-permute-done.6), kind=kOutput, calls=%fused_computation.10 | convolution fusion | flops 404226048 | bytes 3866624 | tf_op jit(solution)/shard_map/dot_general | solution.py:492
  220.8 1.2 collective-permute-start.15
  222.9 1.4 collective-permute-start.17
  224.4 15.0 %collective-permute-done.5 = bf16[2048,256]{1,0:T(8,128)(2,1)} collective-permute-done((bf16[2048,256]{1,0:T(8,128)(2,1)}, bf16[2048,256]{1,0:T(8,128)(2,1)}, u32[]{:S(2)}, u32[]{:S(2)}) %collective-permute-start.5) | collective-permute-done | bytes 1048608 | tf_op jit(solution)/shard_map/ppermute | solution.py:496
  239.4 3.0 %fusion.5 = bf16[1,2048,256]{2,1,0:T(8,128)(2,1)} fusion(bf16[384,2048]{1,0:T(8,128)(2,1)S(1)} %copy-done.43, bf16[384,256]{1,0:T(8,128)(2,1)S(1)} %copy-done.22, bf16[2048,256]{1,0:T(8,128)(2,1)} %collective-permute-done.5), kind=kOutput, calls=%fused_computation.11 | convolution fusion | flops 404226048 | bytes 3866624 | tf_op jit(solution)/shard_map/dot_general | solution.py:492
  242.4 21.0 %collective-permute-done.15.r1_ref = bf16[272,256]{1,0:T(8,128)(2,1)S(1)} collective-permute-done((bf16[272,256]{1,0:T(8,128)(2,1)S(1)}, bf16[272,256]{1,0:T(8,128)(2,1)S(1)}, u32[]{:S(2)}, u32[]{:S(2)}) %collective-permute-start.15) | collective-permute-done | bytes 139296 | tf_op jit(solution)/shard_map/ppermute | solution.py:379
  263.4 1.4 collective-permute-done.16.r2_ref
  264.8 1.6 collective-permute-done.17.r3_ref
  266.7 1.3 collective-permute-start.18
  268.0 1.1 convert_reduce_fusion
  269.1 10.3 %collective-permute-start.14 = (f32[32,256]{1,0:T(8,128)S(1)}, f32[32,256]{1,0:T(8,128)S(1)}, u32[]{:S(2)}, u32[]{:S(2)}) collective-permute-start(f32[32,256]{1,0:T(8,128)S(1)} %convert_reduce_fusion), channel_id=1, source_target_pairs={{0,0},{1,64},{2,128},{3,192},{4,4},{5,68},{6,132},{7,196},{8,8},{9... | collective-permute-start | bytes 98312 | tf_op jit(solution)/shard_map/ppermute | solution.py:533
  279.5 3.0 %fusion.3 = bf16[1,256,2048]{2,1,0:T(8,128)(2,1)} fusion(bf16[384,256]{1,0:T(8,128)(2,1)S(1)} %copy-done.30, bf16[384,2048]{1,0:T(8,128)(2,1)S(1)} %get-tuple-element.54, bf16[256,2048]{1,0:T(8,128)(2,1)} %collective-permute-done.7), kind=kOutput, calls=%fused_computation.9 | convolution fusion | flops 404226048 | bytes 3866624 | tf_op jit(solution)/shard_map/dot_general | solution.py:492
  282.5 2.0 shard_map.223
  (125 shorter events, 18.0 us)
Async XLA Ops:
  0.6 15.7 %copy-start.49 = (f32[256,2]{0,1:T(2,128)S(1)}, f32[256,2]{0,1:T(2,128)}, u32[]{:S(2)}) copy-start(f32[256,2]{0,1:T(2,128)} %param.21) | copy-start | bytes 6148
  0.6 15.7 %copy-start.50 = (f32[256]{0:T(256)S(1)}, f32[256]{0:T(256)}, u32[]{:S(2)}) copy-start(f32[256]{0:T(256)} %param.20) | copy-start | bytes 3076
  4.4 12.0 %copy-start.48 = (s32[2,256]{1,0:T(2,128)S(1)}, s32[2,256]{1,0:T(2,128)}, u32[]{:S(2)}) copy-start(s32[2,256]{1,0:T(2,128)} %get-tuple-element.45.row_ref) | copy-start | bytes 6148
  4.4 35.2 %all-to-all-start = ((bf16[64,24,256]{2,1,0:T(8,128)(2,1)}), bf16[64,24,256]{2,1,0:T(8,128)(2,1)S(1)}, u32[]{:S(2)}, u32[]{:S(2)}) async-start(bf16[64,24,256]{2,1,0:T(8,128)(2,1)} %bitcast.49), calls=%async_computation | async-start | bytes 1572864 | tf_op jit(solution)/shard_map/all_to_all | solution.py:383
  17.6 27.9 %copy-start = (bf16[1,2048,256]{2,1,0:T(8,128)(2,1)S(1)}, bf16[1,2048,256]{2,1,0:T(8,128)(2,1)}, u32[]{:S(2)}) copy-start(bf16[1,2048,256]{2,1,0:T(8,128)(2,1)} %param.22) | copy-start | bytes 3145732
  17.6 29.3 %copy-start.1 = (bf16[1,2048,256]{2,1,0:T(8,128)(2,1)S(1)}, bf16[1,2048,256]{2,1,0:T(8,128)(2,1)}, u32[]{:S(2)}) copy-start(bf16[1,2048,256]{2,1,0:T(8,128)(2,1)} %param.23) | copy-start | bytes 3145732
  17.6 31.3 %copy-start.20 = (bf16[192,192]{1,0:T(8,128)(2,1)S(1)}, bf16[192,192]{1,0:T(8,128)(2,1)}, u32[]{:S(2)}) copy-start(bf16[192,192]{1,0:T(8,128)(2,1)} %constant.6.clone.perm_ref) | copy-start | bytes 221188
  19.9 30.3 %copy-start.44 = (bf16[256,512]{1,0:T(8,128)(2,1)}, bf16[256,512]{1,0:T(8,128)(2,1)S(1)}, u32[]{:S(2)}) copy-start(bf16[256,512]{1,0:T(8,128)(2,1)S(1)} %get-tuple-element.58.grad_ref) | copy-start | bytes 786436
  19.9 30.3 %copy-start.46 = (f32[256,128]{1,0:T(8,128)}, f32[256,128]{1,0:T(8,128)S(1)}, u32[]{:S(2)}) copy-start(f32[256,128]{1,0:T(8,128)S(1)} %get-tuple-element.57.code_ref) | copy-start | bytes 393220
  39.6 29.0 %all-to-all-start.1 = ((bf16[64,24,256]{2,1,0:T(8,128)(2,1)}), bf16[64,24,256]{2,1,0:T(8,128)(2,1)}, u32[]{:S(2)}, u32[]{:S(2)}) async-start(bf16[64,24,256]{2,1,0:T(8,128)(2,1)} %bitcast.45), calls=%async_computation.1 | async-start | bytes 1572864 | tf_op jit(solution)/shard_map/all_to_all | solution.py:383
  45.5 26.2 %collective-permute-start.1 = (bf16[2048,256]{1,0:T(8,128)(2,1)S(1)}, bf16[2048,256]{1,0:T(8,128)(2,1)}, u32[]{:S(2)}, u32[]{:S(2)}) collective-permute-start(bf16[2048,256]{1,0:T(8,128)(2,1)S(1)} %bitcast.33), channel_id=1, source_target_pairs={{0,1},{1,0},{2,3},{3,2},{4,5},{5,4},{6,7},{7,6},{8,9},{9,8},{10,11... | collective-permute-start | bytes 3145736 | tf_op jit(solution)/shard_map/ppermute | solution.py:417
  46.9 47.3 %collective-permute-start.2 = (bf16[2048,256]{1,0:T(8,128)(2,1)S(1)}, bf16[2048,256]{1,0:T(8,128)(2,1)}, u32[]{:S(2)}, u32[]{:S(2)}) collective-permute-start(bf16[2048,256]{1,0:T(8,128)(2,1)S(1)} %bitcast.37), channel_id=1, source_target_pairs={{0,1},{1,0},{2,3},{3,2},{4,5},{5,4},{6,7},{7,6},{8,9},{9,8},{10,11... | collective-permute-start | bytes 3145736 | tf_op jit(solution)/shard_map/ppermute | solution.py:418
  47.6 68.1 %collective-permute-start.4 = (bf16[256,2048]{1,0:T(8,128)(2,1)}, bf16[256,2048]{1,0:T(8,128)(2,1)}, u32[]{:S(2)}, u32[]{:S(2)}) collective-permute-start(bf16[256,2048]{1,0:T(8,128)(2,1)} %bitcast.43), channel_id=1, source_target_pairs={{0,1},{1,0},{2,3},{3,2},{4,5},{5,4},{6,7},{7,6},{8,9},{9,8},{10,11... | collective-permute-start | bytes 3145736 | tf_op jit(solution)/shard_map/ppermute | solution.py:419
  50.2 44.0 %collective-permute-start = (bf16[384,1024]{1,0:T(8,128)(2,1)}, bf16[384,1024]{1,0:T(8,128)(2,1)S(1)}, u32[]{:S(2)}, u32[]{:S(2)}) collective-permute-start(bf16[384,1024]{1,0:T(8,128)(2,1)} %shard_map.209.own_ref), channel_id=1, source_target_pairs={{0,3},{3,0},{1,2},{2,1},{4,7},{7,4},{5,6},{6,5},{8,11},{11,8},{9,1... | collective-permute-start | bytes 2359304 | tf_op jit(solution)/shard_map/ppermute | solution.py:463
  70.1 45.6 %copy-start.2 = (bf16[1,2048,256]{2,1,0:T(8,128)(2,1)S(1)}, bf16[1,2048,256]{2,1,0:T(8,128)(2,1)}, u32[]{:S(2)}) copy-start(bf16[1,2048,256]{2,1,0:T(8,128)(2,1)} %param.23) | copy-start | bytes 3145732
  70.1 45.6 %copy-start.4 = (bf16[1,256,2048]{2,1,0:T(8,128)(2,1)S(1)}, bf16[1,256,2048]{2,1,0:T(8,128)(2,1)}, u32[]{:S(2)}) copy-start(bf16[1,256,2048]{2,1,0:T(8,128)(2,1)} %param.24) | copy-start | bytes 3145732
  70.1 45.6 %collective-permute-start.3 = (bf16[384,1024]{1,0:T(8,128)(2,1)S(1)}, bf16[384,1024]{1,0:T(8,128)(2,1)S(1)}, u32[]{:S(2)}, u32[]{:S(2)}) collective-permute-start(bf16[384,1024]{1,0:T(8,128)(2,1)S(1)} %shard_map.212.own_ref), channel_id=1, source_target_pairs={{0,3},{3,0},{1,2},{2,1},{4,7},{7,4},{5,6},{6,5},{8,11},{11,8},{9,1... | collective-permute-start | bytes 2359304 | tf_op jit(solution)/shard_map/ppermute | solution.py:463
  119.8 20.1 %copy-start.31 = (bf16[384,256]{1,0:T(8,128)(2,1)}, bf16[384,256]{1,0:T(8,128)(2,1)S(1)}, u32[]{:S(2)}) copy-start(bf16[384,256]{1,0:T(8,128)(2,1)S(1)} %get-tuple-element.55) | copy-start | bytes 589828
  119.8 18.8 %collective-permute-start.8 = (bf16[384,1024]{1,0:T(8,128)(2,1)S(1)}, bf16[384,1024]{1,0:T(8,128)(2,1)S(1)}, u32[]{:S(2)}, u32[]{:S(2)}) collective-permute-start(bf16[384,1024]{1,0:T(8,128)(2,1)S(1)} %get-tuple-element.56), channel_id=1, source_target_pairs={{0,3},{3,0},{1,2},{2,1},{4,7},{7,4},{5,6},{6,5},{8,11},{11,8},{9,1... | collective-permute-start | bytes 2359304 | tf_op jit(solution)/shard_map/ppermute | solution.py:482
  120.5 18.1 %copy-start.36 = (bf16[192,192]{1,0:T(8,128)(2,1)S(1)}, bf16[192,192]{1,0:T(8,128)(2,1)}, u32[]{:S(2)}) copy-start(bf16[192,192]{1,0:T(8,128)(2,1)} %constant.7.clone.perm_ref) | copy-start | bytes 221188
  139.9 10.6 %copy-start.5 = (bf16[2048,256]{1,0:T(8,128)(2,1)S(1)}, bf16[2048,256]{1,0:T(8,128)(2,1)}, u32[]{:S(2)}) copy-start(bf16[2048,256]{1,0:T(8,128)(2,1)} %proj_ref.1) | copy-start | bytes 3145732
  139.9 10.7 %copy-start.11 = (bf16[256,256]{1,0:T(8,128)(2,1)S(1)}, bf16[256,256]{1,0:T(8,128)(2,1)}, u32[]{:S(2)}) copy-start(bf16[256,256]{1,0:T(8,128)(2,1)} %hat_ref.3) | copy-start | bytes 393220
  139.9 10.7 %copy-start.38 = (f32[256]{0:T(256)S(1)}, f32[256]{0:T(256)}, u32[]{:S(2)}) copy-start(f32[256]{0:T(256)} %param.30) | copy-start | bytes 3076
  139.9 33.9 %all-to-all-start.2 = ((bf16[64,24,256]{2,1,0:T(8,128)(2,1)}), bf16[64,24,256]{2,1,0:T(8,128)(2,1)S(1)}, u32[]{:S(2)}, u32[]{:S(2)}) async-start(bf16[64,24,256]{2,1,0:T(8,128)(2,1)} %bitcast.12), calls=%async_computation.2 | async-start | bytes 1572864 | tf_op jit(solution)/shard_map/all_to_all | solution.py:383
  152.4 30.3 %copy-start.39 = (f32[256]{0:T(256)S(1)}, f32[256]{0:T(256)}, u32[]{:S(2)}) copy-start(f32[256]{0:T(256)} %param.29) | copy-start | bytes 3076
  152.4 28.8 %collective-permute-start.10 = (bf16[784,256]{1,0:T(8,128)(2,1)}, bf16[784,256]{1,0:T(8,128)(2,1)S(1)}, u32[]{:S(2)}, u32[]{:S(2)}) collective-permute-start(bf16[784,256]{1,0:T(8,128)(2,1)} %get-tuple-element.62), channel_id=1, source_target_pairs={{0,1},{1,2},{2,3},{3,0},{4,5},{5,6},{6,7},{7,4},{8,9},{9,10},{10,1... | collective-permute-start | bytes 1204232 | tf_op jit(solution)/shard_map/ppermute | solution.py:379
  154.9 27.1 %collective-permute-start.11 = (bf16[784,256]{1,0:T(8,128)(2,1)}, bf16[784,256]{1,0:T(8,128)(2,1)S(1)}, u32[]{:S(2)}, u32[]{:S(2)}) collective-permute-start(bf16[784,256]{1,0:T(8,128)(2,1)} %get-tuple-element.63), channel_id=1, source_target_pairs={{0,3},{1,0},{2,1},{3,2},{4,7},{5,4},{6,5},{7,6},{8,11},{9,8},{10,9... | collective-permute-start | bytes 1204232 | tf_op jit(solution)/shard_map/ppermute | solution.py:379
  154.9 27.8 %collective-permute-start.12 = (bf16[784,256]{1,0:T(8,128)(2,1)}, bf16[784,256]{1,0:T(8,128)(2,1)}, u32[]{:S(2)}, u32[]{:S(2)}) collective-permute-start(bf16[784,256]{1,0:T(8,128)(2,1)} %get-tuple-element.64), channel_id=1, source_target_pairs={{0,2},{1,3},{2,0},{3,1},{4,6},{5,7},{6,4},{7,5},{8,10},{9,11},{10,... | collective-permute-start | bytes 1204232 | tf_op jit(solution)/shard_map/ppermute | solution.py:379
  177.6 11.2 %copy-start.28 = (bf16[384,256]{1,0:T(8,128)(2,1)S(1)}, bf16[384,256]{1,0:T(8,128)(2,1)}, u32[]{:S(2)}) copy-start(bf16[384,256]{1,0:T(8,128)(2,1)} %copy-done.27) | copy-start | bytes 589828
  177.6 11.2 %copy-start.42 = (bf16[384,2048]{1,0:T(8,128)(2,1)S(1)}, bf16[384,2048]{1,0:T(8,128)(2,1)}, u32[]{:S(2)}) copy-start(bf16[384,2048]{1,0:T(8,128)(2,1)} %copy-done.41) | copy-start | bytes 4718596
  178.7 9.5 %collective-permute-start.9 = (bf16[256,512]{1,0:T(8,128)(2,1)S(1)}, bf16[256,512]{1,0:T(8,128)(2,1)S(1)}, u32[]{:S(2)}, u32[]{:S(2)}) collective-permute-start(bf16[256,512]{1,0:T(8,128)(2,1)S(1)} %get-tuple-element.60), channel_id=1, source_target_pairs={{0,1},{1,0},{2,3},{3,2},{4,5},{5,4},{6,7},{7,6},{8,9},{9,8},{10,11... | collective-permute-start | bytes 786440 | tf_op jit(solution)/shard_map/ppermute | solution.py:517
  188.7 5.6 %collective-permute-start.13 = (bf16[1024,256]{1,0:T(8,128)(2,1)S(1)}, bf16[1024,256]{1,0:T(8,128)(2,1)S(1)}, u32[]{:S(2)}, u32[]{:S(2)}) collective-permute-start(bf16[1024,256]{1,0:T(8,128)(2,1)S(1)} %get-tuple-element.67), channel_id=1, source_target_pairs={{0,4},{4,0},{8,12},{12,8},{16,20},{20,16},{24,28},{28,24},{32,36},... | collective-permute-start | bytes 1572872 | tf_op jit(solution)/shard_map/ppermute | solution.py:525
  190.6 26.3 %collective-permute-start.6 = (bf16[2048,256]{1,0:T(8,128)(2,1)}, bf16[2048,256]{1,0:T(8,128)(2,1)}, u32[]{:S(2)}, u32[]{:S(2)}) collective-permute-start(bf16[2048,256]{1,0:T(8,128)(2,1)} %convolution_convert_fusion.1), channel_id=1, source_target_pairs={{0,1},{1,0},{2,3},{3,2},{4,5},{5,4},{6,7},{7,6},{8,9},{9,8},{10,11... | collective-permute-start | bytes 3145736 | tf_op jit(solution)/shard_map/ppermute | solution.py:496
  193.4 46.0 %collective-permute-start.5 = (bf16[2048,256]{1,0:T(8,128)(2,1)}, bf16[2048,256]{1,0:T(8,128)(2,1)}, u32[]{:S(2)}, u32[]{:S(2)}) collective-permute-start(bf16[2048,256]{1,0:T(8,128)(2,1)} %convolution_convert_fusion.2), channel_id=1, source_target_pairs={{0,1},{1,0},{2,3},{3,2},{4,5},{5,4},{6,7},{7,6},{8,9},{9,8},{10,11... | collective-permute-start | bytes 3145736 | tf_op jit(solution)/shard_map/ppermute | solution.py:496
  195.3 72.7 %all-to-all-start.3 = ((bf16[32,32,256]{2,1,0:T(8,128)(2,1)}), bf16[32,32,256]{2,1,0:T(8,128)(2,1)}, u32[]{:S(2)}, u32[]{:S(2)}) async-start(bf16[32,32,256]{2,1,0:T(8,128)(2,1)} %bitcast.42), calls=%async_computation.3 | async-start | bytes 1048576 | tf_op jit(solution)/shard_map/all_to_all | solution.py:383
  200.5 16.5 %copy-start.24 = (bf16[384,256]{1,0:T(8,128)(2,1)S(1)}, bf16[384,256]{1,0:T(8,128)(2,1)}, u32[]{:S(2)}) copy-start(bf16[384,256]{1,0:T(8,128)(2,1)} %copy-done.23) | copy-start | bytes 589828
  200.5 16.5 %copy-start.43 = (bf16[384,2048]{1,0:T(8,128)(2,1)S(1)}, bf16[384,2048]{1,0:T(8,128)(2,1)}, u32[]{:S(2)}) copy-start(bf16[384,2048]{1,0:T(8,128)(2,1)} %copy-done.41) | copy-start | bytes 4718596
  203.2 16.7 %copy-start.7 = (bf16[512,1024]{1,0:T(8,128)(2,1)S(1)}, bf16[512,1024]{1,0:T(8,128)(2,1)}, u32[]{:S(2)}) copy-start(bf16[512,1024]{1,0:T(8,128)(2,1)} %copy-done.6) | copy-start | bytes 3145732
  203.3 16.7 %copy-start.13 = (bf16[256,1024]{1,0:T(8,128)(2,1)S(1)}, bf16[256,1024]{1,0:T(8,128)(2,1)}, u32[]{:S(2)}) copy-start(bf16[256,1024]{1,0:T(8,128)(2,1)} %copy-done.12) | copy-start | bytes 1572868
  203.3 76.2 %collective-permute-start.7 = (bf16[256,2048]{1,0:T(8,128)(2,1)}, bf16[256,2048]{1,0:T(8,128)(2,1)}, u32[]{:S(2)}, u32[]{:S(2)}) collective-permute-start(bf16[256,2048]{1,0:T(8,128)(2,1)} %convolution_convert_fusion), channel_id=1, source_target_pairs={{0,1},{1,0},{2,3},{3,2},{4,5},{5,4},{6,7},{7,6},{8,9},{9,8},{10,11... | collective-permute-start | bytes 3145736 | tf_op jit(solution)/shard_map/ppermute | solution.py:496
  219.9 19.5 %copy-start.22 = (bf16[384,256]{1,0:T(8,128)(2,1)S(1)}, bf16[384,256]{1,0:T(8,128)(2,1)}, u32[]{:S(2)}) copy-start(bf16[384,256]{1,0:T(8,128)(2,1)} %copy-done.21) | copy-start | bytes 589828
  220.8 42.6 %collective-permute-start.15 = (bf16[272,256]{1,0:T(8,128)(2,1)S(1)}, bf16[272,256]{1,0:T(8,128)(2,1)S(1)}, u32[]{:S(2)}, u32[]{:S(2)}) collective-permute-start(bf16[272,256]{1,0:T(8,128)(2,1)S(1)} %get-tuple-element.72), channel_id=1, source_target_pairs={{0,1},{1,2},{2,3},{3,0},{4,5},{5,6},{6,7},{7,4},{8,9},{9,10},{10,1... | collective-permute-start | bytes 417800 | tf_op jit(solution)/shard_map/ppermute | solution.py:379
  222.0 42.7 %collective-permute-start.16 = (bf16[272,256]{1,0:T(8,128)(2,1)S(1)}, bf16[272,256]{1,0:T(8,128)(2,1)S(1)}, u32[]{:S(2)}, u32[]{:S(2)}) collective-permute-start(bf16[272,256]{1,0:T(8,128)(2,1)S(1)} %get-tuple-element.73), channel_id=1, source_target_pairs={{0,3},{1,0},{2,1},{3,2},{4,7},{5,4},{6,5},{7,6},{8,11},{9,8},{10,9... | collective-permute-start | bytes 417800 | tf_op jit(solution)/shard_map/ppermute | solution.py:379
  222.9 43.5 %copy-start.33 = (f32[256,128]{1,0:T(8,128)S(1)}, f32[256,128]{1,0:T(8,128)}, u32[]{:S(2)}) copy-start(f32[256,128]{1,0:T(8,128)} %copy-done.32) | copy-start | bytes 393220
  222.9 43.5 %collective-permute-start.17 = (bf16[272,256]{1,0:T(8,128)(2,1)S(1)}, bf16[272,256]{1,0:T(8,128)(2,1)S(1)}, u32[]{:S(2)}, u32[]{:S(2)}) collective-permute-start(bf16[272,256]{1,0:T(8,128)(2,1)S(1)} %get-tuple-element.74), channel_id=1, source_target_pairs={{0,2},{1,3},{2,0},{3,1},{4,6},{5,7},{6,4},{7,5},{8,10},{9,11},{10,... | collective-permute-start | bytes 417800 | tf_op jit(solution)/shard_map/ppermute | solution.py:379
  242.4 37.1 %copy-start.30 = (bf16[384,256]{1,0:T(8,128)(2,1)S(1)}, bf16[384,256]{1,0:T(8,128)(2,1)}, u32[]{:S(2)}) copy-start(bf16[384,256]{1,0:T(8,128)(2,1)} %copy-done.29) | copy-start | bytes 589828
  266.7 15.8 %collective-permute-start.18 = (f32[32,256]{1,0:T(8,128)S(1)}, f32[32,256]{1,0:T(8,128)S(1)}, u32[]{:S(2)}, u32[]{:S(2)}) collective-permute-start(f32[32,256]{1,0:T(8,128)S(1)} %get-tuple-element.77), channel_id=1, source_target_pairs={{4,0},{8,4},{12,8},{16,12},{20,16},{24,20},{28,24},{32,28},{36,32}... | collective-permute-start | bytes 98312 | tf_op jit(solution)/shard_map/ppermute | solution.py:557
  269.1 15.4 %collective-permute-start.14 = (f32[32,256]{1,0:T(8,128)S(1)}, f32[32,256]{1,0:T(8,128)S(1)}, u32[]{:S(2)}, u32[]{:S(2)}) collective-permute-start(f32[32,256]{1,0:T(8,128)S(1)} %convert_reduce_fusion), channel_id=1, source_target_pairs={{0,0},{1,64},{2,128},{3,192},{4,4},{5,68},{6,132},{7,196},{8,8},{9... | collective-permute-start | bytes 98312 | tf_op jit(solution)/shard_map/ppermute | solution.py:533
  (26 other events, 50.2 us)
where the time goes:
time: 286 us; the launch traced here: 285 us
  waiting for transfers between devices  162 us (57%)
  starting transfers between devices  64.1 us (22%)
  Pallas kernels  26.9 us (9%)
  matrix products  15.1 us (5%)
  local copies, waits for them, and re-layouts  14.7 us (5%)
    all_to_all x4, waiting for transfers between devices, exchanged(): lax.all_to_all(array, 'sp', split_axis=0, concat_axis=0, tiled=True, **gr...  54.7 us
    all_to_all x4, starting transfers between devices, exchanged(): lax.all_to_all(array, 'sp', split_axis=0, concat_axis=0, tiled=True, **gr...  33.6 us
    ppermute x3, waiting for transfers between devices, finished(): arrived = lax.ppermute(other, 'tp', PAIR_W)  27.7 us
    pallas_call x16, Pallas kernels, call(): pl.pallas_call(body, out_shape=[jax.ShapeDtypeStruct(s, d) for s, d in ou...  26.9 us
    ppermute x6, waiting for transfers between devices, around(): lax.ppermute(blocks[d], 'tp', [(i, (i + d) % 4) for i in range(4)])  24 us
    ppermute x1, waiting for transfers between devices, on_device(): wu2 = lax.ppermute(wu, 'tp', PAIR_W)  22.5 us
    ppermute x1, waiting for transfers between devices, on_device(): wd2 = lax.ppermute(wd, 'tp', PAIR_W)  16.7 us
    ppermute x1, waiting for transfers between devices, on_device(): rows_recv = lax.ppermute(rows_send, 'tp', PAIR_R)  15.5 us
  transfers between devices with their start and end apart: 23, of which 12 were waited for; matrix products, arithmetic and copies ran while one was open for 6% of the time, Pallas kernels for 6%

commit v1 on v0

--- a/solution.py
+++ b/solution.py
@@ -19,6 +19,7 @@
 CAP = 12
 SUB = 6
 ROWS = 64 * SUB
+PART = ROWS // 2
 SLOTS = 64 * 24
 AUX = 512 + 256 + 16
 VMEM_SMALL = 16 * 1024 * 1024
@@ -44,6 +45,10 @@
     half = lax.shift_right_logical(j, 1)
     row_class = lax.rem(lax.shift_right_logical(j + 1, 1), 2)
     return j, half, row_class
+
+
+def peers(j):
+    return 3 - j, j + 1 - 2 * lax.rem(j, 2), lax.rem(j + 2, 4)
 
 
 def at(start, size):
@@ -157,13 +162,14 @@
     )
 
 
-def unpack_body(recv_ref, perm_ref, out_ref):
+def unpack_body(recv_ref, perm_ref, *out_refs):
+    each = 8 // len(out_refs)
     for group in range(8):
         rows = dot(perm_ref[...], recv_ref[group * 192 : (group + 1) * 192, :]).astype(BF)
+        out_ref = out_refs[group // each]
+        to = slice(group % each * 48, (group % each + 1) * 48)
         for q in range(4):
-            out_ref[group * 48 : (group + 1) * 48, q * 256 : (q + 1) * 256] = rows[
-                q * 48 : (q + 1) * 48
-            ]
+            out_ref[to, q * 256 : (q + 1) * 256] = rows[q * 48 : (q + 1) * 48]
 
 
 def whole_rows(own_ref, other_ref, half, out_ref):
@@ -171,14 +177,15 @@
     out_ref[:, at((1 - half) * HALF, HALF)] = other_ref[...]
 
 
-def forward_body(own_ref, other_ref, wg_ref, wg2_ref, wu_ref, wu2_ref, x_ref, gate_ref, up_ref):
+def forward_body(own_ref, other_ref, wg_ref, wg2_ref, wu_ref, wu2_ref, x_ref, *out_refs):
     _, half, _ = spot()
     whole_rows(own_ref, other_ref, half, x_ref)
     x = x_ref[...]
-    gate_ref[:, :HID] = dot(x, wg_ref[...])
-    gate_ref[:, HID:] = dot(x, wg2_ref[...])
-    up_ref[:, :HID] = dot(x, wu_ref[...])
-    up_ref[:, HID:] = dot(x, wu2_ref[...])
+    for k, w_ref in enumerate((wg_ref, wg2_ref, wu_ref, wu2_ref)):
+        made = dot(x, w_ref[...])
+        cols = slice(k % 2 * HID, (k % 2 + 1) * HID)
+        out_refs[k // 2][:, cols] = made[0:PART]
+        out_refs[2 + k // 2][:, cols] = made[PART:ROWS]
 
 
 def partial_rows(gd, ud, gd2, ud2, wg_ref, wg2_ref, wu_ref, wu2_ref, start):
@@ -193,15 +200,25 @@
 
 def delta_body(
     own_ref, other_ref, gate_ref, up_ref, wd_ref, wd2_ref, wg_ref, wg2_ref, wu_ref, wu2_ref,
-    g_ref, h_ref, h2_ref, gd_ref, gd2_ref, ud_ref, ud2_ref, send_ref,
+    g_ref, h_ref, h2_ref, gd_ref, gd2_ref, ud_ref, ud2_ref, send_ref, down_buf, in_buf, sems,
 ):
     _, half, _ = spot()
+    start = pl.multiple_of((1 - half) * HALF, HALF)
+    copies = [
+        pltpu.make_async_copy(ref, down_buf.at[k], sems.at[k])
+        for k, ref in enumerate((wd_ref, wd2_ref))
+    ] + [
+        pltpu.make_async_copy(ref.at[pl.ds(start, HALF), :], in_buf.at[k], sems.at[2 + k])
+        for k, ref in enumerate((wg_ref, wu_ref, wg2_ref, wu2_ref))
+    ]
+    for copy in copies:
+        copy.start()
     whole_rows(own_ref, other_ref, half, g_ref)
     g = g_ref[...]
-    for k, (w_ref, ho, go, uo) in enumerate(
-        ((wd_ref, h_ref, gd_ref, ud_ref), (wd2_ref, h2_ref, gd2_ref, ud2_ref))
-    ):
-        act_grad = dotg(g, w_ref[...], NT)
+    total = jnp.zeros((PART, HALF), F32)
+    for k, (ho, go, uo) in enumerate(((h_ref, gd_ref, ud_ref), (h2_ref, gd2_ref, ud2_ref))):
+        copies[k].wait()
+        act_grad = dotg(g, down_buf[k], NT)
         gate = gate_ref[:, k * HID : (k + 1) * HID]
         up = up_ref[:, k * HID : (k + 1) * HID]
         sigma = jax.nn.sigmoid(gate)
@@ -209,10 +226,17 @@
         ho[...] = (act * up).astype(BF)
         go[...] = (act_grad * up * (sigma * (1.0 + gate * (1.0 - sigma)))).astype(BF)
         uo[...] = (act_grad * act).astype(BF)
-    send_ref[...] = partial_rows(
-        gd_ref[...], ud_ref[...], gd2_ref[...], ud2_ref[...],
-        wg_ref, wg2_ref, wu_ref, wu2_ref, (1 - half) * HALF,
-    ).astype(BF)
+    for k, ref in enumerate((gd_ref, ud_ref, gd2_ref, ud2_ref)):
+        copies[2 + k].wait()
+        total = total + dotg(ref[...], in_buf[k], NT)
+    send_ref[...] = total.astype(BF)
+
+
+def join_body(*refs):
+    count = len(refs) // 3
+    for k in range(count):
+        refs[2 * count + k][0:PART, :] = refs[k][...]
+        refs[2 * count + k][PART:ROWS, :] = refs[count + k][...]
 
 
 def keep_body(gd_ref, gd2_ref, ud_ref, ud2_ref, wg_ref, wg2_ref, wu_ref, wu2_ref, keep_ref):
@@ -223,10 +247,12 @@
     )
 
 
-def back_body(keep_ref, recv_ref, perm_ref, send_ref):
+def back_body(keep_ref, first_ref, second_ref, perm_ref, send_ref):
     for group in range(8):
         rows = slice(group * 48, (group + 1) * 48)
-        total = (keep_ref[rows, :] + recv_ref[rows, :].astype(F32)).astype(BF)
+        recv_ref = second_ref if group >= 4 else first_ref
+        recv = recv_ref[group % 4 * 48 : (group % 4 + 1) * 48, :]
+        total = (keep_ref[rows, :] + recv.astype(F32)).astype(BF)
         stacked = jnp.concatenate([total[:, q * 256 : (q + 1) * 256] for q in range(4)], axis=0)
         send_ref[group * 192 : (group + 1) * 192, :] = dot(perm_ref[...], stacked).astype(BF)
 
@@ -262,20 +288,19 @@
         top.astype(F32),
         jnp.where(row == 1, mid.astype(F32), jnp.where(row == 2, low.astype(F32), 0.0)),
     ).astype(BF)
-    for d, out_ref in enumerate(out_refs):
-        to = lax.rem(j + d, 4)
+    for to, out_ref in zip((j, *peers(j)), out_refs):
         out_ref[0:512, :] = proj_ref[pl.ds(pl.multiple_of(to * 512, 512), 512), :]
         out_ref[512:768, :] = hat_ref[...]
         out_ref[768:784, :] = gains
 
 
 def channel_body(
-    b0_ref, b1_ref, b3_ref, b2_ref, row_ref, proj_ref, act_ref, slope_ref, hat_ref, rstd_ref
+    own_ref, across_ref, beside_ref, opposite_ref, row_ref, proj_ref, act_ref, slope_ref, hat_ref, rstd_ref
 ):
     rstd_ref[...] = jnp.transpose(jnp.broadcast_to(row_ref[...], (128, TOK)))
     j, _, _ = spot()
-    for d, ref in zip((0, 1, 3, 2), (b0_ref, b1_ref, b3_ref, b2_ref)):
-        cols = at(lax.rem(j + 4 - d, 4) * CH, CH)
+    for owner, ref in zip((j, *peers(j)), (own_ref, across_ref, beside_ref, opposite_ref)):
+        cols = at(owner * CH, CH)
         proj_ref[:, cols] = ref[0:512, :]
         hat = ref[512:768, :]
         gains = ref[768:784, :].astype(F32)
@@ -444,42 +469,56 @@
         (out_proj, norm_hat, norm_gain[None, :]),
         0,
     )
-    blocks = [blocks[0]] + around(blocks)
+    across = lax.ppermute(blocks[1], "tp", PAIR_R)
+    relayed = lax.ppermute(blocks[3], "tp", PAIR_R)
+    beside = lax.ppermute(blocks[2], "tp", PAIR_W)
+    opposite = lax.ppermute(relayed, "tp", PAIR_W)
     proj_rows, act, slope, hat, rstd = call(
         channel_body,
         [((512, 4 * CH), BF), ((TOK, 4 * CH), BF), ((TOK, 4 * CH), F32), ((TOK, 4 * CH), BF), ((TOK, 128), F32)],
-        (*blocks, norm_rstd[None, :]),
+        (blocks[0], across, beside, opposite, norm_rstd[None, :]),
         0,
     )
 
-    def dispatched(send):
+    def dispatched(send, parts):
         recv = exchanged(send.reshape(sp_count, 24, 256))
-        (own,) = call(
+        own = call(
             unpack_body,
-            [((ROWS, HALF), BF)],
+            [((ROWS // parts, HALF), BF)] * parts,
             (recv.reshape(SLOTS, 256), unmix_to),
             2 * SLOTS * 192 * 256,
         )
-        return own, lax.ppermute(own, "tp", PAIR_R)
-
-    x_own, x_other = dispatched(x_send)
-    g_own, g_other = dispatched(g_send)
-    x, gate_pre, up_pre = call(
+        return own, [lax.ppermute(v, "tp", PAIR_R) for v in own]
+
+    (x_own,), (x_other,) = dispatched(x_send, 1)
+    g_own, g_other = dispatched(g_send, 2)
+    x, *pre = call(
         forward_body,
-        [((ROWS, WIDTH), BF), ((ROWS, 2 * HID), F32), ((ROWS, 2 * HID), F32)],
+        [((ROWS, WIDTH), BF)] + [((PART, 2 * HID), F32)] * 4,
         (x_own, x_other, wg, wg2, wu, wu2),
         2 * ROWS * WIDTH * 4 * HID,
         vmem=VMEM_LARGE,
     )
-    small = ((ROWS, HID), BF)
-    g, h, h2, gd, gd2, ud, ud2, rows_send = call(
-        delta_body,
-        [((ROWS, WIDTH), BF), small, small, small, small, small, small, ((ROWS, HALF), BF)],
-        (g_own, g_other, gate_pre, up_pre, wd, wd2, wg, wg2, wu, wu2),
-        2 * ROWS * WIDTH * 4 * HID,
-        vmem=VMEM_LARGE,
-    )
-    rows_recv = lax.ppermute(rows_send, "tp", PAIR_R)
+    halves, rows_recv = [], []
+    for k in range(2):
+        *made, rows_send = call(
+            delta_body,
+            [((PART, WIDTH), BF)] + [((PART, HID), BF)] * 6 + [((PART, HALF), BF)],
+            (g_own[k], g_other[k], pre[2 * k], pre[2 * k + 1], wd, wd2, wg, wg2, wu, wu2),
+            2 * PART * WIDTH * 4 * HID,
+            in_place=range(4, 10),
+            scratch=[pltpu.VMEM((2, HID, WIDTH), BF), pltpu.VMEM((4, HALF, HID), BF)]
+            + [pltpu.SemaphoreType.DMA((6,))],
+            vmem=VMEM_LARGE,
+        )
+        halves += made
+        rows_recv.append(lax.ppermute(rows_send, "tp", PAIR_R))
+    g, h, h2, gd, gd2, ud, ud2 = call(
+        join_body,
+        [((ROWS, WIDTH), BF)] + [((ROWS, HID), BF)] * 6,
+        halves,
+        0,
+    )
     (rows_keep,) = call(
         keep_body,
         [((ROWS, HALF), F32)],
@@ -498,12 +537,17 @@
 
     gate_grad = finished(x, gd, (x, gd2))
     up_grad = finished(x, ud, (x, ud2))
-    down_grad = finished(h, g, (h2, g))
+    down_own = lax.optimization_barrier(outer(h, g))
+    down_arrived = []
+    for k in range(2):
+        part = outer(h2[:, k * 128 : (k + 1) * 128], g).astype(BF)
+        down_arrived.append(lax.ppermute(part, "tp", PAIR_W))
+    down_grad = (down_own + jnp.concatenate(down_arrived).astype(F32)).astype(BF)[None]
 
     (back_send,) = call(
         back_body,
         [((SLOTS, 256), BF)],
-        (rows_keep, rows_recv, unmix_from),
+        (rows_keep, *rows_recv, unmix_from),
         2 * SLOTS * 192 * 256,
     )
     back = exchanged(back_send.reshape(sp_count, 24, 256))

time: 286 us -> 277 us (0.969)
  the two profiles are of different devices: /device:TPU:16 before, /device:TPU:17 now
where the time goes in v1:
time: 277 us; the launch traced here: 276 us
  waiting for transfers between devices  136 us (49%)
  starting transfers between devices  84.6 us (31%)
  Pallas kernels  28.3 us (10%)
  matrix products  14 us (5%)
  local copies, waits for them, and re-layouts  8.4 us (3%)
  other arithmetic  3.75 us (1%)
    all_to_all x4, starting transfers between devices, exchanged(): lax.all_to_all(array, 'sp', split_axis=0, concat_axis=0, tiled=True, **gr...  40.3 us
    all_to_all x4, waiting for transfers between devices, exchanged(): lax.all_to_all(array, 'sp', split_axis=0, concat_axis=0, tiled=True, **gr...  38.6 us
    pallas_call x18, Pallas kernels, call(): pl.pallas_call(body, out_shape=[jax.ShapeDtypeStruct(s, d) for s, d in ou...  28.3 us
    ppermute x3, waiting for transfers between devices, around(): lax.ppermute(blocks[d], 'tp', [(i, (i + d) % 4) for i in range(4)])  24.6 us
    ppermute x1, waiting for transfers between devices, on_device(): wu2 = lax.ppermute(wu, 'tp', PAIR_W)  20.9 us
    ppermute x1, waiting for transfers between devices, on_device(): wd2 = lax.ppermute(wd, 'tp', PAIR_W)  18.8 us
    dot_general x7, matrix products, outer(): return lax.dot_general(a, b, TN, preferred_element_type=F32)  14 us
    ppermute x1, starting transfers between devices, on_device(): lax.ppermute(piece, ('sp', 'tp'), [(s * 4 + t, (per_tp * t + s % per_tp)...  10.9 us
  transfers between devices with their start and end apart: 27, of which 14 were waited for; matrix products, arithmetic and copies ran while one was open for 6% of the time, Pallas kernels for 8%

profile of v1, /device:TPU:17, one launch (start us, length us, event | category | flops | bytes accessed | tf_op | source)
XLA Modules:
  0.0 276.1 jit_solution(405092702158420035)
XLA Ops:
  0.7 3.7 %shard_map.208 = (bf16[1536,256]{1,0:T(8,128)(2,1)}, s32[2,256]{1,0:T(2,128)}) custom-call(s32[2,256]{1,0:T(2,128)} %bitcast.52, bf16[256,2048]{1,0:T(8,128)(2,1)} %input_ref.1), custom_call_target="tpu_custom_call" | custom-call | flops 805306368 | bytes 1839104 | tf_op jit(solution)/shard_map/pallas_call | solution.py:62
  4.4 12.2 %all-to-all-start = ((bf16[64,24,256]{2,1,0:T(8,128)(2,1)}), bf16[64,24,256]{2,1,0:T(8,128)(2,1)S(1)}, u32[]{:S(2)}, u32[]{:S(2)}) async-start(bf16[64,24,256]{2,1,0:T(8,128)(2,1)} %bitcast.51), calls=%async_computation | async-start | bytes 1572864 | tf_op jit(solution)/shard_map/all_to_all | solution.py:408
  16.6 1.2 copy-done.36
  17.8 1.3 shard_map.211
  20.1 19.5 %all-to-all-done = bf16[64,24,256]{2,1,0:T(8,128)(2,1)S(1)} async-done(((bf16[64,24,256]{2,1,0:T(8,128)(2,1)}), bf16[64,24,256]{2,1,0:T(8,128)(2,1)S(1)}, u32[]{:S(2)}, u32[]{:S(2)}) %all-to-all-start) | async-done | bytes 786464 | tf_op jit(solution)/shard_map/all_to_all | solution.py:408
  39.6 6.1 %all-to-all-start.1 = ((bf16[64,24,256]{2,1,0:T(8,128)(2,1)}), bf16[64,24,256]{2,1,0:T(8,128)(2,1)}, u32[]{:S(2)}, u32[]{:S(2)}) async-start(bf16[64,24,256]{2,1,0:T(8,128)(2,1)} %bitcast.48), calls=%async_computation.1 | async-start | bytes 1572864 | tf_op jit(solution)/shard_map/all_to_all | solution.py:408
  48.2 1.2 shard_map.209.own_ref
  49.5 19.1 %all-to-all-done.1 = bf16[64,24,256]{2,1,0:T(8,128)(2,1)} async-done(((bf16[64,24,256]{2,1,0:T(8,128)(2,1)}), bf16[64,24,256]{2,1,0:T(8,128)(2,1)}, u32[]{:S(2)}, u32[]{:S(2)}) %all-to-all-start.1) | async-done | bytes 786464 | tf_op jit(solution)/shard_map/all_to_all | solution.py:408
  68.6 1.5 shard_map.212
  70.3 1.3 collective-permute-start.5
  71.6 20.9 %collective-permute-done.2.wu2_ref = bf16[2048,256]{1,0:T(8,128)(2,1)} collective-permute-done((bf16[2048,256]{1,0:T(8,128)(2,1)S(1)}, bf16[2048,256]{1,0:T(8,128)(2,1)}, u32[]{:S(2)}, u32[]{:S(2)}) %collective-permute-start.2) | collective-permute-done | bytes 1048608 | tf_op jit(solution)/shard_map/ppermute | solution.py:443
  92.5 3.6 %shard_map.210 = (bf16[384,2048]{1,0:T(8,128)(2,1)S(1)}, f32[192,512]{1,0:T(8,128)S(1)}, f32[192,512]{1,0:T(8,128)S(1)}, f32[192,512]{1,0:T(8,128)S(1)}, f32[192,512]{1,0:T(8,128)S(1)}) custom-call(bf16[384,1024]{1,0:T(8,128)(2,1)} %shard_map.209.own_ref, bf16[384,1024]{1,0:T(8,128)(2,1)S(1)} %collective-permute-done.other_ref, ...), custom_call_target="tpu_custom_call" | custom-call | flops 1610612736 | bytes 8912896 | tf_op jit(solution)/shard_map/pallas_call | solution.py:62
  96.1 18.8 %collective-permute-done.4.wd2_ref = bf16[256,2048]{1,0:T(8,128)(2,1)} collective-permute-done((bf16[256,2048]{1,0:T(8,128)(2,1)}, bf16[256,2048]{1,0:T(8,128)(2,1)}, u32[]{:S(2)}, u32[]{:S(2)}) %collective-permute-start.4) | collective-permute-done | bytes 1048608 | tf_op jit(solution)/shard_map/ppermute | solution.py:444
  115.0 3.0 %shard_map.213 = (bf16[192,2048]{1,0:T(8,128)(2,1)S(1)}, bf16[192,256]{1,0:T(8,128)(2,1)S(1)}, bf16[192,256]{1,0:T(8,128)(2,1)S(1)}, bf16[192,256]{1,0:T(8,128)(...) custom-call(bf16[192,1024]{1,0:T(8,128)(2,1)S(1)} %get-tuple-element, ...), custom_call_target="tpu_custom_call" | custom-call | flops 805306368 | bytes 9633792 | tf_op jit(solution)/shard_map/pallas_call | solution.py:62
  118.5 3.0 %shard_map.214 = (bf16[192,2048]{1,0:T(8,128)(2,1)S(1)}, bf16[192,256]{1,0:T(8,128)(2,1)S(1)}, bf16[192,256]{1,0:T(8,128)(2,1)S(1)}, bf16[192,256]{1,0:T(8,128)(...) custom-call(bf16[192,1024]{1,0:T(8,128)(2,1)S(1)} %get-tuple-element, ...), custom_call_target="tpu_custom_call" | custom-call | flops 805306368 | bytes 9633792 | tf_op jit(solution)/shard_map/pallas_call | solution.py:62
  121.5 1.4 collective-permute-start.11
  123.8 2.9 %shard_map.216.keep_ref = f32[384,1024]{1,0:T(8,128)S(1)} custom-call(bf16[384,256]{1,0:T(8,128)(2,1)S(1)} %get-tuple-element.86.gd_ref, bf16[384,256]{1,0:T(8,128)(2,1)S(1)} %get-tuple-element.87.gd2_ref, bf16[384,256]{1,0:T(8,128)(2,1)S(1)} %get-tuple-element.88.ud_ref, bf16[384,256]{1,0:T(8,128)(2,1)S(1)} %get-tuple-element.89.ud2_ref, ...), custom_call_target="tpu_custom_call" | custom-call | flops 805306368 | bytes 6553600 | tf_op jit(solution)/shard_map/pallas_call | solution.py:62
  127.6 8.4 %collective-permute-done.11.second_ref = bf16[192,1024]{1,0:T(8,128)(2,1)S(1)} collective-permute-done((bf16[192,1024]{1,0:T(8,128)(2,1)S(1)}, bf16[192,1024]{1,0:T(8,128)(2,1)S(1)}, u32[]{:S(2)}, u32[]{:S(2)}) %collective-permute-start.11) | collective-permute-done | bytes 393248 | tf_op jit(solution)/shard_map/ppermute | solution.py:515
  136.0 1.3 shard_map.217
  137.3 12.4 %all-to-all-start.2 = ((bf16[64,24,256]{2,1,0:T(8,128)(2,1)}), bf16[64,24,256]{2,1,0:T(8,128)(2,1)S(1)}, u32[]{:S(2)}, u32[]{:S(2)}) async-start(bf16[64,24,256]{2,1,0:T(8,128)(2,1)} %bitcast.12), calls=%async_computation.2 | async-start | bytes 1572864 | tf_op jit(solution)/shard_map/all_to_all | solution.py:408
  150.1 1.3 collective-permute-start.13
  151.4 3.4 %collective-permute-start.14 = (bf16[784,256]{1,0:T(8,128)(2,1)S(1)}, bf16[784,256]{1,0:T(8,128)(2,1)S(1)}, u32[]{:S(2)}, u32[]{:S(2)}) collective-permute-start(bf16[784,256]{1,0:T(8,128)(2,1)S(1)} %get-tuple-element.101), channel_id=1, source_target_pairs={{0,1},{1,0},{2,3},{3,2},{4,5},{5,4},{6,7},{7,6},{8,9},{9,8},{10,11... | collective-permute-start | bytes 1204232 | tf_op jit(solution)/shard_map/ppermute | solution.py:474
  154.9 5.5 %collective-permute-done.15 = bf16[784,256]{1,0:T(8,128)(2,1)S(1)} collective-permute-done((bf16[784,256]{1,0:T(8,128)(2,1)S(1)}, bf16[784,256]{1,0:T(8,128)(2,1)S(1)}, u32[]{:S(2)}, u32[]{:S(2)}) %collective-permute-start.15) | collective-permute-done | bytes 401440 | tf_op jit(solution)/shard_map/ppermute | solution.py:473
  160.4 3.4 %collective-permute-start.16 = (bf16[784,256]{1,0:T(8,128)(2,1)S(1)}, bf16[784,256]{1,0:T(8,128)(2,1)S(1)}, u32[]{:S(2)}, u32[]{:S(2)}) collective-permute-start(bf16[784,256]{1,0:T(8,128)(2,1)S(1)} %collective-permute-done.15), channel_id=1, source_target_pairs={{0,1},{1,0},{2,3},{3,2},{4,5},{5,4},{6,7},{7,6},{8,9},{9,8},{10,11... | collective-permute-start | bytes 1204232 | tf_op jit(solution)/shard_map/ppermute | solution.py:475
  163.8 5.2 %collective-permute-done.13.across_ref = bf16[784,256]{1,0:T(8,128)(2,1)S(1)} collective-permute-done((bf16[784,256]{1,0:T(8,128)(2,1)S(1)}, bf16[784,256]{1,0:T(8,128)(2,1)S(1)}, u32[]{:S(2)}, u32[]{:S(2)}) %collective-permute-start.13) | collective-permute-done | bytes 401440 | tf_op jit(solution)/shard_map/ppermute | solution.py:472
  169.0 2.3 collective-permute-done.16.opposite_ref
  172.9 1.3 convolution_convert_fusion.3
  174.2 1.3 collective-permute-start.8
  180.8 1.3 convolution_convert_fusion.2
  182.0 1.2 collective-permute-start.9
  183.2 7.7 %collective-permute-done.12.recv_ref = bf16[256,512]{1,0:T(8,128)(2,1)S(1)} collective-permute-done((bf16[256,512]{1,0:T(8,128)(2,1)S(1)}, bf16[256,512]{1,0:T(8,128)(2,1)S(1)}, u32[]{:S(2)}, u32[]{:S(2)}) %collective-permute-start.12) | collective-permute-done | bytes 262176 | tf_op jit(solution)/shard_map/ppermute | solution.py:561
  191.4 7.1 %collective-permute-start.17 = (bf16[1024,256]{1,0:T(8,128)(2,1)S(1)}, bf16[1024,256]{1,0:T(8,128)(2,1)S(1)}, u32[]{:S(2)}, u32[]{:S(2)}) collective-permute-start(bf16[1024,256]{1,0:T(8,128)(2,1)S(1)} %get-tuple-element.105), channel_id=1, source_target_pairs={{0,4},{4,0},{8,12},{12,8},{16,20},{20,16},{24,28},{28,24},{32,36},... | collective-permute-start | bytes 1572872 | tf_op jit(solution)/shard_map/ppermute | solution.py:569
  198.6 1.7 convolution_convert_fusion
  200.3 1.5 collective-permute-start.7
  201.7 1.7 convolution_convert_fusion.1
  204.4 9.7 %all-to-all-start.3 = ((bf16[32,32,256]{2,1,0:T(8,128)(2,1)}), bf16[32,32,256]{2,1,0:T(8,128)(2,1)}, u32[]{:S(2)}, u32[]{:S(2)}) async-start(bf16[32,32,256]{2,1,0:T(8,128)(2,1)} %bitcast.16), calls=%async_computation.3 | async-start | bytes 1048576 | tf_op jit(solution)/shard_map/all_to_all | solution.py:408
  214.1 1.7 fusion.7
  215.8 2.6 fusion.4
  219.3 1.5 collective-permute-start.19
  220.9 1.9 collective-permute-start.21
  222.7 3.0 %collective-permute-done.7 = bf16[2048,256]{1,0:T(8,128)(2,1)} collective-permute-done((bf16[2048,256]{1,0:T(8,128)(2,1)}, bf16[2048,256]{1,0:T(8,128)(2,1)}, u32[]{:S(2)}, u32[]{:S(2)}) %collective-permute-start.7) | collective-permute-done | bytes 1048608 | tf_op jit(solution)/shard_map/ppermute | solution.py:535
  225.8 3.0 %fusion.2 = bf16[1,2048,256]{2,1,0:T(8,128)(2,1)} fusion(bf16[384,2048]{1,0:T(8,128)(2,1)S(1)} %copy-done.39, bf16[384,256]{1,0:T(8,128)(2,1)S(1)} %copy-done.19, bf16[2048,256]{1,0:T(8,128)(2,1)} %collective-permute-done.7), kind=kOutput, calls=%fused_computation.6 | convolution fusion | flops 404226048 | bytes 3866624 | tf_op jit(solution)/shard_map/dot_general | solution.py:531
  228.7 21.6 %collective-permute-done.19.r1_ref = bf16[272,256]{1,0:T(8,128)(2,1)S(1)} collective-permute-done((bf16[272,256]{1,0:T(8,128)(2,1)S(1)}, bf16[272,256]{1,0:T(8,128)(2,1)S(1)}, u32[]{:S(2)}, u32[]{:S(2)}) %collective-permute-start.19) | collective-permute-done | bytes 139296 | tf_op jit(solution)/shard_map/ppermute | solution.py:404
  251.2 2.1 collective-permute-done.21.r3_ref
  253.6 4.2 %collective-permute-start.22 = (f32[32,256]{1,0:T(8,128)S(1)}, f32[32,256]{1,0:T(8,128)S(1)}, u32[]{:S(2)}, u32[]{:S(2)}) collective-permute-start(f32[32,256]{1,0:T(8,128)S(1)} %get-tuple-element.115), channel_id=1, source_target_pairs={{4,0},{8,4},{12,8},{16,12},{20,16},{24,20},{28,24},{32,28},{36,32}... | collective-permute-start | bytes 98312 | tf_op jit(solution)/shard_map/ppermute | solution.py:601
  259.1 10.9 %collective-permute-start.18 = (f32[32,256]{1,0:T(8,128)S(1)}, f32[32,256]{1,0:T(8,128)S(1)}, u32[]{:S(2)}, u32[]{:S(2)}) collective-permute-start(f32[32,256]{1,0:T(8,128)S(1)} %convert_reduce_fusion), channel_id=1, source_target_pairs={{0,0},{1,64},{2,128},{3,192},{4,4},{5,68},{6,132},{7,196},{8,8},{9... | collective-permute-start | bytes 98312 | tf_op jit(solution)/shard_map/ppermute | solution.py:577
  270.0 3.4 %fusion.3 = bf16[1,2048,256]{2,1,0:T(8,128)(2,1)} fusion(bf16[384,2048]{1,0:T(8,128)(2,1)} %copy-done.37, bf16[384,256]{1,0:T(8,128)(2,1)S(1)} %copy-done.17, bf16[2048,256]{1,0:T(8,128)(2,1)} %collective-permute-done.6), kind=kOutput, calls=%fused_computation.7 | convolution fusion | flops 404226048 | bytes 3866624 | tf_op jit(solution)/shard_map/dot_general | solution.py:531
  273.4 2.0 shard_map.225
  (129 shorter events, 18.5 us)
Async XLA Ops:
  0.6 15.9 %copy-start.45 = (f32[256,2]{0,1:T(2,128)S(1)}, f32[256,2]{0,1:T(2,128)}, u32[]{:S(2)}) copy-start(f32[256,2]{0,1:T(2,128)} %param.21) | copy-start | bytes 6148
  0.6 15.9 %copy-start.46 = (f32[256]{0:T(256)S(1)}, f32[256]{0:T(256)}, u32[]{:S(2)}) copy-start(f32[256]{0:T(256)} %param.20) | copy-start | bytes 3076
  4.4 35.2 %all-to-all-start = ((bf16[64,24,256]{2,1,0:T(8,128)(2,1)}), bf16[64,24,256]{2,1,0:T(8,128)(2,1)S(1)}, u32[]{:S(2)}, u32[]{:S(2)}) async-start(bf16[64,24,256]{2,1,0:T(8,128)(2,1)} %bitcast.51), calls=%async_computation | async-start | bytes 1572864 | tf_op jit(solution)/shard_map/all_to_all | solution.py:408
  17.8 27.8 %copy-start = (bf16[1,2048,256]{2,1,0:T(8,128)(2,1)S(1)}, bf16[1,2048,256]{2,1,0:T(8,128)(2,1)}, u32[]{:S(2)}) copy-start(bf16[1,2048,256]{2,1,0:T(8,128)(2,1)} %param.22) | copy-start | bytes 3145732
  17.8 28.9 %copy-start.1 = (bf16[1,2048,256]{2,1,0:T(8,128)(2,1)S(1)}, bf16[1,2048,256]{2,1,0:T(8,128)(2,1)}, u32[]{:S(2)}) copy-start(bf16[1,2048,256]{2,1,0:T(8,128)(2,1)} %param.23) | copy-start | bytes 3145732
  17.8 30.4 %copy-start.15 = (bf16[192,192]{1,0:T(8,128)(2,1)S(1)}, bf16[192,192]{1,0:T(8,128)(2,1)}, u32[]{:S(2)}) copy-start(bf16[192,192]{1,0:T(8,128)(2,1)} %constant.6.clone.perm_ref) | copy-start | bytes 221188
  20.1 29.4 %copy-start.40 = (bf16[256,512]{1,0:T(8,128)(2,1)}, bf16[256,512]{1,0:T(8,128)(2,1)S(1)}, u32[]{:S(2)}) copy-start(bf16[256,512]{1,0:T(8,128)(2,1)S(1)} %get-tuple-element.96.grad_ref) | copy-start | bytes 786436
  20.1 29.4 %copy-start.42 = (f32[256,128]{1,0:T(8,128)}, f32[256,128]{1,0:T(8,128)S(1)}, u32[]{:S(2)}) copy-start(f32[256,128]{1,0:T(8,128)S(1)} %get-tuple-element.95.code_ref) | copy-start | bytes 393220
  39.6 29.0 %all-to-all-start.1 = ((bf16[64,24,256]{2,1,0:T(8,128)(2,1)}), bf16[64,24,256]{2,1,0:T(8,128)(2,1)}, u32[]{:S(2)}, u32[]{:S(2)}) async-start(bf16[64,24,256]{2,1,0:T(8,128)(2,1)} %bitcast.48), calls=%async_computation.1 | async-start | bytes 1572864 | tf_op jit(solution)/shard_map/all_to_all | solution.py:408
  45.7 24.7 %collective-permute-start.1 = (bf16[2048,256]{1,0:T(8,128)(2,1)S(1)}, bf16[2048,256]{1,0:T(8,128)(2,1)}, u32[]{:S(2)}, u32[]{:S(2)}) collective-permute-start(bf16[2048,256]{1,0:T(8,128)(2,1)S(1)} %bitcast.33), channel_id=1, source_target_pairs={{0,1},{1,0},{2,3},{3,2},{4,5},{5,4},{6,7},{7,6},{8,9},{9,8},{10,11... | collective-permute-start | bytes 3145736 | tf_op jit(solution)/shard_map/ppermute | solution.py:442
  46.7 45.8 %collective-permute-start.2 = (bf16[2048,256]{1,0:T(8,128)(2,1)S(1)}, bf16[2048,256]{1,0:T(8,128)(2,1)}, u32[]{:S(2)}, u32[]{:S(2)}) collective-permute-start(bf16[2048,256]{1,0:T(8,128)(2,1)S(1)} %bitcast.38), channel_id=1, source_target_pairs={{0,1},{1,0},{2,3},{3,2},{4,5},{5,4},{6,7},{7,6},{8,9},{9,8},{10,11... | collective-permute-start | bytes 3145736 | tf_op jit(solution)/shard_map/ppermute | solution.py:443
  47.2 67.8 %collective-permute-start.4 = (bf16[256,2048]{1,0:T(8,128)(2,1)}, bf16[256,2048]{1,0:T(8,128)(2,1)}, u32[]{:S(2)}, u32[]{:S(2)}) collective-permute-start(bf16[256,2048]{1,0:T(8,128)(2,1)} %bitcast.43), channel_id=1, source_target_pairs={{0,1},{1,0},{2,3},{3,2},{4,5},{5,4},{6,7},{7,6},{8,9},{9,8},{10,11... | collective-permute-start | bytes 3145736 | tf_op jit(solution)/shard_map/ppermute | solution.py:444
  49.5 43.1 %collective-permute-start = (bf16[384,1024]{1,0:T(8,128)(2,1)}, bf16[384,1024]{1,0:T(8,128)(2,1)S(1)}, u32[]{:S(2)}, u32[]{:S(2)}) collective-permute-start(bf16[384,1024]{1,0:T(8,128)(2,1)} %shard_map.209.own_ref), channel_id=1, source_target_pairs={{0,3},{3,0},{1,2},{2,1},{4,7},{7,4},{5,6},{6,5},{8,11},{11,8},{9,1... | collective-permute-start | bytes 2359304 | tf_op jit(solution)/shard_map/ppermute | solution.py:491
  70.1 44.9 %collective-permute-start.3 = (bf16[192,1024]{1,0:T(8,128)(2,1)S(1)}, bf16[192,1024]{1,0:T(8,128)(2,1)S(1)}, u32[]{:S(2)}, u32[]{:S(2)}) collective-permute-start(bf16[192,1024]{1,0:T(8,128)(2,1)S(1)} %get-tuple-element.66.own_ref), channel_id=1, source_target_pairs={{0,3},{3,0},{1,2},{2,1},{4,7},{7,4},{5,6},{6,5},{8,11},{11,8},{9,1... | collective-permute-start | bytes 1179656 | tf_op jit(solution)/shard_map/ppermute | solution.py:491
  70.3 44.7 %copy-start.3 = (bf16[1,256,2048]{2,1,0:T(8,128)(2,1)S(1)}, bf16[1,256,2048]{2,1,0:T(8,128)(2,1)}, u32[]{:S(2)}) copy-start(bf16[1,256,2048]{2,1,0:T(8,128)(2,1)} %param.24) | copy-start | bytes 3145732
  70.3 48.1 %collective-permute-start.5 = (bf16[192,1024]{1,0:T(8,128)(2,1)S(1)}, bf16[192,1024]{1,0:T(8,128)(2,1)S(1)}, u32[]{:S(2)}, u32[]{:S(2)}) collective-permute-start(bf16[192,1024]{1,0:T(8,128)(2,1)S(1)} %get-tuple-element.76.own_ref), channel_id=1, source_target_pairs={{0,3},{3,0},{1,2},{2,1},{4,7},{7,4},{5,6},{6,5},{8,11},{11,8},{9,1... | collective-permute-start | bytes 1179656 | tf_op jit(solution)/shard_map/ppermute | solution.py:491
  96.1 18.9 %copy-start.37 = (bf16[384,2048]{1,0:T(8,128)(2,1)}, bf16[384,2048]{1,0:T(8,128)(2,1)S(1)}, u32[]{:S(2)}) copy-start(bf16[384,2048]{1,0:T(8,128)(2,1)S(1)} %get-tuple-element.63) | copy-start | bytes 4718596
  118.0 9.6 %collective-permute-start.10 = (bf16[192,1024]{1,0:T(8,128)(2,1)S(1)}, bf16[192,1024]{1,0:T(8,128)(2,1)S(1)}, u32[]{:S(2)}, u32[]{:S(2)}) collective-permute-start(bf16[192,1024]{1,0:T(8,128)(2,1)S(1)} %get-tuple-element.93), channel_id=1, source_target_pairs={{0,3},{3,0},{1,2},{2,1},{4,7},{7,4},{5,6},{6,5},{8,11},{11,8},{9,1... | collective-permute-start | bytes 1179656 | tf_op jit(solution)/shard_map/ppermute | solution.py:515
  121.5 14.5 %collective-permute-start.11 = (bf16[192,1024]{1,0:T(8,128)(2,1)S(1)}, bf16[192,1024]{1,0:T(8,128)(2,1)S(1)}, u32[]{:S(2)}, u32[]{:S(2)}) collective-permute-start(bf16[192,1024]{1,0:T(8,128)(2,1)S(1)} %get-tuple-element.94), channel_id=1, source_target_pairs={{0,3},{3,0},{1,2},{2,1},{4,7},{7,4},{5,6},{6,5},{8,11},{11,8},{9,1... | collective-permute-start | bytes 1179656 | tf_op jit(solution)/shard_map/ppermute | solution.py:515
  137.3 12.5 %copy-start.4 = (bf16[2048,256]{1,0:T(8,128)(2,1)S(1)}, bf16[2048,256]{1,0:T(8,128)(2,1)}, u32[]{:S(2)}) copy-start(bf16[2048,256]{1,0:T(8,128)(2,1)} %proj_ref.1) | copy-start | bytes 3145732
  137.3 12.5 %copy-start.10 = (bf16[256,256]{1,0:T(8,128)(2,1)S(1)}, bf16[256,256]{1,0:T(8,128)(2,1)}, u32[]{:S(2)}) copy-start(bf16[256,256]{1,0:T(8,128)(2,1)} %hat_ref.3) | copy-start | bytes 393220
  137.3 12.5 %copy-start.34 = (f32[256]{0:T(256)S(1)}, f32[256]{0:T(256)}, u32[]{:S(2)}) copy-start(f32[256]{0:T(256)} %param.30) | copy-start | bytes 3076
  137.3 33.9 %copy-start.35 = (f32[256]{0:T(256)S(1)}, f32[256]{0:T(256)}, u32[]{:S(2)}) copy-start(f32[256]{0:T(256)} %param.29) | copy-start | bytes 3076
  137.3 38.1 %all-to-all-start.2 = ((bf16[64,24,256]{2,1,0:T(8,128)(2,1)}), bf16[64,24,256]{2,1,0:T(8,128)(2,1)S(1)}, u32[]{:S(2)}, u32[]{:S(2)}) async-start(bf16[64,24,256]{2,1,0:T(8,128)(2,1)} %bitcast.12), calls=%async_computation.2 | async-start | bytes 1572864 | tf_op jit(solution)/shard_map/all_to_all | solution.py:408
  149.7 23.1 %copy-start.25 = (bf16[384,256]{1,0:T(8,128)(2,1)S(1)}, bf16[384,256]{1,0:T(8,128)(2,1)}, u32[]{:S(2)}) copy-start(bf16[384,256]{1,0:T(8,128)(2,1)} %copy-done.24) | copy-start | bytes 589828
  149.9 10.5 %collective-permute-start.15 = (bf16[784,256]{1,0:T(8,128)(2,1)S(1)}, bf16[784,256]{1,0:T(8,128)(2,1)S(1)}, u32[]{:S(2)}, u32[]{:S(2)}) collective-permute-start(bf16[784,256]{1,0:T(8,128)(2,1)S(1)} %get-tuple-element.102), channel_id=1, source_target_pairs={{0,3},{3,0},{1,2},{2,1},{4,7},{7,4},{5,6},{6,5},{8,11},{11,8},{9,1... | collective-permute-start | bytes 1204232 | tf_op jit(solution)/shard_map/ppermute | solution.py:473
  150.1 18.8 %collective-permute-start.13 = (bf16[784,256]{1,0:T(8,128)(2,1)S(1)}, bf16[784,256]{1,0:T(8,128)(2,1)S(1)}, u32[]{:S(2)}, u32[]{:S(2)}) collective-permute-start(bf16[784,256]{1,0:T(8,128)(2,1)S(1)} %get-tuple-element.100), channel_id=1, source_target_pairs={{0,3},{3,0},{1,2},{2,1},{4,7},{7,4},{5,6},{6,5},{8,11},{11,8},{9,1... | collective-permute-start | bytes 1204232 | tf_op jit(solution)/shard_map/ppermute | solution.py:472
  151.4 17.5 %collective-permute-start.14 = (bf16[784,256]{1,0:T(8,128)(2,1)S(1)}, bf16[784,256]{1,0:T(8,128)(2,1)S(1)}, u32[]{:S(2)}, u32[]{:S(2)}) collective-permute-start(bf16[784,256]{1,0:T(8,128)(2,1)S(1)} %get-tuple-element.101), channel_id=1, source_target_pairs={{0,1},{1,0},{2,3},{3,2},{4,5},{5,4},{6,7},{7,6},{8,9},{9,8},{10,11... | collective-permute-start | bytes 1204232 | tf_op jit(solution)/shard_map/ppermute | solution.py:474
  160.4 10.9 %collective-permute-start.16 = (bf16[784,256]{1,0:T(8,128)(2,1)S(1)}, bf16[784,256]{1,0:T(8,128)(2,1)S(1)}, u32[]{:S(2)}, u32[]{:S(2)}) collective-permute-start(bf16[784,256]{1,0:T(8,128)(2,1)S(1)} %collective-permute-done.15), channel_id=1, source_target_pairs={{0,1},{1,0},{2,3},{3,2},{4,5},{5,4},{6,7},{7,6},{8,9},{9,8},{10,11... | collective-permute-start | bytes 1204232 | tf_op jit(solution)/shard_map/ppermute | solution.py:475
  174.2 41.6 %collective-permute-start.8 = (bf16[128,2048]{1,0:T(8,128)(2,1)}, bf16[128,2048]{1,0:T(8,128)(2,1)}, u32[]{:S(2)}, u32[]{:S(2)}) collective-permute-start(bf16[128,2048]{1,0:T(8,128)(2,1)} %convolution_convert_fusion.3), channel_id=1, source_target_pairs={{0,1},{1,0},{2,3},{3,2},{4,5},{5,4},{6,7},{7,6},{8,9},{9,8},{10,11... | collective-permute-start | bytes 1572872 | tf_op jit(solution)/shard_map/ppermute | solution.py:544
  180.4 18.2 %copy-start.23 = (bf16[384,256]{1,0:T(8,128)(2,1)S(1)}, bf16[384,256]{1,0:T(8,128)(2,1)}, u32[]{:S(2)}) copy-start(bf16[384,256]{1,0:T(8,128)(2,1)} %copy-done.22) | copy-start | bytes 589828
  180.4 18.2 %copy-start.38 = (bf16[384,2048]{1,0:T(8,128)(2,1)S(1)}, bf16[384,2048]{1,0:T(8,128)(2,1)}, u32[]{:S(2)}) copy-start(bf16[384,2048]{1,0:T(8,128)(2,1)} %copy-done.37) | copy-start | bytes 4718596
  180.4 10.5 %collective-permute-start.12 = (bf16[256,512]{1,0:T(8,128)(2,1)S(1)}, bf16[256,512]{1,0:T(8,128)(2,1)S(1)}, u32[]{:S(2)}, u32[]{:S(2)}) collective-permute-start(bf16[256,512]{1,0:T(8,128)(2,1)S(1)} %get-tuple-element.98), channel_id=1, source_target_pairs={{0,1},{1,0},{2,3},{3,2},{4,5},{5,4},{6,7},{7,6},{8,9},{9,8},{10,11... | collective-permute-start | bytes 786440 | tf_op jit(solution)/shard_map/ppermute | solution.py:561
  182.0 33.7 %collective-permute-start.9 = (bf16[128,2048]{1,0:T(8,128)(2,1)}, bf16[128,2048]{1,0:T(8,128)(2,1)}, u32[]{:S(2)}, u32[]{:S(2)}) collective-permute-start(bf16[128,2048]{1,0:T(8,128)(2,1)} %convolution_convert_fusion.2), channel_id=1, source_target_pairs={{0,1},{1,0},{2,3},{3,2},{4,5},{5,4},{6,7},{7,6},{8,9},{9,8},{10,11... | collective-permute-start | bytes 1572872 | tf_op jit(solution)/shard_map/ppermute | solution.py:544
  191.4 12.0 %collective-permute-start.17 = (bf16[1024,256]{1,0:T(8,128)(2,1)S(1)}, bf16[1024,256]{1,0:T(8,128)(2,1)S(1)}, u32[]{:S(2)}, u32[]{:S(2)}) collective-permute-start(bf16[1024,256]{1,0:T(8,128)(2,1)S(1)} %get-tuple-element.105), channel_id=1, source_target_pairs={{0,4},{4,0},{8,12},{12,8},{16,20},{20,16},{24,28},{28,24},{32,36},... | collective-permute-start | bytes 1572872 | tf_op jit(solution)/shard_map/ppermute | solution.py:569
  200.3 25.5 %collective-permute-start.7 = (bf16[2048,256]{1,0:T(8,128)(2,1)}, bf16[2048,256]{1,0:T(8,128)(2,1)}, u32[]{:S(2)}, u32[]{:S(2)}) collective-permute-start(bf16[2048,256]{1,0:T(8,128)(2,1)} %convolution_convert_fusion), channel_id=1, source_target_pairs={{0,1},{1,0},{2,3},{3,2},{4,5},{5,4},{6,7},{7,6},{8,9},{9,8},{10,11... | collective-permute-start | bytes 3145736 | tf_op jit(solution)/shard_map/ppermute | solution.py:535
  203.5 66.5 %collective-permute-start.6 = (bf16[2048,256]{1,0:T(8,128)(2,1)}, bf16[2048,256]{1,0:T(8,128)(2,1)}, u32[]{:S(2)}, u32[]{:S(2)}) collective-permute-start(bf16[2048,256]{1,0:T(8,128)(2,1)} %convolution_convert_fusion.1), channel_id=1, source_target_pairs={{0,1},{1,0},{2,3},{3,2},{4,5},{5,4},{6,7},{7,6},{8,9},{9,8},{10,11... | collective-permute-start | bytes 3145736 | tf_op jit(solution)/shard_map/ppermute | solution.py:535
  204.4 53.5 %all-to-all-start.3 = ((bf16[32,32,256]{2,1,0:T(8,128)(2,1)}), bf16[32,32,256]{2,1,0:T(8,128)(2,1)}, u32[]{:S(2)}, u32[]{:S(2)}) async-start(bf16[32,32,256]{2,1,0:T(8,128)(2,1)} %bitcast.16), calls=%async_computation.3 | async-start | bytes 1048576 | tf_op jit(solution)/shard_map/all_to_all | solution.py:408
  219.3 31.1 %collective-permute-start.19 = (bf16[272,256]{1,0:T(8,128)(2,1)S(1)}, bf16[272,256]{1,0:T(8,128)(2,1)S(1)}, u32[]{:S(2)}, u32[]{:S(2)}) collective-permute-start(bf16[272,256]{1,0:T(8,128)(2,1)S(1)} %get-tuple-element.110), channel_id=1, source_target_pairs={{0,1},{1,2},{2,3},{3,0},{4,5},{5,6},{6,7},{7,4},{8,9},{9,10},{10,1... | collective-permute-start | bytes 417800 | tf_op jit(solution)/shard_map/ppermute | solution.py:404
  220.9 30.4 %collective-permute-start.20 = (bf16[272,256]{1,0:T(8,128)(2,1)S(1)}, bf16[272,256]{1,0:T(8,128)(2,1)S(1)}, u32[]{:S(2)}, u32[]{:S(2)}) collective-permute-start(bf16[272,256]{1,0:T(8,128)(2,1)S(1)} %get-tuple-element.111), channel_id=1, source_target_pairs={{0,3},{1,0},{2,1},{3,2},{4,7},{5,4},{6,5},{7,6},{8,11},{9,8},{10,9... | collective-permute-start | bytes 417800 | tf_op jit(solution)/shard_map/ppermute | solution.py:404
  220.9 32.5 %copy-start.29 = (f32[256,128]{1,0:T(8,128)S(1)}, f32[256,128]{1,0:T(8,128)}, u32[]{:S(2)}) copy-start(f32[256,128]{1,0:T(8,128)} %copy-done.28) | copy-start | bytes 393220
  220.9 32.5 %collective-permute-start.21 = (bf16[272,256]{1,0:T(8,128)(2,1)S(1)}, bf16[272,256]{1,0:T(8,128)(2,1)S(1)}, u32[]{:S(2)}, u32[]{:S(2)}) collective-permute-start(bf16[272,256]{1,0:T(8,128)(2,1)S(1)} %get-tuple-element.112), channel_id=1, source_target_pairs={{0,2},{1,3},{2,0},{3,1},{4,6},{5,7},{6,4},{7,5},{8,10},{9,11},{10,... | collective-permute-start | bytes 417800 | tf_op jit(solution)/shard_map/ppermute | solution.py:404
  228.7 41.2 %copy-start.17 = (bf16[384,256]{1,0:T(8,128)(2,1)S(1)}, bf16[384,256]{1,0:T(8,128)(2,1)}, u32[]{:S(2)}) copy-start(bf16[384,256]{1,0:T(8,128)(2,1)} %copy-done.16) | copy-start | bytes 589828
  253.6 19.8 %collective-permute-start.22 = (f32[32,256]{1,0:T(8,128)S(1)}, f32[32,256]{1,0:T(8,128)S(1)}, u32[]{:S(2)}, u32[]{:S(2)}) collective-permute-start(f32[32,256]{1,0:T(8,128)S(1)} %get-tuple-element.115), channel_id=1, source_target_pairs={{4,0},{8,4},{12,8},{16,12},{20,16},{24,20},{28,24},{32,28},{36,32}... | collective-permute-start | bytes 98312 | tf_op jit(solution)/shard_map/ppermute | solution.py:601
  259.0 14.4 %copy-start.30 = (bf16[256,256]{1,0:T(8,128)(2,1)S(1)}, bf16[256,256]{1,0:T(8,128)(2,1)}, u32[]{:S(2)}) copy-start(bf16[256,256]{1,0:T(8,128)(2,1)} %gate_ref.1) | copy-start | bytes 393220
  259.0 14.4 %copy-start.31 = (bf16[256,256]{1,0:T(8,128)(2,1)S(1)}, bf16[256,256]{1,0:T(8,128)(2,1)}, u32[]{:S(2)}) copy-start(bf16[256,256]{1,0:T(8,128)(2,1)} %value_ref.1) | copy-start | bytes 393220
  259.0 14.4 %copy-start.33 = (bf16[31,256]{1,0:T(8,128)(2,1)S(1)}, bf16[31,256]{1,0:T(8,128)(2,1)}, u32[]{:S(2)}) copy-start(bf16[31,256]{1,0:T(8,128)(2,1)} %taps_ref.1) | copy-start | bytes 47620
  259.1 16.4 %collective-permute-start.18 = (f32[32,256]{1,0:T(8,128)S(1)}, f32[32,256]{1,0:T(8,128)S(1)}, u32[]{:S(2)}, u32[]{:S(2)}) collective-permute-start(f32[32,256]{1,0:T(8,128)S(1)} %convert_reduce_fusion), channel_id=1, source_target_pairs={{0,0},{1,64},{2,128},{3,192},{4,4},{5,68},{6,132},{7,196},{8,8},{9... | collective-permute-start | bytes 98312 | tf_op jit(solution)/shard_map/ppermute | solution.py:577
  (26 other events, 88.4 us)

commit v2 on v1

--- a/solution.py
+++ b/solution.py
@@ -25,6 +25,7 @@
 VMEM_SMALL = 16 * 1024 * 1024
 VMEM_LARGE = 24 * 1024 * 1024
 VMEM_WHOLE = 60 * 1024 * 1024
+SP, TP = "sp", "tp"
 PAIR_W = [(0, 1), (1, 0), (2, 3), (3, 2)]
 PAIR_R = [(0, 3), (3, 0), (1, 2), (2, 1)]
 
@@ -41,7 +42,7 @@
 
 
 def spot():
-    j = lax.axis_index("tp")
+    j = lax.axis_index(TP)
     half = lax.shift_right_logical(j, 1)
     row_class = lax.rem(lax.shift_right_logical(j + 1, 1), 2)
     return j, half, row_class
@@ -113,7 +114,7 @@
     return jnp.concatenate([buffer[:, q * 256 : (q + 1) * 256] for q in range(4)], axis=0)
 
 
-def pack_input_body(routes_ref, input_ref, send_ref, row_ref, buffer, sem):
+def pack_x_body(routes_ref, input_ref, send_ref, row_ref, buffer, sem):
     _, half, row_class = spot()
     copy = half_copy(input_ref, buffer, sem, half)
     copy.start()
@@ -137,7 +138,7 @@
     pick_rows(code_first, code_second, row_class, stacked_quarters(buffer[...]), send_ref)
 
 
-def pack_grad_body(row_ref, weight_ref, grad_ref, send_ref, code_ref, cols_ref, buffer, sem):
+def pack_g_body(row_ref, weight_ref, grad_ref, send_ref, cols_ref, buffer, sem):
     j, half, row_class = spot()
     copy = half_copy(grad_ref, buffer, sem, half)
     copy.start()
@@ -149,9 +150,13 @@
         ],
         axis=0,
     )
-    code_ref[...] = jnp.transpose(codes)
+    codes = jnp.transpose(codes)
+    high = jnp.floor(codes * (1.0 / 256.0))
+    lane = lax.broadcasted_iota(jnp.int32, (TOK, 128), 1)
+    split = jnp.where(lax.rem(lane, 2) == 0, codes - 256.0 * high, high)
+    cols_ref[:, QUART : QUART + 128] = split.astype(BF)
     copy.wait()
-    cols_ref[...] = buffer[:, at(lax.rem(j, 2) * QUART, QUART)]
+    cols_ref[:, 0:QUART] = buffer[:, at(lax.rem(j, 2) * QUART, QUART)]
     pick_rows(
         code_first,
         code_second,
@@ -247,7 +252,7 @@
     )
 
 
-def back_body(keep_ref, first_ref, second_ref, perm_ref, send_ref):
+def back_pack_body(keep_ref, first_ref, second_ref, perm_ref, send_ref):
     for group in range(8):
         rows = slice(group * 48, (group + 1) * 48)
         recv_ref = second_ref if group >= 4 else first_ref
@@ -257,13 +262,14 @@
         send_ref[group * 192 : (group + 1) * 192, :] = dot(perm_ref[...], stacked).astype(BF)
 
 
-def combine_body(back_ref, code_ref, grad_ref, keep_ref, send_ref):
+def combine_body(back_ref, cols_ref, keep_ref, send_ref):
     j, _, row_class = spot()
     who, part, rank = slot_parts(lax.broadcasted_iota(jnp.int32, (1, SLOTS), 1))
     target = (who * CAP + rank + row_class * SUB).astype(F32)
-    hit = jnp.where(
-        target == code_ref[:, 0:1], 1.0, jnp.where(target == code_ref[:, 64:65], 1.0, 0.0)
-    )
+    codes = cols_ref[:, QUART : QUART + 128].astype(F32)
+    code_first = codes[:, 0:1] + 256.0 * codes[:, 1:2]
+    code_second = codes[:, 64:65] + 256.0 * codes[:, 65:66]
+    hit = jnp.where(target == code_first, 1.0, jnp.where(target == code_second, 1.0, 0.0))
     kept = lax.rem(j, 2) * 2
     back = back_ref[...]
     for a in range(2):
@@ -272,7 +278,7 @@
     for a in range(2):
         cols = slice(a * 256, (a + 1) * 256)
         mine = dot(jnp.where(part == kept + a, hit, 0.0).astype(BF), back)
-        keep_ref[:, cols] = grad_ref[:, cols].astype(F32) + mine
+        keep_ref[:, cols] = cols_ref[:, cols].astype(F32) + mine
 
 
 def aux_body(proj_ref, hat_ref, gain_ref, *out_refs):
@@ -319,7 +325,7 @@
 def outer_body(keep_ref, recv_ref, act_ref, own_ref, other_ref, turned_ref):
     mix = mixed(keep_ref, recv_ref)
     turned_ref[...] = jnp.transpose(mix.astype(F32))
-    core = lax.rem(lax.axis_index("sp"), 2)
+    core = lax.rem(lax.axis_index(SP), 2)
 
     def rows_of(parity):
         return jnp.concatenate(
@@ -401,11 +407,11 @@
 
 
 def around(blocks):
-    return [lax.ppermute(blocks[d], "tp", [(i, (i + d) % 4) for i in range(4)]) for d in (1, 3, 2)]
+    return [lax.ppermute(blocks[d], TP, [(i, (i + d) % 4) for i in range(4)]) for d in (1, 3, 2)]
 
 
 def exchanged(array, **groups):
-    return lax.all_to_all(array, "sp", split_axis=0, concat_axis=0, tiled=True, **groups)
+    return lax.all_to_all(array, SP, split_axis=0, concat_axis=0, tiled=True, **groups)
 
 
 def unmix_matrix():
@@ -434,19 +440,19 @@
     norm_gain,
     out_proj,
 ):
-    sp_count = lax.axis_size("sp")
+    sp_count = lax.axis_size(SP)
     unmix = unmix_matrix()
     unmix_to = jnp.asarray(unmix, BF)
     unmix_from = jnp.asarray(unmix.T, BF)
     wg, wu, wd = gate_weight[0], up_weight[0], down_weight[0]
-    wg2 = lax.ppermute(wg, "tp", PAIR_W)
-    wu2 = lax.ppermute(wu, "tp", PAIR_W)
-    wd2 = lax.ppermute(wd, "tp", PAIR_W)
+    wg2 = lax.ppermute(wg, TP, PAIR_W)
+    wu2 = lax.ppermute(wu, TP, PAIR_W)
+    wd2 = lax.ppermute(wd, TP, PAIR_W)
 
     route_weight = group_weight[None, :] * inner_weight.T
     buffer = [pltpu.VMEM((TOK, HALF), BF), pltpu.SemaphoreType.DMA]
     x_send, code_rows = call(
-        pack_input_body,
+        pack_x_body,
         [((SLOTS, 256), BF), ((2, TOK), jnp.int32)],
         (routes.T, moe_input),
         2 * SLOTS * 1024 * 256,
@@ -454,9 +460,9 @@
         in_place=(1,),
         scratch=buffer,
     )
-    g_send, codes, own_cols = call(
-        pack_grad_body,
-        [((SLOTS, 256), BF), ((TOK, 128), F32), ((TOK, QUART), BF)],
+    g_send, own_cols = call(
+        pack_g_body,
+        [((SLOTS, 256), BF), ((TOK, QUART + 128), BF)],
         (code_rows, route_weight, out_cotangent),
         2 * SLOTS * 1024 * 256,
         in_place=(2,),
@@ -469,10 +475,10 @@
         (out_proj, norm_hat, norm_gain[None, :]),
         0,
     )
-    across = lax.ppermute(blocks[1], "tp", PAIR_R)
-    relayed = lax.ppermute(blocks[3], "tp", PAIR_R)
-    beside = lax.ppermute(blocks[2], "tp", PAIR_W)
-    opposite = lax.ppermute(relayed, "tp", PAIR_W)
+    across = lax.ppermute(blocks[1], TP, PAIR_R)
+    relayed = lax.ppermute(blocks[3], TP, PAIR_R)
+    beside = lax.ppermute(blocks[2], TP, PAIR_W)
+    opposite = lax.ppermute(relayed, TP, PAIR_W)
     proj_rows, act, slope, hat, rstd = call(
         channel_body,
         [((512, 4 * CH), BF), ((TOK, 4 * CH), BF), ((TOK, 4 * CH), F32), ((TOK, 4 * CH), BF), ((TOK, 128), F32)],
@@ -488,7 +494,7 @@
             (recv.reshape(SLOTS, 256), unmix_to),
             2 * SLOTS * 192 * 256,
         )
-        return own, [lax.ppermute(v, "tp", PAIR_R) for v in own]
+        return own, [lax.ppermute(v, TP, PAIR_R) for v in own]
 
     (x_own,), (x_other,) = dispatched(x_send, 1)
     g_own, g_other = dispatched(g_send, 2)
@@ -512,7 +518,7 @@
             vmem=VMEM_LARGE,
         )
         halves += made
-        rows_recv.append(lax.ppermute(rows_send, "tp", PAIR_R))
+        rows_recv.append(lax.ppermute(rows_send, TP, PAIR_R))
     g, h, h2, gd, gd2, ud, ud2 = call(
         join_body,
         [((ROWS, WIDTH), BF)] + [((ROWS, HID), BF)] * 6,
@@ -532,7 +538,7 @@
 
     def finished(a, b, b_other):
         other = outer(*b_other).astype(BF)
-        arrived = lax.ppermute(other, "tp", PAIR_W)
+        arrived = lax.ppermute(other, TP, PAIR_W)
         return (outer(a, b) + arrived.astype(F32)).astype(BF)[None]
 
     gate_grad = finished(x, gd, (x, gd2))
@@ -541,11 +547,11 @@
     down_arrived = []
     for k in range(2):
         part = outer(h2[:, k * 128 : (k + 1) * 128], g).astype(BF)
-        down_arrived.append(lax.ppermute(part, "tp", PAIR_W))
+        down_arrived.append(lax.ppermute(part, TP, PAIR_W))
     down_grad = (down_own + jnp.concatenate(down_arrived).astype(F32)).astype(BF)[None]
 
     (back_send,) = call(
-        back_body,
+        back_pack_body,
         [((SLOTS, 256), BF)],
         (rows_keep, *rows_recv, unmix_from),
         2 * SLOTS * 192 * 256,
@@ -555,10 +561,10 @@
     mix_keep, mix_send = call(
         combine_body,
         [((TOK, QUART), F32), ((TOK, QUART), BF)],
-        (back.reshape(SLOTS, 256), codes, own_cols),
+        (back.reshape(SLOTS, 256), own_cols),
         2 * SLOTS * 1024 * 256,
     )
-    mix_recv = lax.ppermute(mix_send, "tp", PAIR_W)
+    mix_recv = lax.ppermute(mix_send, TP, PAIR_W)
     outer_own, outer_other = call(
         outer_body,
         [((1024, CH), F32), ((1024, CH), BF)],
@@ -566,7 +572,7 @@
         2 * TOK * 512 * 1024,
         scratch=[pltpu.VMEM((512, TOK), F32)],
     )
-    outer_recv = lax.ppermute(outer_other, "sp", [(i, i ^ 1) for i in range(sp_count)])
+    outer_recv = lax.ppermute(outer_other, SP, [(i, i ^ 1) for i in range(sp_count)])
     (outer_sum,) = call(sum_body, [((1024, CH), BF)], (outer_own, outer_recv), 0)
     pieces = exchanged(
         outer_sum.reshape(sp_count // 2, 32, CH),
@@ -576,7 +582,7 @@
     per_tp = sp_count // 4
     proj_grad = lax.ppermute(
         piece,
-        ("sp", "tp"),
+        (SP, TP),
         [
             (s * 4 + t, (per_tp * t + s % per_tp) * 4 + s // per_tp)
             for s in range(sp_count)
@@ -598,7 +604,7 @@
         (*silu_parts, slope, norm_hat, rstd),
         0,
     )
-    incoming = lax.ppermute(head, "sp", [(i, i - 1) for i in range(1, sp_count)])
+    incoming = lax.ppermute(head, SP, [(i, i - 1) for i in range(1, sp_count)])
     value_grad, gate_in_grad = call(
         taps_body,
         [((TOK, CH), BF), ((TOK, CH), BF)],
@@ -614,29 +620,29 @@
         on_device,
         mesh=mesh,
         in_specs=(
-            P("sp", None),
-            P("sp", None),
-            P("sp", None),
-            P("sp"),
-            P("sp", None),
-            P("sp", None, "tp"),
-            P("sp", None, "tp"),
-            P("sp", "tp", None),
-            P("sp", "tp"),
-            P("sp", "tp"),
-            P(None, "tp"),
-            P("sp", "tp"),
-            P("sp"),
-            P("tp"),
-            P(None, "tp"),
+            P(SP, None),
+            P(SP, None),
+            P(SP, None),
+            P(SP),
+            P(SP, None),
+            P(SP, None, TP),
+            P(SP, None, TP),
+            P(SP, TP, None),
+            P(SP, TP),
+            P(SP, TP),
+            P(None, TP),
+            P(SP, TP),
+            P(SP),
+            P(TP),
+            P(None, TP),
         ),
         out_specs=(
-            P("sp", None, "tp"),
-            P("sp", None, "tp"),
-            P("sp", "tp", None),
-            P("sp", "tp"),
-            P("sp", "tp"),
-            P("sp", "tp"),
+            P(SP, None, TP),
+            P(SP, None, TP),
+            P(SP, TP, None),
+            P(SP, TP),
+            P(SP, TP),
+            P(SP, TP),
         ),
         check_vma=False,
     )

time: 277 us -> 277 us (level)
    unnamed x95 -> x91, local copies, waits for them, and re-layouts: 8.4 us -> 7.5 us
where the time goes in v2:
time: 277 us; the launch traced here: 276 us
  waiting for transfers between devices  137 us (49%)
  starting transfers between devices  84.6 us (31%)
  Pallas kernels  28.4 us (10%)
  matrix products  14 us (5%)
  local copies, waits for them, and re-layouts  7.5 us (3%)
  other arithmetic  3.75 us (1%)
    all_to_all x4, starting transfers between devices, exchanged(): lax.all_to_all(array, SP, split_axis=0, concat_axis=0, tiled=True, **groups)  40.3 us
    all_to_all x4, waiting for transfers between devices, exchanged(): lax.all_to_all(array, SP, split_axis=0, concat_axis=0, tiled=True, **groups)  38.6 us
    pallas_call x18, Pallas kernels, call(): pl.pallas_call(body, out_shape=[jax.ShapeDtypeStruct(s, d) for s, d in ou...  28.4 us
    ppermute x3, waiting for transfers between devices, around(): lax.ppermute(blocks[d], TP, [(i, (i + d) % 4) for i in range(4)])  24.6 us
    ppermute x1, waiting for transfers between devices, on_device(): wu2 = lax.ppermute(wu, TP, PAIR_W)  20.9 us
    ppermute x1, waiting for transfers between devices, on_device(): wd2 = lax.ppermute(wd, TP, PAIR_W)  18.8 us
    dot_general x7, matrix products, outer(): return lax.dot_general(a, b, TN, preferred_element_type=F32)  14 us
    ppermute x1, starting transfers between devices, on_device(): lax.ppermute(piece, (SP, TP), [(s * 4 + t, (per_tp * t + s % per_tp) * 4...  10.9 us
  transfers between devices with their start and end apart: 27, of which 14 were waited for; matrix products, arithmetic and copies ran while one was open for 6% of the time, Pallas kernels for 8%

profile of v2, /device:TPU:17, one launch (start us, length us, event | category | flops | bytes accessed | tf_op | source)
XLA Modules:
  0.0 276.0 jit_solution(7199062346146789930)
XLA Ops:
  0.7 3.7 %shard_map.208 = (bf16[1536,256]{1,0:T(8,128)(2,1)}, s32[2,256]{1,0:T(2,128)}) custom-call(s32[2,256]{1,0:T(2,128)} %bitcast.52, bf16[256,2048]{1,0:T(8,128)(2,1)} %input_ref.1), custom_call_target="tpu_custom_call" | custom-call | flops 805306368 | bytes 1839104 | tf_op jit(solution)/shard_map/pallas_call | solution.py:63
  4.4 12.2 %all-to-all-start = ((bf16[64,24,256]{2,1,0:T(8,128)(2,1)}), bf16[64,24,256]{2,1,0:T(8,128)(2,1)S(1)}, u32[]{:S(2)}, u32[]{:S(2)}) async-start(bf16[64,24,256]{2,1,0:T(8,128)(2,1)} %bitcast.51), calls=%async_computation | async-start | bytes 1572864 | tf_op jit(solution)/shard_map/all_to_all | solution.py:414
  16.6 1.2 copy-done.36
  17.8 1.3 shard_map.211
  20.1 19.5 %all-to-all-done = bf16[64,24,256]{2,1,0:T(8,128)(2,1)S(1)} async-done(((bf16[64,24,256]{2,1,0:T(8,128)(2,1)}), bf16[64,24,256]{2,1,0:T(8,128)(2,1)S(1)}, u32[]{:S(2)}, u32[]{:S(2)}) %all-to-all-start) | async-done | bytes 786464 | tf_op jit(solution)/shard_map/all_to_all | solution.py:414
  39.6 6.1 %all-to-all-start.1 = ((bf16[64,24,256]{2,1,0:T(8,128)(2,1)}), bf16[64,24,256]{2,1,0:T(8,128)(2,1)}, u32[]{:S(2)}, u32[]{:S(2)}) async-start(bf16[64,24,256]{2,1,0:T(8,128)(2,1)} %bitcast.48), calls=%async_computation.1 | async-start | bytes 1572864 | tf_op jit(solution)/shard_map/all_to_all | solution.py:414
  48.2 1.2 shard_map.209.own_ref
  49.5 19.1 %all-to-all-done.1 = bf16[64,24,256]{2,1,0:T(8,128)(2,1)} async-done(((bf16[64,24,256]{2,1,0:T(8,128)(2,1)}), bf16[64,24,256]{2,1,0:T(8,128)(2,1)}, u32[]{:S(2)}, u32[]{:S(2)}) %all-to-all-start.1) | async-done | bytes 786464 | tf_op jit(solution)/shard_map/all_to_all | solution.py:414
  68.6 1.5 shard_map.212
  70.3 1.3 collective-permute-start.5
  71.6 20.9 %collective-permute-done.2.wu2_ref = bf16[2048,256]{1,0:T(8,128)(2,1)} collective-permute-done((bf16[2048,256]{1,0:T(8,128)(2,1)S(1)}, bf16[2048,256]{1,0:T(8,128)(2,1)}, u32[]{:S(2)}, u32[]{:S(2)}) %collective-permute-start.2) | collective-permute-done | bytes 1048608 | tf_op jit(solution)/shard_map/ppermute | solution.py:449
  92.5 3.6 %shard_map.210 = (bf16[384,2048]{1,0:T(8,128)(2,1)S(1)}, f32[192,512]{1,0:T(8,128)S(1)}, f32[192,512]{1,0:T(8,128)S(1)}, f32[192,512]{1,0:T(8,128)S(1)}, f32[192,512]{1,0:T(8,128)S(1)}) custom-call(bf16[384,1024]{1,0:T(8,128)(2,1)} %shard_map.209.own_ref, bf16[384,1024]{1,0:T(8,128)(2,1)S(1)} %collective-permute-done.other_ref, ...), custom_call_target="tpu_custom_call" | custom-call | flops 1610612736 | bytes 8912896 | tf_op jit(solution)/shard_map/pallas_call | solution.py:63
  96.1 18.8 %collective-permute-done.4.wd2_ref = bf16[256,2048]{1,0:T(8,128)(2,1)} collective-permute-done((bf16[256,2048]{1,0:T(8,128)(2,1)}, bf16[256,2048]{1,0:T(8,128)(2,1)}, u32[]{:S(2)}, u32[]{:S(2)}) %collective-permute-start.4) | collective-permute-done | bytes 1048608 | tf_op jit(solution)/shard_map/ppermute | solution.py:450
  115.0 3.0 %shard_map.213 = (bf16[192,2048]{1,0:T(8,128)(2,1)S(1)}, bf16[192,256]{1,0:T(8,128)(2,1)S(1)}, bf16[192,256]{1,0:T(8,128)(2,1)S(1)}, bf16[192,256]{1,0:T(8,128)(...) custom-call(bf16[192,1024]{1,0:T(8,128)(2,1)S(1)} %get-tuple-element, ...), custom_call_target="tpu_custom_call" | custom-call | flops 805306368 | bytes 9633792 | tf_op jit(solution)/shard_map/pallas_call | solution.py:63
  118.5 3.0 %shard_map.214 = (bf16[192,2048]{1,0:T(8,128)(2,1)S(1)}, bf16[192,256]{1,0:T(8,128)(2,1)S(1)}, bf16[192,256]{1,0:T(8,128)(2,1)S(1)}, bf16[192,256]{1,0:T(8,128)(...) custom-call(bf16[192,1024]{1,0:T(8,128)(2,1)S(1)} %get-tuple-element, ...), custom_call_target="tpu_custom_call" | custom-call | flops 805306368 | bytes 9633792 | tf_op jit(solution)/shard_map/pallas_call | solution.py:63
  121.5 1.4 collective-permute-start.11
  123.8 2.9 %shard_map.216.keep_ref = f32[384,1024]{1,0:T(8,128)S(1)} custom-call(bf16[384,256]{1,0:T(8,128)(2,1)S(1)} %get-tuple-element.85.gd_ref, bf16[384,256]{1,0:T(8,128)(2,1)S(1)} %get-tuple-element.86.gd2_ref, bf16[384,256]{1,0:T(8,128)(2,1)S(1)} %get-tuple-element.87.ud_ref, bf16[384,256]{1,0:T(8,128)(2,1)S(1)} %get-tuple-element.88.ud2_ref, ...), custom_call_target="tpu_custom_call" | custom-call | flops 805306368 | bytes 6553600 | tf_op jit(solution)/shard_map/pallas_call | solution.py:63
  127.6 8.4 %collective-permute-done.11.second_ref = bf16[192,1024]{1,0:T(8,128)(2,1)S(1)} collective-permute-done((bf16[192,1024]{1,0:T(8,128)(2,1)S(1)}, bf16[192,1024]{1,0:T(8,128)(2,1)S(1)}, u32[]{:S(2)}, u32[]{:S(2)}) %collective-permute-start.11) | collective-permute-done | bytes 393248 | tf_op jit(solution)/shard_map/ppermute | solution.py:521
  136.0 1.3 shard_map.217
  137.3 12.4 %all-to-all-start.2 = ((bf16[64,24,256]{2,1,0:T(8,128)(2,1)}), bf16[64,24,256]{2,1,0:T(8,128)(2,1)S(1)}, u32[]{:S(2)}, u32[]{:S(2)}) async-start(bf16[64,24,256]{2,1,0:T(8,128)(2,1)} %bitcast.12), calls=%async_computation.2 | async-start | bytes 1572864 | tf_op jit(solution)/shard_map/all_to_all | solution.py:414
  150.1 1.3 collective-permute-start.13
  151.4 3.4 %collective-permute-start.14 = (bf16[784,256]{1,0:T(8,128)(2,1)S(1)}, bf16[784,256]{1,0:T(8,128)(2,1)S(1)}, u32[]{:S(2)}, u32[]{:S(2)}) collective-permute-start(bf16[784,256]{1,0:T(8,128)(2,1)S(1)} %get-tuple-element.99), channel_id=1, source_target_pairs={{0,1},{1,0},{2,3},{3,2},{4,5},{5,4},{6,7},{7,6},{8,9},{9,8},{10,11... | collective-permute-start | bytes 1204232 | tf_op jit(solution)/shard_map/ppermute | solution.py:480
  154.9 5.5 %collective-permute-done.15 = bf16[784,256]{1,0:T(8,128)(2,1)S(1)} collective-permute-done((bf16[784,256]{1,0:T(8,128)(2,1)S(1)}, bf16[784,256]{1,0:T(8,128)(2,1)S(1)}, u32[]{:S(2)}, u32[]{:S(2)}) %collective-permute-start.15) | collective-permute-done | bytes 401440 | tf_op jit(solution)/shard_map/ppermute | solution.py:479
  160.4 3.4 %collective-permute-start.16 = (bf16[784,256]{1,0:T(8,128)(2,1)S(1)}, bf16[784,256]{1,0:T(8,128)(2,1)S(1)}, u32[]{:S(2)}, u32[]{:S(2)}) collective-permute-start(bf16[784,256]{1,0:T(8,128)(2,1)S(1)} %collective-permute-done.15), channel_id=1, source_target_pairs={{0,1},{1,0},{2,3},{3,2},{4,5},{5,4},{6,7},{7,6},{8,9},{9,8},{10,11... | collective-permute-start | bytes 1204232 | tf_op jit(solution)/shard_map/ppermute | solution.py:481
  163.8 5.2 %collective-permute-done.13.across_ref = bf16[784,256]{1,0:T(8,128)(2,1)S(1)} collective-permute-done((bf16[784,256]{1,0:T(8,128)(2,1)S(1)}, bf16[784,256]{1,0:T(8,128)(2,1)S(1)}, u32[]{:S(2)}, u32[]{:S(2)}) %collective-permute-start.13) | collective-permute-done | bytes 401440 | tf_op jit(solution)/shard_map/ppermute | solution.py:478
  169.0 2.3 collective-permute-done.16.opposite_ref
  172.9 1.3 convolution_convert_fusion.3
  174.2 1.3 collective-permute-start.8
  180.0 1.3 convolution_convert_fusion.2
  181.3 1.2 collective-permute-start.9
  182.4 8.4 %collective-permute-done.12.recv_ref = bf16[256,512]{1,0:T(8,128)(2,1)S(1)} collective-permute-done((bf16[256,512]{1,0:T(8,128)(2,1)S(1)}, bf16[256,512]{1,0:T(8,128)(2,1)S(1)}, u32[]{:S(2)}, u32[]{:S(2)}) %collective-permute-start.12) | collective-permute-done | bytes 262176 | tf_op jit(solution)/shard_map/ppermute | solution.py:567
  191.4 7.1 %collective-permute-start.17 = (bf16[1024,256]{1,0:T(8,128)(2,1)S(1)}, bf16[1024,256]{1,0:T(8,128)(2,1)S(1)}, u32[]{:S(2)}, u32[]{:S(2)}) collective-permute-start(bf16[1024,256]{1,0:T(8,128)(2,1)S(1)} %get-tuple-element.103), channel_id=1, source_target_pairs={{0,4},{4,0},{8,12},{12,8},{16,20},{20,16},{24,28},{28,24},{32,36},... | collective-permute-start | bytes 1572872 | tf_op jit(solution)/shard_map/ppermute | solution.py:575
  198.5 1.7 convolution_convert_fusion
  200.3 1.5 collective-permute-start.7
  201.7 1.7 convolution_convert_fusion.1
  204.4 9.7 %all-to-all-start.3 = ((bf16[32,32,256]{2,1,0:T(8,128)(2,1)}), bf16[32,32,256]{2,1,0:T(8,128)(2,1)}, u32[]{:S(2)}, u32[]{:S(2)}) async-start(bf16[32,32,256]{2,1,0:T(8,128)(2,1)} %bitcast.16), calls=%async_computation.3 | async-start | bytes 1048576 | tf_op jit(solution)/shard_map/all_to_all | solution.py:414
  214.1 1.7 fusion.7
  215.8 2.6 fusion.4
  219.3 1.5 collective-permute-start.19
  220.8 1.9 collective-permute-start.21
  222.7 3.0 %collective-permute-done.7 = bf16[2048,256]{1,0:T(8,128)(2,1)} collective-permute-done((bf16[2048,256]{1,0:T(8,128)(2,1)}, bf16[2048,256]{1,0:T(8,128)(2,1)}, u32[]{:S(2)}, u32[]{:S(2)}) %collective-permute-start.7) | collective-permute-done | bytes 1048608 | tf_op jit(solution)/shard_map/ppermute | solution.py:541
  225.8 3.0 %fusion.2 = bf16[1,2048,256]{2,1,0:T(8,128)(2,1)} fusion(bf16[384,2048]{1,0:T(8,128)(2,1)S(1)} %copy-done.39, bf16[384,256]{1,0:T(8,128)(2,1)S(1)} %copy-done.19, bf16[2048,256]{1,0:T(8,128)(2,1)} %collective-permute-done.7), kind=kOutput, calls=%fused_computation.6 | convolution fusion | flops 404226048 | bytes 3866624 | tf_op jit(solution)/shard_map/dot_general | solution.py:537
  228.7 21.6 %collective-permute-done.19.r1_ref = bf16[272,256]{1,0:T(8,128)(2,1)S(1)} collective-permute-done((bf16[272,256]{1,0:T(8,128)(2,1)S(1)}, bf16[272,256]{1,0:T(8,128)(2,1)S(1)}, u32[]{:S(2)}, u32[]{:S(2)}) %collective-permute-start.19) | collective-permute-done | bytes 139296 | tf_op jit(solution)/shard_map/ppermute | solution.py:410
  251.2 2.1 collective-permute-done.21.r3_ref
  253.6 4.2 %collective-permute-start.22 = (f32[32,256]{1,0:T(8,128)S(1)}, f32[32,256]{1,0:T(8,128)S(1)}, u32[]{:S(2)}, u32[]{:S(2)}) collective-permute-start(f32[32,256]{1,0:T(8,128)S(1)} %get-tuple-element.113), channel_id=1, source_target_pairs={{4,0},{8,4},{12,8},{16,12},{20,16},{24,20},{28,24},{32,28},{36,32}... | collective-permute-start | bytes 98312 | tf_op jit(solution)/shard_map/ppermute | solution.py:607
  259.0 10.9 %collective-permute-start.18 = (f32[32,256]{1,0:T(8,128)S(1)}, f32[32,256]{1,0:T(8,128)S(1)}, u32[]{:S(2)}, u32[]{:S(2)}) collective-permute-start(f32[32,256]{1,0:T(8,128)S(1)} %convert_reduce_fusion), channel_id=1, source_target_pairs={{0,0},{1,64},{2,128},{3,192},{4,4},{5,68},{6,132},{7,196},{8,8},{9... | collective-permute-start | bytes 98312 | tf_op jit(solution)/shard_map/ppermute | solution.py:583
  269.9 3.4 %fusion.3 = bf16[1,2048,256]{2,1,0:T(8,128)(2,1)} fusion(bf16[384,2048]{1,0:T(8,128)(2,1)} %copy-done.37, bf16[384,256]{1,0:T(8,128)(2,1)S(1)} %copy-done.17, bf16[2048,256]{1,0:T(8,128)(2,1)} %collective-permute-done.6), kind=kOutput, calls=%fused_computation.7 | convolution fusion | flops 404226048 | bytes 3866624 | tf_op jit(solution)/shard_map/dot_general | solution.py:537
  273.4 2.0 shard_map.225
  (125 shorter events, 17.7 us)
Async XLA Ops:
  0.6 15.9 %copy-start.43 = (f32[256,2]{0,1:T(2,128)S(1)}, f32[256,2]{0,1:T(2,128)}, u32[]{:S(2)}) copy-start(f32[256,2]{0,1:T(2,128)} %param.21) | copy-start | bytes 6148
  0.6 15.9 %copy-start.44 = (f32[256]{0:T(256)S(1)}, f32[256]{0:T(256)}, u32[]{:S(2)}) copy-start(f32[256]{0:T(256)} %param.20) | copy-start | bytes 3076
  4.4 12.2 %copy-start.42 = (s32[2,256]{1,0:T(2,128)S(1)}, s32[2,256]{1,0:T(2,128)}, u32[]{:S(2)}) copy-start(s32[2,256]{1,0:T(2,128)} %get-tuple-element.63.row_ref) | copy-start | bytes 6148
  4.4 35.2 %all-to-all-start = ((bf16[64,24,256]{2,1,0:T(8,128)(2,1)}), bf16[64,24,256]{2,1,0:T(8,128)(2,1)S(1)}, u32[]{:S(2)}, u32[]{:S(2)}) async-start(bf16[64,24,256]{2,1,0:T(8,128)(2,1)} %bitcast.51), calls=%async_computation | async-start | bytes 1572864 | tf_op jit(solution)/shard_map/all_to_all | solution.py:414
  17.8 27.8 %copy-start = (bf16[1,2048,256]{2,1,0:T(8,128)(2,1)S(1)}, bf16[1,2048,256]{2,1,0:T(8,128)(2,1)}, u32[]{:S(2)}) copy-start(bf16[1,2048,256]{2,1,0:T(8,128)(2,1)} %param.22) | copy-start | bytes 3145732
  17.8 28.9 %copy-start.1 = (bf16[1,2048,256]{2,1,0:T(8,128)(2,1)S(1)}, bf16[1,2048,256]{2,1,0:T(8,128)(2,1)}, u32[]{:S(2)}) copy-start(bf16[1,2048,256]{2,1,0:T(8,128)(2,1)} %param.23) | copy-start | bytes 3145732
  17.8 30.4 %copy-start.15 = (bf16[192,192]{1,0:T(8,128)(2,1)S(1)}, bf16[192,192]{1,0:T(8,128)(2,1)}, u32[]{:S(2)}) copy-start(bf16[192,192]{1,0:T(8,128)(2,1)} %constant.6.clone.perm_ref) | copy-start | bytes 221188
  20.1 29.4 %copy-start.40 = (bf16[256,640]{1,0:T(8,128)(2,1)}, bf16[256,640]{1,0:T(8,128)(2,1)S(1)}, u32[]{:S(2)}) copy-start(bf16[256,640]{1,0:T(8,128)(2,1)S(1)} %get-tuple-element.94.cols_ref) | copy-start | bytes 983044
  39.6 29.0 %all-to-all-start.1 = ((bf16[64,24,256]{2,1,0:T(8,128)(2,1)}), bf16[64,24,256]{2,1,0:T(8,128)(2,1)}, u32[]{:S(2)}, u32[]{:S(2)}) async-start(bf16[64,24,256]{2,1,0:T(8,128)(2,1)} %bitcast.48), calls=%async_computation.1 | async-start | bytes 1572864 | tf_op jit(solution)/shard_map/all_to_all | solution.py:414
  45.7 24.7 %collective-permute-start.1 = (bf16[2048,256]{1,0:T(8,128)(2,1)S(1)}, bf16[2048,256]{1,0:T(8,128)(2,1)}, u32[]{:S(2)}, u32[]{:S(2)}) collective-permute-start(bf16[2048,256]{1,0:T(8,128)(2,1)S(1)} %bitcast.33), channel_id=1, source_target_pairs={{0,1},{1,0},{2,3},{3,2},{4,5},{5,4},{6,7},{7,6},{8,9},{9,8},{10,11... | collective-permute-start | bytes 3145736 | tf_op jit(solution)/shard_map/ppermute | solution.py:448
  46.7 45.8 %collective-permute-start.2 = (bf16[2048,256]{1,0:T(8,128)(2,1)S(1)}, bf16[2048,256]{1,0:T(8,128)(2,1)}, u32[]{:S(2)}, u32[]{:S(2)}) collective-permute-start(bf16[2048,256]{1,0:T(8,128)(2,1)S(1)} %bitcast.38), channel_id=1, source_target_pairs={{0,1},{1,0},{2,3},{3,2},{4,5},{5,4},{6,7},{7,6},{8,9},{9,8},{10,11... | collective-permute-start | bytes 3145736 | tf_op jit(solution)/shard_map/ppermute | solution.py:449
  47.2 67.8 %collective-permute-start.4 = (bf16[256,2048]{1,0:T(8,128)(2,1)}, bf16[256,2048]{1,0:T(8,128)(2,1)}, u32[]{:S(2)}, u32[]{:S(2)}) collective-permute-start(bf16[256,2048]{1,0:T(8,128)(2,1)} %bitcast.43), channel_id=1, source_target_pairs={{0,1},{1,0},{2,3},{3,2},{4,5},{5,4},{6,7},{7,6},{8,9},{9,8},{10,11... | collective-permute-start | bytes 3145736 | tf_op jit(solution)/shard_map/ppermute | solution.py:450
  49.5 43.1 %collective-permute-start = (bf16[384,1024]{1,0:T(8,128)(2,1)}, bf16[384,1024]{1,0:T(8,128)(2,1)S(1)}, u32[]{:S(2)}, u32[]{:S(2)}) collective-permute-start(bf16[384,1024]{1,0:T(8,128)(2,1)} %shard_map.209.own_ref), channel_id=1, source_target_pairs={{0,3},{3,0},{1,2},{2,1},{4,7},{7,4},{5,6},{6,5},{8,11},{11,8},{9,1... | collective-permute-start | bytes 2359304 | tf_op jit(solution)/shard_map/ppermute | solution.py:497
  70.1 44.9 %collective-permute-start.3 = (bf16[192,1024]{1,0:T(8,128)(2,1)S(1)}, bf16[192,1024]{1,0:T(8,128)(2,1)S(1)}, u32[]{:S(2)}, u32[]{:S(2)}) collective-permute-start(bf16[192,1024]{1,0:T(8,128)(2,1)S(1)} %get-tuple-element.65.own_ref), channel_id=1, source_target_pairs={{0,3},{3,0},{1,2},{2,1},{4,7},{7,4},{5,6},{6,5},{8,11},{11,8},{9,1... | collective-permute-start | bytes 1179656 | tf_op jit(solution)/shard_map/ppermute | solution.py:497
  70.3 44.7 %copy-start.3 = (bf16[1,256,2048]{2,1,0:T(8,128)(2,1)S(1)}, bf16[1,256,2048]{2,1,0:T(8,128)(2,1)}, u32[]{:S(2)}) copy-start(bf16[1,256,2048]{2,1,0:T(8,128)(2,1)} %param.24) | copy-start | bytes 3145732
  70.3 48.1 %collective-permute-start.5 = (bf16[192,1024]{1,0:T(8,128)(2,1)S(1)}, bf16[192,1024]{1,0:T(8,128)(2,1)S(1)}, u32[]{:S(2)}, u32[]{:S(2)}) collective-permute-start(bf16[192,1024]{1,0:T(8,128)(2,1)S(1)} %get-tuple-element.75.own_ref), channel_id=1, source_target_pairs={{0,3},{3,0},{1,2},{2,1},{4,7},{7,4},{5,6},{6,5},{8,11},{11,8},{9,1... | collective-permute-start | bytes 1179656 | tf_op jit(solution)/shard_map/ppermute | solution.py:497
  96.1 18.9 %copy-start.37 = (bf16[384,2048]{1,0:T(8,128)(2,1)}, bf16[384,2048]{1,0:T(8,128)(2,1)S(1)}, u32[]{:S(2)}) copy-start(bf16[384,2048]{1,0:T(8,128)(2,1)S(1)} %get-tuple-element.62) | copy-start | bytes 4718596
  118.0 9.6 %collective-permute-start.10 = (bf16[192,1024]{1,0:T(8,128)(2,1)S(1)}, bf16[192,1024]{1,0:T(8,128)(2,1)S(1)}, u32[]{:S(2)}, u32[]{:S(2)}) collective-permute-start(bf16[192,1024]{1,0:T(8,128)(2,1)S(1)} %get-tuple-element.92), channel_id=1, source_target_pairs={{0,3},{3,0},{1,2},{2,1},{4,7},{7,4},{5,6},{6,5},{8,11},{11,8},{9,1... | collective-permute-start | bytes 1179656 | tf_op jit(solution)/shard_map/ppermute | solution.py:521
  121.5 14.5 %collective-permute-start.11 = (bf16[192,1024]{1,0:T(8,128)(2,1)S(1)}, bf16[192,1024]{1,0:T(8,128)(2,1)S(1)}, u32[]{:S(2)}, u32[]{:S(2)}) collective-permute-start(bf16[192,1024]{1,0:T(8,128)(2,1)S(1)} %get-tuple-element.93), channel_id=1, source_target_pairs={{0,3},{3,0},{1,2},{2,1},{4,7},{7,4},{5,6},{6,5},{8,11},{11,8},{9,1... | collective-permute-start | bytes 1179656 | tf_op jit(solution)/shard_map/ppermute | solution.py:521
  137.3 12.5 %copy-start.4 = (bf16[2048,256]{1,0:T(8,128)(2,1)S(1)}, bf16[2048,256]{1,0:T(8,128)(2,1)}, u32[]{:S(2)}) copy-start(bf16[2048,256]{1,0:T(8,128)(2,1)} %proj_ref.1) | copy-start | bytes 3145732
  137.3 12.5 %copy-start.10 = (bf16[256,256]{1,0:T(8,128)(2,1)S(1)}, bf16[256,256]{1,0:T(8,128)(2,1)}, u32[]{:S(2)}) copy-start(bf16[256,256]{1,0:T(8,128)(2,1)} %hat_ref.3) | copy-start | bytes 393220
  137.3 12.5 %copy-start.34 = (f32[256]{0:T(256)S(1)}, f32[256]{0:T(256)}, u32[]{:S(2)}) copy-start(f32[256]{0:T(256)} %param.30) | copy-start | bytes 3076
  137.3 33.9 %copy-start.35 = (f32[256]{0:T(256)S(1)}, f32[256]{0:T(256)}, u32[]{:S(2)}) copy-start(f32[256]{0:T(256)} %param.29) | copy-start | bytes 3076
  137.3 38.1 %all-to-all-start.2 = ((bf16[64,24,256]{2,1,0:T(8,128)(2,1)}), bf16[64,24,256]{2,1,0:T(8,128)(2,1)S(1)}, u32[]{:S(2)}, u32[]{:S(2)}) async-start(bf16[64,24,256]{2,1,0:T(8,128)(2,1)} %bitcast.12), calls=%async_computation.2 | async-start | bytes 1572864 | tf_op jit(solution)/shard_map/all_to_all | solution.py:414
  149.7 23.1 %copy-start.25 = (bf16[384,256]{1,0:T(8,128)(2,1)S(1)}, bf16[384,256]{1,0:T(8,128)(2,1)}, u32[]{:S(2)}) copy-start(bf16[384,256]{1,0:T(8,128)(2,1)} %copy-done.24) | copy-start | bytes 589828
  149.9 10.5 %collective-permute-start.15 = (bf16[784,256]{1,0:T(8,128)(2,1)S(1)}, bf16[784,256]{1,0:T(8,128)(2,1)S(1)}, u32[]{:S(2)}, u32[]{:S(2)}) collective-permute-start(bf16[784,256]{1,0:T(8,128)(2,1)S(1)} %get-tuple-element.100), channel_id=1, source_target_pairs={{0,3},{3,0},{1,2},{2,1},{4,7},{7,4},{5,6},{6,5},{8,11},{11,8},{9,1... | collective-permute-start | bytes 1204232 | tf_op jit(solution)/shard_map/ppermute | solution.py:479
  150.1 18.8 %collective-permute-start.13 = (bf16[784,256]{1,0:T(8,128)(2,1)S(1)}, bf16[784,256]{1,0:T(8,128)(2,1)S(1)}, u32[]{:S(2)}, u32[]{:S(2)}) collective-permute-start(bf16[784,256]{1,0:T(8,128)(2,1)S(1)} %get-tuple-element.98), channel_id=1, source_target_pairs={{0,3},{3,0},{1,2},{2,1},{4,7},{7,4},{5,6},{6,5},{8,11},{11,8},{9,1... | collective-permute-start | bytes 1204232 | tf_op jit(solution)/shard_map/ppermute | solution.py:478
  151.4 17.5 %collective-permute-start.14 = (bf16[784,256]{1,0:T(8,128)(2,1)S(1)}, bf16[784,256]{1,0:T(8,128)(2,1)S(1)}, u32[]{:S(2)}, u32[]{:S(2)}) collective-permute-start(bf16[784,256]{1,0:T(8,128)(2,1)S(1)} %get-tuple-element.99), channel_id=1, source_target_pairs={{0,1},{1,0},{2,3},{3,2},{4,5},{5,4},{6,7},{7,6},{8,9},{9,8},{10,11... | collective-permute-start | bytes 1204232 | tf_op jit(solution)/shard_map/ppermute | solution.py:480
  160.4 10.9 %collective-permute-start.16 = (bf16[784,256]{1,0:T(8,128)(2,1)S(1)}, bf16[784,256]{1,0:T(8,128)(2,1)S(1)}, u32[]{:S(2)}, u32[]{:S(2)}) collective-permute-start(bf16[784,256]{1,0:T(8,128)(2,1)S(1)} %collective-permute-done.15), channel_id=1, source_target_pairs={{0,1},{1,0},{2,3},{3,2},{4,5},{5,4},{6,7},{7,6},{8,9},{9,8},{10,11... | collective-permute-start | bytes 1204232 | tf_op jit(solution)/shard_map/ppermute | solution.py:481
  174.2 41.6 %collective-permute-start.8 = (bf16[128,2048]{1,0:T(8,128)(2,1)}, bf16[128,2048]{1,0:T(8,128)(2,1)}, u32[]{:S(2)}, u32[]{:S(2)}) collective-permute-start(bf16[128,2048]{1,0:T(8,128)(2,1)} %convolution_convert_fusion.3), channel_id=1, source_target_pairs={{0,1},{1,0},{2,3},{3,2},{4,5},{5,4},{6,7},{7,6},{8,9},{9,8},{10,11... | collective-permute-start | bytes 1572872 | tf_op jit(solution)/shard_map/ppermute | solution.py:550
  179.6 19.0 %copy-start.23 = (bf16[384,256]{1,0:T(8,128)(2,1)S(1)}, bf16[384,256]{1,0:T(8,128)(2,1)}, u32[]{:S(2)}) copy-start(bf16[384,256]{1,0:T(8,128)(2,1)} %copy-done.22) | copy-start | bytes 589828
  179.6 18.9 %copy-start.38 = (bf16[384,2048]{1,0:T(8,128)(2,1)S(1)}, bf16[384,2048]{1,0:T(8,128)(2,1)}, u32[]{:S(2)}) copy-start(bf16[384,2048]{1,0:T(8,128)(2,1)} %copy-done.37) | copy-start | bytes 4718596
  179.6 11.2 %collective-permute-start.12 = (bf16[256,512]{1,0:T(8,128)(2,1)S(1)}, bf16[256,512]{1,0:T(8,128)(2,1)S(1)}, u32[]{:S(2)}, u32[]{:S(2)}) collective-permute-start(bf16[256,512]{1,0:T(8,128)(2,1)S(1)} %get-tuple-element.96), channel_id=1, source_target_pairs={{0,1},{1,0},{2,3},{3,2},{4,5},{5,4},{6,7},{7,6},{8,9},{9,8},{10,11... | collective-permute-start | bytes 786440 | tf_op jit(solution)/shard_map/ppermute | solution.py:567
  181.3 34.5 %collective-permute-start.9 = (bf16[128,2048]{1,0:T(8,128)(2,1)}, bf16[128,2048]{1,0:T(8,128)(2,1)}, u32[]{:S(2)}, u32[]{:S(2)}) collective-permute-start(bf16[128,2048]{1,0:T(8,128)(2,1)} %convolution_convert_fusion.2), channel_id=1, source_target_pairs={{0,1},{1,0},{2,3},{3,2},{4,5},{5,4},{6,7},{7,6},{8,9},{9,8},{10,11... | collective-permute-start | bytes 1572872 | tf_op jit(solution)/shard_map/ppermute | solution.py:550
  191.4 12.0 %collective-permute-start.17 = (bf16[1024,256]{1,0:T(8,128)(2,1)S(1)}, bf16[1024,256]{1,0:T(8,128)(2,1)S(1)}, u32[]{:S(2)}, u32[]{:S(2)}) collective-permute-start(bf16[1024,256]{1,0:T(8,128)(2,1)S(1)} %get-tuple-element.103), channel_id=1, source_target_pairs={{0,4},{4,0},{8,12},{12,8},{16,20},{20,16},{24,28},{28,24},{32,36},... | collective-permute-start | bytes 1572872 | tf_op jit(solution)/shard_map/ppermute | solution.py:575
  200.3 25.5 %collective-permute-start.7 = (bf16[2048,256]{1,0:T(8,128)(2,1)}, bf16[2048,256]{1,0:T(8,128)(2,1)}, u32[]{:S(2)}, u32[]{:S(2)}) collective-permute-start(bf16[2048,256]{1,0:T(8,128)(2,1)} %convolution_convert_fusion), channel_id=1, source_target_pairs={{0,1},{1,0},{2,3},{3,2},{4,5},{5,4},{6,7},{7,6},{8,9},{9,8},{10,11... | collective-permute-start | bytes 3145736 | tf_op jit(solution)/shard_map/ppermute | solution.py:541
  203.4 66.5 %collective-permute-start.6 = (bf16[2048,256]{1,0:T(8,128)(2,1)}, bf16[2048,256]{1,0:T(8,128)(2,1)}, u32[]{:S(2)}, u32[]{:S(2)}) collective-permute-start(bf16[2048,256]{1,0:T(8,128)(2,1)} %convolution_convert_fusion.1), channel_id=1, source_target_pairs={{0,1},{1,0},{2,3},{3,2},{4,5},{5,4},{6,7},{7,6},{8,9},{9,8},{10,11... | collective-permute-start | bytes 3145736 | tf_op jit(solution)/shard_map/ppermute | solution.py:541
  204.4 53.5 %all-to-all-start.3 = ((bf16[32,32,256]{2,1,0:T(8,128)(2,1)}), bf16[32,32,256]{2,1,0:T(8,128)(2,1)}, u32[]{:S(2)}, u32[]{:S(2)}) async-start(bf16[32,32,256]{2,1,0:T(8,128)(2,1)} %bitcast.16), calls=%async_computation.3 | async-start | bytes 1048576 | tf_op jit(solution)/shard_map/all_to_all | solution.py:414
  219.3 31.1 %collective-permute-start.19 = (bf16[272,256]{1,0:T(8,128)(2,1)S(1)}, bf16[272,256]{1,0:T(8,128)(2,1)S(1)}, u32[]{:S(2)}, u32[]{:S(2)}) collective-permute-start(bf16[272,256]{1,0:T(8,128)(2,1)S(1)} %get-tuple-element.108), channel_id=1, source_target_pairs={{0,1},{1,2},{2,3},{3,0},{4,5},{5,6},{6,7},{7,4},{8,9},{9,10},{10,1... | collective-permute-start | bytes 417800 | tf_op jit(solution)/shard_map/ppermute | solution.py:410
  220.8 30.4 %collective-permute-start.20 = (bf16[272,256]{1,0:T(8,128)(2,1)S(1)}, bf16[272,256]{1,0:T(8,128)(2,1)S(1)}, u32[]{:S(2)}, u32[]{:S(2)}) collective-permute-start(bf16[272,256]{1,0:T(8,128)(2,1)S(1)} %get-tuple-element.109), channel_id=1, source_target_pairs={{0,3},{1,0},{2,1},{3,2},{4,7},{5,4},{6,5},{7,6},{8,11},{9,8},{10,9... | collective-permute-start | bytes 417800 | tf_op jit(solution)/shard_map/ppermute | solution.py:410
  220.8 32.5 %copy-start.29 = (f32[256,128]{1,0:T(8,128)S(1)}, f32[256,128]{1,0:T(8,128)}, u32[]{:S(2)}) copy-start(f32[256,128]{1,0:T(8,128)} %copy-done.28) | copy-start | bytes 393220
  220.8 32.5 %collective-permute-start.21 = (bf16[272,256]{1,0:T(8,128)(2,1)S(1)}, bf16[272,256]{1,0:T(8,128)(2,1)S(1)}, u32[]{:S(2)}, u32[]{:S(2)}) collective-permute-start(bf16[272,256]{1,0:T(8,128)(2,1)S(1)} %get-tuple-element.110), channel_id=1, source_target_pairs={{0,2},{1,3},{2,0},{3,1},{4,6},{5,7},{6,4},{7,5},{8,10},{9,11},{10,... | collective-permute-start | bytes 417800 | tf_op jit(solution)/shard_map/ppermute | solution.py:410
  228.7 41.2 %copy-start.17 = (bf16[384,256]{1,0:T(8,128)(2,1)S(1)}, bf16[384,256]{1,0:T(8,128)(2,1)}, u32[]{:S(2)}) copy-start(bf16[384,256]{1,0:T(8,128)(2,1)} %copy-done.16) | copy-start | bytes 589828
  253.6 19.8 %collective-permute-start.22 = (f32[32,256]{1,0:T(8,128)S(1)}, f32[32,256]{1,0:T(8,128)S(1)}, u32[]{:S(2)}, u32[]{:S(2)}) collective-permute-start(f32[32,256]{1,0:T(8,128)S(1)} %get-tuple-element.113), channel_id=1, source_target_pairs={{4,0},{8,4},{12,8},{16,12},{20,16},{24,20},{28,24},{32,28},{36,32}... | collective-permute-start | bytes 98312 | tf_op jit(solution)/shard_map/ppermute | solution.py:607
  259.0 14.4 %copy-start.30 = (bf16[256,256]{1,0:T(8,128)(2,1)S(1)}, bf16[256,256]{1,0:T(8,128)(2,1)}, u32[]{:S(2)}) copy-start(bf16[256,256]{1,0:T(8,128)(2,1)} %gate_ref.1) | copy-start | bytes 393220
  259.0 14.4 %copy-start.31 = (bf16[256,256]{1,0:T(8,128)(2,1)S(1)}, bf16[256,256]{1,0:T(8,128)(2,1)}, u32[]{:S(2)}) copy-start(bf16[256,256]{1,0:T(8,128)(2,1)} %value_ref.1) | copy-start | bytes 393220
  259.0 14.4 %copy-start.33 = (bf16[31,256]{1,0:T(8,128)(2,1)S(1)}, bf16[31,256]{1,0:T(8,128)(2,1)}, u32[]{:S(2)}) copy-start(bf16[31,256]{1,0:T(8,128)(2,1)} %taps_ref.1) | copy-start | bytes 47620
  259.0 16.4 %collective-permute-start.18 = (f32[32,256]{1,0:T(8,128)S(1)}, f32[32,256]{1,0:T(8,128)S(1)}, u32[]{:S(2)}, u32[]{:S(2)}) collective-permute-start(f32[32,256]{1,0:T(8,128)S(1)} %convert_reduce_fusion), channel_id=1, source_target_pairs={{0,0},{1,64},{2,128},{3,192},{4,4},{5,68},{6,132},{7,196},{8,8},{9... | collective-permute-start | bytes 98312 | tf_op jit(solution)/shard_map/ppermute | solution.py:583
  (24 other events, 76.1 us)

commit v3 on v2

--- a/solution.py
+++ b/solution.py
@@ -91,7 +91,8 @@
     step = 384
     who, part, rank = slot_parts(lax.broadcasted_iota(jnp.int32, (step, TOK), 0))
     base = who * CAP + rank
-    for k in range(SLOTS // step):
+
+    def one(k):
         target = base + (k * (step // 24) * CAP + row_class * SUB)
         hit_first = target == code_first
         hit_second = target == code_second
@@ -107,7 +108,13 @@
                 axis=1,
                 keepdims=True,
             )
-        send_ref[k * step : (k + 1) * step, :] = rows.astype(BF)
+        send_ref[pl.ds(pl.multiple_of(k * step, step), step), :] = rows.astype(BF)
+
+    if weights is None:
+        for k in range(SLOTS // step):
+            one(k)
+    else:
+        pl.loop(0, SLOTS // step)(one)
 
 
 def stacked_quarters(buffer):
@@ -194,7 +201,7 @@
 
 
 def partial_rows(gd, ud, gd2, ud2, wg_ref, wg2_ref, wu_ref, wu2_ref, start):
-    rows = at(start, HALF)
+    rows = at(start, 256)
     return (
         dotg(gd, wg_ref[rows, :], NT)
         + dotg(ud, wu_ref[rows, :], NT)
@@ -246,10 +253,14 @@
 
 def keep_body(gd_ref, gd2_ref, ud_ref, ud2_ref, wg_ref, wg2_ref, wu_ref, wu2_ref, keep_ref):
     _, half, _ = spot()
-    keep_ref[...] = partial_rows(
-        gd_ref[...], ud_ref[...], gd2_ref[...], ud2_ref[...],
-        wg_ref, wg2_ref, wu_ref, wu2_ref, half * HALF,
-    )
+    deltas = gd_ref[...], ud_ref[...], gd2_ref[...], ud2_ref[...]
+
+    @pl.loop(0, 4)
+    def _(k):
+        start = half * HALF + k * 256
+        keep_ref[:, at(k * 256, 256)] = partial_rows(
+            *deltas, wg_ref, wg2_ref, wu_ref, wu2_ref, start
+        )
 
 
 def back_pack_body(keep_ref, first_ref, second_ref, perm_ref, send_ref):

time: 277 us -> 277 us (level)
  transfers between devices with their start and end apart: 27 -> 27, of which waited for: 14 -> 14; matrix products, arithmetic and copies ran while one was open for 6% -> 6% of each run, Pallas kernels for 8% -> 9%
where the time goes in v3:
time: 277 us; the launch traced here: 276 us
  waiting for transfers between devices  135 us (49%)
  starting transfers between devices  84.6 us (31%)
  Pallas kernels  29.6 us (11%)
  matrix products  14 us (5%)
  local copies, waits for them, and re-layouts  7.5 us (3%)
  other arithmetic  3.75 us (1%)
    all_to_all x4, starting transfers between devices, exchanged(): lax.all_to_all(array, SP, split_axis=0, concat_axis=0, tiled=True, **groups)  40.3 us
    all_to_all x4, waiting for transfers between devices, exchanged(): lax.all_to_all(array, SP, split_axis=0, concat_axis=0, tiled=True, **groups)  38.1 us
    pallas_call x18, Pallas kernels, call(): pl.pallas_call(body, out_shape=[jax.ShapeDtypeStruct(s, d) for s, d in ou...  29.6 us
    ppermute x3, waiting for transfers between devices, around(): lax.ppermute(blocks[d], TP, [(i, (i + d) % 4) for i in range(4)])  24.6 us
    ppermute x1, waiting for transfers between devices, on_device(): wu2 = lax.ppermute(wu, TP, PAIR_W)  20.9 us
    ppermute x1, waiting for transfers between devices, on_device(): wd2 = lax.ppermute(wd, TP, PAIR_W)  18.8 us
    dot_general x7, matrix products, outer(): return lax.dot_general(a, b, TN, preferred_element_type=F32)  14 us
    ppermute x1, starting transfers between devices, on_device(): lax.ppermute(piece, (SP, TP), [(s * 4 + t, (per_tp * t + s % per_tp) * 4...  10.9 us
  transfers between devices with their start and end apart: 27, of which 14 were waited for; matrix products, arithmetic and copies ran while one was open for 6% of the time, Pallas kernels for 9%

profile of v3, /device:TPU:17, one launch (start us, length us, event | category | flops | bytes accessed | tf_op | source)
XLA Modules:
  0.0 276.0 jit_solution(2894931258898176117)
XLA Ops:
  0.7 3.7 %shard_map.208 = (bf16[1536,256]{1,0:T(8,128)(2,1)}, s32[2,256]{1,0:T(2,128)}) custom-call(s32[2,256]{1,0:T(2,128)} %bitcast.52, bf16[256,2048]{1,0:T(8,128)(2,1)} %input_ref.1), custom_call_target="tpu_custom_call" | custom-call | flops 805306368 | bytes 1839104 | tf_op jit(solution)/shard_map/pallas_call | solution.py:63
  4.4 12.2 %all-to-all-start = ((bf16[64,24,256]{2,1,0:T(8,128)(2,1)}), bf16[64,24,256]{2,1,0:T(8,128)(2,1)S(1)}, u32[]{:S(2)}, u32[]{:S(2)}) async-start(bf16[64,24,256]{2,1,0:T(8,128)(2,1)} %bitcast.51), calls=%async_computation | async-start | bytes 1572864 | tf_op jit(solution)/shard_map/all_to_all | solution.py:425
  16.6 1.2 copy-done.36
  17.8 1.9 shard_map.211
  20.6 19.0 %all-to-all-done = bf16[64,24,256]{2,1,0:T(8,128)(2,1)S(1)} async-done(((bf16[64,24,256]{2,1,0:T(8,128)(2,1)}), bf16[64,24,256]{2,1,0:T(8,128)(2,1)S(1)}, u32[]{:S(2)}, u32[]{:S(2)}) %all-to-all-start) | async-done | bytes 786464 | tf_op jit(solution)/shard_map/all_to_all | solution.py:425
  39.6 6.1 %all-to-all-start.1 = ((bf16[64,24,256]{2,1,0:T(8,128)(2,1)}), bf16[64,24,256]{2,1,0:T(8,128)(2,1)}, u32[]{:S(2)}, u32[]{:S(2)}) async-start(bf16[64,24,256]{2,1,0:T(8,128)(2,1)} %bitcast.48), calls=%async_computation.1 | async-start | bytes 1572864 | tf_op jit(solution)/shard_map/all_to_all | solution.py:425
  48.2 1.2 shard_map.209.own_ref
  49.5 19.1 %all-to-all-done.1 = bf16[64,24,256]{2,1,0:T(8,128)(2,1)} async-done(((bf16[64,24,256]{2,1,0:T(8,128)(2,1)}), bf16[64,24,256]{2,1,0:T(8,128)(2,1)}, u32[]{:S(2)}, u32[]{:S(2)}) %all-to-all-start.1) | async-done | bytes 786464 | tf_op jit(solution)/shard_map/all_to_all | solution.py:425
  68.6 1.5 shard_map.212
  70.3 1.3 collective-permute-start.5
  71.6 20.9 %collective-permute-done.2.wu2_ref = bf16[2048,256]{1,0:T(8,128)(2,1)} collective-permute-done((bf16[2048,256]{1,0:T(8,128)(2,1)S(1)}, bf16[2048,256]{1,0:T(8,128)(2,1)}, u32[]{:S(2)}, u32[]{:S(2)}) %collective-permute-start.2) | collective-permute-done | bytes 1048608 | tf_op jit(solution)/shard_map/ppermute | solution.py:460
  92.5 3.6 %shard_map.210 = (bf16[384,2048]{1,0:T(8,128)(2,1)S(1)}, f32[192,512]{1,0:T(8,128)S(1)}, f32[192,512]{1,0:T(8,128)S(1)}, f32[192,512]{1,0:T(8,128)S(1)}, f32[192,512]{1,0:T(8,128)S(1)}) custom-call(bf16[384,1024]{1,0:T(8,128)(2,1)} %shard_map.209.own_ref, bf16[384,1024]{1,0:T(8,128)(2,1)S(1)} %collective-permute-done.other_ref, ...), custom_call_target="tpu_custom_call" | custom-call | flops 1610612736 | bytes 8912896 | tf_op jit(solution)/shard_map/pallas_call | solution.py:63
  96.1 18.8 %collective-permute-done.4.wd2_ref = bf16[256,2048]{1,0:T(8,128)(2,1)} collective-permute-done((bf16[256,2048]{1,0:T(8,128)(2,1)}, bf16[256,2048]{1,0:T(8,128)(2,1)}, u32[]{:S(2)}, u32[]{:S(2)}) %collective-permute-start.4) | collective-permute-done | bytes 1048608 | tf_op jit(solution)/shard_map/ppermute | solution.py:461
  115.0 3.0 %shard_map.213 = (bf16[192,2048]{1,0:T(8,128)(2,1)S(1)}, bf16[192,256]{1,0:T(8,128)(2,1)S(1)}, bf16[192,256]{1,0:T(8,128)(2,1)S(1)}, bf16[192,256]{1,0:T(8,128)(...) custom-call(bf16[192,1024]{1,0:T(8,128)(2,1)S(1)} %get-tuple-element, ...), custom_call_target="tpu_custom_call" | custom-call | flops 805306368 | bytes 9633792 | tf_op jit(solution)/shard_map/pallas_call | solution.py:63
  118.5 3.0 %shard_map.214 = (bf16[192,2048]{1,0:T(8,128)(2,1)S(1)}, bf16[192,256]{1,0:T(8,128)(2,1)S(1)}, bf16[192,256]{1,0:T(8,128)(2,1)S(1)}, bf16[192,256]{1,0:T(8,128)(...) custom-call(bf16[192,1024]{1,0:T(8,128)(2,1)S(1)} %get-tuple-element, ...), custom_call_target="tpu_custom_call" | custom-call | flops 805306368 | bytes 9633792 | tf_op jit(solution)/shard_map/pallas_call | solution.py:63
  121.5 1.4 collective-permute-start.11
  123.8 3.6 %shard_map.216.keep_ref = f32[384,1024]{1,0:T(8,128)S(1)} custom-call(bf16[384,256]{1,0:T(8,128)(2,1)S(1)} %get-tuple-element.85.gd_ref, bf16[384,256]{1,0:T(8,128)(2,1)S(1)} %get-tuple-element.86.gd2_ref, bf16[384,256]{1,0:T(8,128)(2,1)S(1)} %get-tuple-element.87.ud_ref, bf16[384,256]{1,0:T(8,128)(2,1)S(1)} %get-tuple-element.88.ud2_ref, ...), custom_call_target="tpu_custom_call" | custom-call | flops 805306368 | bytes 6553600 | tf_op jit(solution)/shard_map/pallas_call | solution.py:63
  127.6 8.4 %collective-permute-done.11.second_ref = bf16[192,1024]{1,0:T(8,128)(2,1)S(1)} collective-permute-done((bf16[192,1024]{1,0:T(8,128)(2,1)S(1)}, bf16[192,1024]{1,0:T(8,128)(2,1)S(1)}, u32[]{:S(2)}, u32[]{:S(2)}) %collective-permute-start.11) | collective-permute-done | bytes 393248 | tf_op jit(solution)/shard_map/ppermute | solution.py:532
  136.0 1.3 shard_map.217
  137.3 12.4 %all-to-all-start.2 = ((bf16[64,24,256]{2,1,0:T(8,128)(2,1)}), bf16[64,24,256]{2,1,0:T(8,128)(2,1)S(1)}, u32[]{:S(2)}, u32[]{:S(2)}) async-start(bf16[64,24,256]{2,1,0:T(8,128)(2,1)} %bitcast.12), calls=%async_computation.2 | async-start | bytes 1572864 | tf_op jit(solution)/shard_map/all_to_all | solution.py:425
  150.1 1.3 collective-permute-start.13
  151.4 3.4 %collective-permute-start.14 = (bf16[784,256]{1,0:T(8,128)(2,1)S(1)}, bf16[784,256]{1,0:T(8,128)(2,1)S(1)}, u32[]{:S(2)}, u32[]{:S(2)}) collective-permute-start(bf16[784,256]{1,0:T(8,128)(2,1)S(1)} %get-tuple-element.99), channel_id=1, source_target_pairs={{0,1},{1,0},{2,3},{3,2},{4,5},{5,4},{6,7},{7,6},{8,9},{9,8},{10,11... | collective-permute-start | bytes 1204232 | tf_op jit(solution)/shard_map/ppermute | solution.py:491
  154.9 5.5 %collective-permute-done.15 = bf16[784,256]{1,0:T(8,128)(2,1)S(1)} collective-permute-done((bf16[784,256]{1,0:T(8,128)(2,1)S(1)}, bf16[784,256]{1,0:T(8,128)(2,1)S(1)}, u32[]{:S(2)}, u32[]{:S(2)}) %collective-permute-start.15) | collective-permute-done | bytes 401440 | tf_op jit(solution)/shard_map/ppermute | solution.py:490
  160.4 3.4 %collective-permute-start.16 = (bf16[784,256]{1,0:T(8,128)(2,1)S(1)}, bf16[784,256]{1,0:T(8,128)(2,1)S(1)}, u32[]{:S(2)}, u32[]{:S(2)}) collective-permute-start(bf16[784,256]{1,0:T(8,128)(2,1)S(1)} %collective-permute-done.15), channel_id=1, source_target_pairs={{0,1},{1,0},{2,3},{3,2},{4,5},{5,4},{6,7},{7,6},{8,9},{9,8},{10,11... | collective-permute-start | bytes 1204232 | tf_op jit(solution)/shard_map/ppermute | solution.py:492
  163.8 5.2 %collective-permute-done.13.across_ref = bf16[784,256]{1,0:T(8,128)(2,1)S(1)} collective-permute-done((bf16[784,256]{1,0:T(8,128)(2,1)S(1)}, bf16[784,256]{1,0:T(8,128)(2,1)S(1)}, u32[]{:S(2)}, u32[]{:S(2)}) %collective-permute-start.13) | collective-permute-done | bytes 401440 | tf_op jit(solution)/shard_map/ppermute | solution.py:489
  169.0 2.3 collective-permute-done.16.opposite_ref
  172.9 1.3 convolution_convert_fusion.3
  174.2 1.3 collective-permute-start.8
  180.0 1.3 convolution_convert_fusion.2
  181.3 1.2 collective-permute-start.9
  182.4 8.4 %collective-permute-done.12.recv_ref = bf16[256,512]{1,0:T(8,128)(2,1)S(1)} collective-permute-done((bf16[256,512]{1,0:T(8,128)(2,1)S(1)}, bf16[256,512]{1,0:T(8,128)(2,1)S(1)}, u32[]{:S(2)}, u32[]{:S(2)}) %collective-permute-start.12) | collective-permute-done | bytes 262176 | tf_op jit(solution)/shard_map/ppermute | solution.py:578
  191.4 6.9 %collective-permute-start.17 = (bf16[1024,256]{1,0:T(8,128)(2,1)S(1)}, bf16[1024,256]{1,0:T(8,128)(2,1)S(1)}, u32[]{:S(2)}, u32[]{:S(2)}) collective-permute-start(bf16[1024,256]{1,0:T(8,128)(2,1)S(1)} %get-tuple-element.103), channel_id=1, source_target_pairs={{0,4},{4,0},{8,12},{12,8},{16,20},{20,16},{24,28},{28,24},{32,36},... | collective-permute-start | bytes 1572872 | tf_op jit(solution)/shard_map/ppermute | solution.py:586
  198.3 1.7 convolution_convert_fusion
  200.0 1.5 collective-permute-start.7
  201.5 1.7 convolution_convert_fusion.1
  204.2 9.7 %all-to-all-start.3 = ((bf16[32,32,256]{2,1,0:T(8,128)(2,1)}), bf16[32,32,256]{2,1,0:T(8,128)(2,1)}, u32[]{:S(2)}, u32[]{:S(2)}) async-start(bf16[32,32,256]{2,1,0:T(8,128)(2,1)} %bitcast.16), calls=%async_computation.3 | async-start | bytes 1048576 | tf_op jit(solution)/shard_map/all_to_all | solution.py:425
  213.8 1.7 fusion.7
  215.5 2.6 fusion.4
  219.1 1.5 collective-permute-start.19
  220.6 1.9 collective-permute-start.21
  222.5 3.0 %collective-permute-done.7 = bf16[2048,256]{1,0:T(8,128)(2,1)} collective-permute-done((bf16[2048,256]{1,0:T(8,128)(2,1)}, bf16[2048,256]{1,0:T(8,128)(2,1)}, u32[]{:S(2)}, u32[]{:S(2)}) %collective-permute-start.7) | collective-permute-done | bytes 1048608 | tf_op jit(solution)/shard_map/ppermute | solution.py:552
  225.5 3.0 %fusion.2 = bf16[1,2048,256]{2,1,0:T(8,128)(2,1)} fusion(bf16[384,2048]{1,0:T(8,128)(2,1)S(1)} %copy-done.39, bf16[384,256]{1,0:T(8,128)(2,1)S(1)} %copy-done.19, bf16[2048,256]{1,0:T(8,128)(2,1)} %collective-permute-done.7), kind=kOutput, calls=%fused_computation.6 | convolution fusion | flops 404226048 | bytes 3866624 | tf_op jit(solution)/shard_map/dot_general | solution.py:548
  228.5 21.6 %collective-permute-done.19.r1_ref = bf16[272,256]{1,0:T(8,128)(2,1)S(1)} collective-permute-done((bf16[272,256]{1,0:T(8,128)(2,1)S(1)}, bf16[272,256]{1,0:T(8,128)(2,1)S(1)}, u32[]{:S(2)}, u32[]{:S(2)}) %collective-permute-start.19) | collective-permute-done | bytes 139296 | tf_op jit(solution)/shard_map/ppermute | solution.py:421
  251.0 2.1 collective-permute-done.21.r3_ref
  253.4 4.5 %collective-permute-start.22 = (f32[32,256]{1,0:T(8,128)S(1)}, f32[32,256]{1,0:T(8,128)S(1)}, u32[]{:S(2)}, u32[]{:S(2)}) collective-permute-start(f32[32,256]{1,0:T(8,128)S(1)} %get-tuple-element.113), channel_id=1, source_target_pairs={{4,0},{8,4},{12,8},{16,12},{20,16},{24,20},{28,24},{32,28},{36,32}... | collective-permute-start | bytes 98312 | tf_op jit(solution)/shard_map/ppermute | solution.py:618
  259.0 10.9 %collective-permute-start.18 = (f32[32,256]{1,0:T(8,128)S(1)}, f32[32,256]{1,0:T(8,128)S(1)}, u32[]{:S(2)}, u32[]{:S(2)}) collective-permute-start(f32[32,256]{1,0:T(8,128)S(1)} %convert_reduce_fusion), channel_id=1, source_target_pairs={{0,0},{1,64},{2,128},{3,192},{4,4},{5,68},{6,132},{7,196},{8,8},{9... | collective-permute-start | bytes 98312 | tf_op jit(solution)/shard_map/ppermute | solution.py:594
  269.9 3.4 %fusion.3 = bf16[1,2048,256]{2,1,0:T(8,128)(2,1)} fusion(bf16[384,2048]{1,0:T(8,128)(2,1)} %copy-done.37, bf16[384,256]{1,0:T(8,128)(2,1)S(1)} %copy-done.17, bf16[2048,256]{1,0:T(8,128)(2,1)} %collective-permute-done.6), kind=kOutput, calls=%fused_computation.7 | convolution fusion | flops 404226048 | bytes 3866624 | tf_op jit(solution)/shard_map/dot_general | solution.py:548
  273.4 2.0 shard_map.225
  (125 shorter events, 17.1 us)
Async XLA Ops:
  0.6 15.9 %copy-start.43 = (f32[256,2]{0,1:T(2,128)S(1)}, f32[256,2]{0,1:T(2,128)}, u32[]{:S(2)}) copy-start(f32[256,2]{0,1:T(2,128)} %param.21) | copy-start | bytes 6148
  0.6 15.9 %copy-start.44 = (f32[256]{0:T(256)S(1)}, f32[256]{0:T(256)}, u32[]{:S(2)}) copy-start(f32[256]{0:T(256)} %param.20) | copy-start | bytes 3076
  4.4 12.2 %copy-start.42 = (s32[2,256]{1,0:T(2,128)S(1)}, s32[2,256]{1,0:T(2,128)}, u32[]{:S(2)}) copy-start(s32[2,256]{1,0:T(2,128)} %get-tuple-element.63.row_ref) | copy-start | bytes 6148
  4.4 35.2 %all-to-all-start = ((bf16[64,24,256]{2,1,0:T(8,128)(2,1)}), bf16[64,24,256]{2,1,0:T(8,128)(2,1)S(1)}, u32[]{:S(2)}, u32[]{:S(2)}) async-start(bf16[64,24,256]{2,1,0:T(8,128)(2,1)} %bitcast.51), calls=%async_computation | async-start | bytes 1572864 | tf_op jit(solution)/shard_map/all_to_all | solution.py:425
  17.8 27.8 %copy-start = (bf16[1,2048,256]{2,1,0:T(8,128)(2,1)S(1)}, bf16[1,2048,256]{2,1,0:T(8,128)(2,1)}, u32[]{:S(2)}) copy-start(bf16[1,2048,256]{2,1,0:T(8,128)(2,1)} %param.22) | copy-start | bytes 3145732
  17.8 28.9 %copy-start.1 = (bf16[1,2048,256]{2,1,0:T(8,128)(2,1)S(1)}, bf16[1,2048,256]{2,1,0:T(8,128)(2,1)}, u32[]{:S(2)}) copy-start(bf16[1,2048,256]{2,1,0:T(8,128)(2,1)} %param.23) | copy-start | bytes 3145732
  17.8 30.4 %copy-start.15 = (bf16[192,192]{1,0:T(8,128)(2,1)S(1)}, bf16[192,192]{1,0:T(8,128)(2,1)}, u32[]{:S(2)}) copy-start(bf16[192,192]{1,0:T(8,128)(2,1)} %constant.6.clone.perm_ref) | copy-start | bytes 221188
  20.6 28.9 %copy-start.40 = (bf16[256,640]{1,0:T(8,128)(2,1)}, bf16[256,640]{1,0:T(8,128)(2,1)S(1)}, u32[]{:S(2)}) copy-start(bf16[256,640]{1,0:T(8,128)(2,1)S(1)} %get-tuple-element.94.cols_ref) | copy-start | bytes 983044
  39.6 29.0 %all-to-all-start.1 = ((bf16[64,24,256]{2,1,0:T(8,128)(2,1)}), bf16[64,24,256]{2,1,0:T(8,128)(2,1)}, u32[]{:S(2)}, u32[]{:S(2)}) async-start(bf16[64,24,256]{2,1,0:T(8,128)(2,1)} %bitcast.48), calls=%async_computation.1 | async-start | bytes 1572864 | tf_op jit(solution)/shard_map/all_to_all | solution.py:425
  45.7 24.7 %collective-permute-start.1 = (bf16[2048,256]{1,0:T(8,128)(2,1)S(1)}, bf16[2048,256]{1,0:T(8,128)(2,1)}, u32[]{:S(2)}, u32[]{:S(2)}) collective-permute-start(bf16[2048,256]{1,0:T(8,128)(2,1)S(1)} %bitcast.33), channel_id=1, source_target_pairs={{0,1},{1,0},{2,3},{3,2},{4,5},{5,4},{6,7},{7,6},{8,9},{9,8},{10,11... | collective-permute-start | bytes 3145736 | tf_op jit(solution)/shard_map/ppermute | solution.py:459
  46.7 45.8 %collective-permute-start.2 = (bf16[2048,256]{1,0:T(8,128)(2,1)S(1)}, bf16[2048,256]{1,0:T(8,128)(2,1)}, u32[]{:S(2)}, u32[]{:S(2)}) collective-permute-start(bf16[2048,256]{1,0:T(8,128)(2,1)S(1)} %bitcast.38), channel_id=1, source_target_pairs={{0,1},{1,0},{2,3},{3,2},{4,5},{5,4},{6,7},{7,6},{8,9},{9,8},{10,11... | collective-permute-start | bytes 3145736 | tf_op jit(solution)/shard_map/ppermute | solution.py:460
  47.2 67.8 %collective-permute-start.4 = (bf16[256,2048]{1,0:T(8,128)(2,1)}, bf16[256,2048]{1,0:T(8,128)(2,1)}, u32[]{:S(2)}, u32[]{:S(2)}) collective-permute-start(bf16[256,2048]{1,0:T(8,128)(2,1)} %bitcast.43), channel_id=1, source_target_pairs={{0,1},{1,0},{2,3},{3,2},{4,5},{5,4},{6,7},{7,6},{8,9},{9,8},{10,11... | collective-permute-start | bytes 3145736 | tf_op jit(solution)/shard_map/ppermute | solution.py:461
  49.5 43.1 %collective-permute-start = (bf16[384,1024]{1,0:T(8,128)(2,1)}, bf16[384,1024]{1,0:T(8,128)(2,1)S(1)}, u32[]{:S(2)}, u32[]{:S(2)}) collective-permute-start(bf16[384,1024]{1,0:T(8,128)(2,1)} %shard_map.209.own_ref), channel_id=1, source_target_pairs={{0,3},{3,0},{1,2},{2,1},{4,7},{7,4},{5,6},{6,5},{8,11},{11,8},{9,1... | collective-permute-start | bytes 2359304 | tf_op jit(solution)/shard_map/ppermute | solution.py:508
  70.1 44.9 %collective-permute-start.3 = (bf16[192,1024]{1,0:T(8,128)(2,1)S(1)}, bf16[192,1024]{1,0:T(8,128)(2,1)S(1)}, u32[]{:S(2)}, u32[]{:S(2)}) collective-permute-start(bf16[192,1024]{1,0:T(8,128)(2,1)S(1)} %get-tuple-element.65.own_ref), channel_id=1, source_target_pairs={{0,3},{3,0},{1,2},{2,1},{4,7},{7,4},{5,6},{6,5},{8,11},{11,8},{9,1... | collective-permute-start | bytes 1179656 | tf_op jit(solution)/shard_map/ppermute | solution.py:508
  70.3 44.7 %copy-start.3 = (bf16[1,256,2048]{2,1,0:T(8,128)(2,1)S(1)}, bf16[1,256,2048]{2,1,0:T(8,128)(2,1)}, u32[]{:S(2)}) copy-start(bf16[1,256,2048]{2,1,0:T(8,128)(2,1)} %param.24) | copy-start | bytes 3145732
  70.3 48.1 %collective-permute-start.5 = (bf16[192,1024]{1,0:T(8,128)(2,1)S(1)}, bf16[192,1024]{1,0:T(8,128)(2,1)S(1)}, u32[]{:S(2)}, u32[]{:S(2)}) collective-permute-start(bf16[192,1024]{1,0:T(8,128)(2,1)S(1)} %get-tuple-element.75.own_ref), channel_id=1, source_target_pairs={{0,3},{3,0},{1,2},{2,1},{4,7},{7,4},{5,6},{6,5},{8,11},{11,8},{9,1... | collective-permute-start | bytes 1179656 | tf_op jit(solution)/shard_map/ppermute | solution.py:508
  96.1 18.9 %copy-start.37 = (bf16[384,2048]{1,0:T(8,128)(2,1)}, bf16[384,2048]{1,0:T(8,128)(2,1)S(1)}, u32[]{:S(2)}) copy-start(bf16[384,2048]{1,0:T(8,128)(2,1)S(1)} %get-tuple-element.62) | copy-start | bytes 4718596
  118.0 9.6 %collective-permute-start.10 = (bf16[192,1024]{1,0:T(8,128)(2,1)S(1)}, bf16[192,1024]{1,0:T(8,128)(2,1)S(1)}, u32[]{:S(2)}, u32[]{:S(2)}) collective-permute-start(bf16[192,1024]{1,0:T(8,128)(2,1)S(1)} %get-tuple-element.92), channel_id=1, source_target_pairs={{0,3},{3,0},{1,2},{2,1},{4,7},{7,4},{5,6},{6,5},{8,11},{11,8},{9,1... | collective-permute-start | bytes 1179656 | tf_op jit(solution)/shard_map/ppermute | solution.py:532
  121.5 14.5 %collective-permute-start.11 = (bf16[192,1024]{1,0:T(8,128)(2,1)S(1)}, bf16[192,1024]{1,0:T(8,128)(2,1)S(1)}, u32[]{:S(2)}, u32[]{:S(2)}) collective-permute-start(bf16[192,1024]{1,0:T(8,128)(2,1)S(1)} %get-tuple-element.93), channel_id=1, source_target_pairs={{0,3},{3,0},{1,2},{2,1},{4,7},{7,4},{5,6},{6,5},{8,11},{11,8},{9,1... | collective-permute-start | bytes 1179656 | tf_op jit(solution)/shard_map/ppermute | solution.py:532
  137.3 12.5 %copy-start.4 = (bf16[2048,256]{1,0:T(8,128)(2,1)S(1)}, bf16[2048,256]{1,0:T(8,128)(2,1)}, u32[]{:S(2)}) copy-start(bf16[2048,256]{1,0:T(8,128)(2,1)} %proj_ref.1) | copy-start | bytes 3145732
  137.3 12.5 %copy-start.10 = (bf16[256,256]{1,0:T(8,128)(2,1)S(1)}, bf16[256,256]{1,0:T(8,128)(2,1)}, u32[]{:S(2)}) copy-start(bf16[256,256]{1,0:T(8,128)(2,1)} %hat_ref.3) | copy-start | bytes 393220
  137.3 12.5 %copy-start.34 = (f32[256]{0:T(256)S(1)}, f32[256]{0:T(256)}, u32[]{:S(2)}) copy-start(f32[256]{0:T(256)} %param.30) | copy-start | bytes 3076
  137.3 33.9 %copy-start.35 = (f32[256]{0:T(256)S(1)}, f32[256]{0:T(256)}, u32[]{:S(2)}) copy-start(f32[256]{0:T(256)} %param.29) | copy-start | bytes 3076
  137.3 38.1 %all-to-all-start.2 = ((bf16[64,24,256]{2,1,0:T(8,128)(2,1)}), bf16[64,24,256]{2,1,0:T(8,128)(2,1)S(1)}, u32[]{:S(2)}, u32[]{:S(2)}) async-start(bf16[64,24,256]{2,1,0:T(8,128)(2,1)} %bitcast.12), calls=%async_computation.2 | async-start | bytes 1572864 | tf_op jit(solution)/shard_map/all_to_all | solution.py:425
  149.7 23.1 %copy-start.25 = (bf16[384,256]{1,0:T(8,128)(2,1)S(1)}, bf16[384,256]{1,0:T(8,128)(2,1)}, u32[]{:S(2)}) copy-start(bf16[384,256]{1,0:T(8,128)(2,1)} %copy-done.24) | copy-start | bytes 589828
  149.9 10.5 %collective-permute-start.15 = (bf16[784,256]{1,0:T(8,128)(2,1)S(1)}, bf16[784,256]{1,0:T(8,128)(2,1)S(1)}, u32[]{:S(2)}, u32[]{:S(2)}) collective-permute-start(bf16[784,256]{1,0:T(8,128)(2,1)S(1)} %get-tuple-element.100), channel_id=1, source_target_pairs={{0,3},{3,0},{1,2},{2,1},{4,7},{7,4},{5,6},{6,5},{8,11},{11,8},{9,1... | collective-permute-start | bytes 1204232 | tf_op jit(solution)/shard_map/ppermute | solution.py:490
  150.1 18.8 %collective-permute-start.13 = (bf16[784,256]{1,0:T(8,128)(2,1)S(1)}, bf16[784,256]{1,0:T(8,128)(2,1)S(1)}, u32[]{:S(2)}, u32[]{:S(2)}) collective-permute-start(bf16[784,256]{1,0:T(8,128)(2,1)S(1)} %get-tuple-element.98), channel_id=1, source_target_pairs={{0,3},{3,0},{1,2},{2,1},{4,7},{7,4},{5,6},{6,5},{8,11},{11,8},{9,1... | collective-permute-start | bytes 1204232 | tf_op jit(solution)/shard_map/ppermute | solution.py:489
  151.4 17.5 %collective-permute-start.14 = (bf16[784,256]{1,0:T(8,128)(2,1)S(1)}, bf16[784,256]{1,0:T(8,128)(2,1)S(1)}, u32[]{:S(2)}, u32[]{:S(2)}) collective-permute-start(bf16[784,256]{1,0:T(8,128)(2,1)S(1)} %get-tuple-element.99), channel_id=1, source_target_pairs={{0,1},{1,0},{2,3},{3,2},{4,5},{5,4},{6,7},{7,6},{8,9},{9,8},{10,11... | collective-permute-start | bytes 1204232 | tf_op jit(solution)/shard_map/ppermute | solution.py:491
  160.4 10.9 %collective-permute-start.16 = (bf16[784,256]{1,0:T(8,128)(2,1)S(1)}, bf16[784,256]{1,0:T(8,128)(2,1)S(1)}, u32[]{:S(2)}, u32[]{:S(2)}) collective-permute-start(bf16[784,256]{1,0:T(8,128)(2,1)S(1)} %collective-permute-done.15), channel_id=1, source_target_pairs={{0,1},{1,0},{2,3},{3,2},{4,5},{5,4},{6,7},{7,6},{8,9},{9,8},{10,11... | collective-permute-start | bytes 1204232 | tf_op jit(solution)/shard_map/ppermute | solution.py:492
  174.2 41.4 %collective-permute-start.8 = (bf16[128,2048]{1,0:T(8,128)(2,1)}, bf16[128,2048]{1,0:T(8,128)(2,1)}, u32[]{:S(2)}, u32[]{:S(2)}) collective-permute-start(bf16[128,2048]{1,0:T(8,128)(2,1)} %convolution_convert_fusion.3), channel_id=1, source_target_pairs={{0,1},{1,0},{2,3},{3,2},{4,5},{5,4},{6,7},{7,6},{8,9},{9,8},{10,11... | collective-permute-start | bytes 1572872 | tf_op jit(solution)/shard_map/ppermute | solution.py:561
  179.6 18.7 %copy-start.23 = (bf16[384,256]{1,0:T(8,128)(2,1)S(1)}, bf16[384,256]{1,0:T(8,128)(2,1)}, u32[]{:S(2)}) copy-start(bf16[384,256]{1,0:T(8,128)(2,1)} %copy-done.22) | copy-start | bytes 589828
  179.6 18.7 %copy-start.38 = (bf16[384,2048]{1,0:T(8,128)(2,1)S(1)}, bf16[384,2048]{1,0:T(8,128)(2,1)}, u32[]{:S(2)}) copy-start(bf16[384,2048]{1,0:T(8,128)(2,1)} %copy-done.37) | copy-start | bytes 4718596
  179.6 11.2 %collective-permute-start.12 = (bf16[256,512]{1,0:T(8,128)(2,1)S(1)}, bf16[256,512]{1,0:T(8,128)(2,1)S(1)}, u32[]{:S(2)}, u32[]{:S(2)}) collective-permute-start(bf16[256,512]{1,0:T(8,128)(2,1)S(1)} %get-tuple-element.96), channel_id=1, source_target_pairs={{0,1},{1,0},{2,3},{3,2},{4,5},{5,4},{6,7},{7,6},{8,9},{9,8},{10,11... | collective-permute-start | bytes 786440 | tf_op jit(solution)/shard_map/ppermute | solution.py:578
  181.3 34.3 %collective-permute-start.9 = (bf16[128,2048]{1,0:T(8,128)(2,1)}, bf16[128,2048]{1,0:T(8,128)(2,1)}, u32[]{:S(2)}, u32[]{:S(2)}) collective-permute-start(bf16[128,2048]{1,0:T(8,128)(2,1)} %convolution_convert_fusion.2), channel_id=1, source_target_pairs={{0,1},{1,0},{2,3},{3,2},{4,5},{5,4},{6,7},{7,6},{8,9},{9,8},{10,11... | collective-permute-start | bytes 1572872 | tf_op jit(solution)/shard_map/ppermute | solution.py:561
  191.4 11.8 %collective-permute-start.17 = (bf16[1024,256]{1,0:T(8,128)(2,1)S(1)}, bf16[1024,256]{1,0:T(8,128)(2,1)S(1)}, u32[]{:S(2)}, u32[]{:S(2)}) collective-permute-start(bf16[1024,256]{1,0:T(8,128)(2,1)S(1)} %get-tuple-element.103), channel_id=1, source_target_pairs={{0,4},{4,0},{8,12},{12,8},{16,20},{20,16},{24,28},{28,24},{32,36},... | collective-permute-start | bytes 1572872 | tf_op jit(solution)/shard_map/ppermute | solution.py:586
  200.0 25.5 %collective-permute-start.7 = (bf16[2048,256]{1,0:T(8,128)(2,1)}, bf16[2048,256]{1,0:T(8,128)(2,1)}, u32[]{:S(2)}, u32[]{:S(2)}) collective-permute-start(bf16[2048,256]{1,0:T(8,128)(2,1)} %convolution_convert_fusion), channel_id=1, source_target_pairs={{0,1},{1,0},{2,3},{3,2},{4,5},{5,4},{6,7},{7,6},{8,9},{9,8},{10,11... | collective-permute-start | bytes 3145736 | tf_op jit(solution)/shard_map/ppermute | solution.py:552
  203.2 66.7 %collective-permute-start.6 = (bf16[2048,256]{1,0:T(8,128)(2,1)}, bf16[2048,256]{1,0:T(8,128)(2,1)}, u32[]{:S(2)}, u32[]{:S(2)}) collective-permute-start(bf16[2048,256]{1,0:T(8,128)(2,1)} %convolution_convert_fusion.1), channel_id=1, source_target_pairs={{0,1},{1,0},{2,3},{3,2},{4,5},{5,4},{6,7},{7,6},{8,9},{9,8},{10,11... | collective-permute-start | bytes 3145736 | tf_op jit(solution)/shard_map/ppermute | solution.py:552
  204.2 53.7 %all-to-all-start.3 = ((bf16[32,32,256]{2,1,0:T(8,128)(2,1)}), bf16[32,32,256]{2,1,0:T(8,128)(2,1)}, u32[]{:S(2)}, u32[]{:S(2)}) async-start(bf16[32,32,256]{2,1,0:T(8,128)(2,1)} %bitcast.16), calls=%async_computation.3 | async-start | bytes 1048576 | tf_op jit(solution)/shard_map/all_to_all | solution.py:425
  219.1 31.1 %collective-permute-start.19 = (bf16[272,256]{1,0:T(8,128)(2,1)S(1)}, bf16[272,256]{1,0:T(8,128)(2,1)S(1)}, u32[]{:S(2)}, u32[]{:S(2)}) collective-permute-start(bf16[272,256]{1,0:T(8,128)(2,1)S(1)} %get-tuple-element.108), channel_id=1, source_target_pairs={{0,1},{1,2},{2,3},{3,0},{4,5},{5,6},{6,7},{7,4},{8,9},{9,10},{10,1... | collective-permute-start | bytes 417800 | tf_op jit(solution)/shard_map/ppermute | solution.py:421
  220.6 30.4 %collective-permute-start.20 = (bf16[272,256]{1,0:T(8,128)(2,1)S(1)}, bf16[272,256]{1,0:T(8,128)(2,1)S(1)}, u32[]{:S(2)}, u32[]{:S(2)}) collective-permute-start(bf16[272,256]{1,0:T(8,128)(2,1)S(1)} %get-tuple-element.109), channel_id=1, source_target_pairs={{0,3},{1,0},{2,1},{3,2},{4,7},{5,4},{6,5},{7,6},{8,11},{9,8},{10,9... | collective-permute-start | bytes 417800 | tf_op jit(solution)/shard_map/ppermute | solution.py:421
  220.6 32.5 %copy-start.29 = (f32[256,128]{1,0:T(8,128)S(1)}, f32[256,128]{1,0:T(8,128)}, u32[]{:S(2)}) copy-start(f32[256,128]{1,0:T(8,128)} %copy-done.28) | copy-start | bytes 393220
  220.6 32.5 %collective-permute-start.21 = (bf16[272,256]{1,0:T(8,128)(2,1)S(1)}, bf16[272,256]{1,0:T(8,128)(2,1)S(1)}, u32[]{:S(2)}, u32[]{:S(2)}) collective-permute-start(bf16[272,256]{1,0:T(8,128)(2,1)S(1)} %get-tuple-element.110), channel_id=1, source_target_pairs={{0,2},{1,3},{2,0},{3,1},{4,6},{5,7},{6,4},{7,5},{8,10},{9,11},{10,... | collective-permute-start | bytes 417800 | tf_op jit(solution)/shard_map/ppermute | solution.py:421
  228.5 41.4 %copy-start.17 = (bf16[384,256]{1,0:T(8,128)(2,1)S(1)}, bf16[384,256]{1,0:T(8,128)(2,1)}, u32[]{:S(2)}) copy-start(bf16[384,256]{1,0:T(8,128)(2,1)} %copy-done.16) | copy-start | bytes 589828
  253.4 20.0 %collective-permute-start.22 = (f32[32,256]{1,0:T(8,128)S(1)}, f32[32,256]{1,0:T(8,128)S(1)}, u32[]{:S(2)}, u32[]{:S(2)}) collective-permute-start(f32[32,256]{1,0:T(8,128)S(1)} %get-tuple-element.113), channel_id=1, source_target_pairs={{4,0},{8,4},{12,8},{16,12},{20,16},{24,20},{28,24},{32,28},{36,32}... | collective-permute-start | bytes 98312 | tf_op jit(solution)/shard_map/ppermute | solution.py:618
  259.0 14.4 %copy-start.30 = (bf16[256,256]{1,0:T(8,128)(2,1)S(1)}, bf16[256,256]{1,0:T(8,128)(2,1)}, u32[]{:S(2)}) copy-start(bf16[256,256]{1,0:T(8,128)(2,1)} %gate_ref.1) | copy-start | bytes 393220
  259.0 14.4 %copy-start.31 = (bf16[256,256]{1,0:T(8,128)(2,1)S(1)}, bf16[256,256]{1,0:T(8,128)(2,1)}, u32[]{:S(2)}) copy-start(bf16[256,256]{1,0:T(8,128)(2,1)} %value_ref.1) | copy-start | bytes 393220
  259.0 14.4 %copy-start.33 = (bf16[31,256]{1,0:T(8,128)(2,1)S(1)}, bf16[31,256]{1,0:T(8,128)(2,1)}, u32[]{:S(2)}) copy-start(bf16[31,256]{1,0:T(8,128)(2,1)} %taps_ref.1) | copy-start | bytes 47620
  259.0 16.4 %collective-permute-start.18 = (f32[32,256]{1,0:T(8,128)S(1)}, f32[32,256]{1,0:T(8,128)S(1)}, u32[]{:S(2)}, u32[]{:S(2)}) collective-permute-start(f32[32,256]{1,0:T(8,128)S(1)} %convert_reduce_fusion), channel_id=1, source_target_pairs={{0,0},{1,64},{2,128},{3,192},{4,4},{5,68},{6,132},{7,196},{8,8},{9... | collective-permute-start | bytes 98312 | tf_op jit(solution)/shard_map/ppermute | solution.py:594
  (24 other events, 79.4 us)
